TPU v7x, 768 devices: a whole 4x8x12 slice. The times are simulated.
768 devices in a mesh: ep: 48 (over z, x), tp: 16 (over y, core).
Axes of the slice: x: 4, y: 8, z: 12, core: 2. Of those that a mesh axis runs over, the one named last changes fastest.
Arguments:
- tokens: bfloat16 [12288, 4096], P('ep', 'tp'), may hold values from -540 to 540
- norm_gain: float32 [4096], P('tp'), may hold values from 0.1 to 1.9
- expert_ids: int32 [12288, 2], P('ep'), may hold values from 0 to 47, all different within a row; in each aligned block of 256 rows (0 to 255, 256 to 511, ...) at most 16 rows name the same one
- expert_weights: float32 [12288, 2], P('ep'), may hold values from 0.1 to 1
- gate_weight: bfloat16 [48, 4096, 2048], P('ep', None, 'tp'), may hold values from -0.09375 to 0.09375
- up_weight: bfloat16 [48, 4096, 2048], P('ep', None, 'tp'), may hold values from -0.09375 to 0.09375
- down_weight: bfloat16 [48, 2048, 4096], P('ep', None, 'tp'), may hold values from -0.125 to 0.125
Outputs:
- mixed: bfloat16 [12288, 4096], P('ep', 'tp')
Inputs may be any that keep to these rules, and one draw needn't show every extreme that they name: `expert_ids`: each row names 2 different experts. Among the rows of one index of ep, no expert is named by more than 16 rows, a bound that some block reaches.
All inputs are finite; a program needn't handle non-finite values.
Results may differ from a plain program's by a relative error of at most 0.007.
Values may be sent and summed in bfloat16 or wider, within the bound.
No kernel may reach another device: no remote copies, remote signals or barrier semaphores. Data moves between devices by JAX's collectives and lax.ppermute only.
A program may use at most 64 MiB of HBM per device.

v0:
```python
import jax
import jax.numpy as jnp
from jax import lax
from jax.sharding import PartitionSpec as P


def copy_for_each(value, axis):
    devices = lax.axis_size(axis)
    return lax.all_to_all(
        jnp.broadcast_to(value[None], (devices, *value.shape)), axis, 0, 0, tiled=True
    )


def taken_together(value, axis):
    everything = copy_for_each(value, axis)
    return jnp.sum(everything, axis=0)


def body(tokens, norm_gain, expert_ids, expert_weights, gate_weight, up_weight, down_weight):
    ep_count = lax.axis_size("ep")
    tp_count = lax.axis_size("tp")
    local_count = gate_weight.shape[0]
    tok_rows, col_width = tokens.shape
    top_count = expert_ids.shape[1]
    experts = local_count * ep_count
    capacity = 3 * tok_rows * top_count // (2 * experts)
    slot_rows = ep_count * capacity
    tok_f32 = tokens.astype(jnp.float32)
    squares = taken_together(jnp.sum(tok_f32 * tok_f32, axis=1), "tp")
    inv_rms = lax.rsqrt(squares / (col_width * tp_count) + 1e-06)
    normed = (tok_f32 * inv_rms[:, None] * norm_gain[None, :]).astype(jnp.bfloat16)
    flat_ids = expert_ids.reshape(-1)
    onehot = (flat_ids[:, None] == jnp.arange(experts, dtype=jnp.int32)[None, :]).astype(jnp.int32)
    earlier = jnp.cumsum(onehot, axis=0) - onehot
    slot_idx = jnp.sum(earlier * onehot, axis=1)
    target = flat_ids // local_count
    member_idx = flat_ids % local_count
    row_index = member_idx * slot_rows + target * capacity + slot_idx
    token_idx = jnp.arange(tok_rows * top_count, dtype=jnp.int32) // top_count
    outgoing = (
        jnp.zeros((local_count * slot_rows, col_width), jnp.bfloat16)
        .at[row_index]
        .set(normed[token_idx])
    )
    outgoing = outgoing.reshape(local_count, slot_rows, col_width)
    arrived = lax.all_to_all(outgoing, "ep", split_axis=1, concat_axis=1, tiled=True)
    block_part = lax.all_gather(arrived, "tp", axis=2, tiled=True)
    gate_new = jnp.einsum(
        "erd,edf->erf", block_part, gate_weight, preferred_element_type=jnp.float32
    )
    up_new = jnp.einsum("erd,edf->erf", block_part, up_weight, preferred_element_type=jnp.float32)
    hidden = (jax.nn.silu(gate_new) * up_new).astype(jnp.bfloat16)
    produced = jnp.einsum(
        "erf,efd->erd",
        lax.all_gather(hidden, "tp", axis=2, tiled=True),
        down_weight,
        preferred_element_type=jnp.float32,
    )
    returned = lax.all_to_all(
        produced.astype(jnp.bfloat16), "ep", split_axis=1, concat_axis=1, tiled=True
    )
    picked = returned.reshape(local_count * slot_rows, col_width)[row_index].astype(jnp.float32)
    picked = picked.reshape(tok_rows, top_count, col_width)
    mixed = jnp.sum(picked * expert_weights[:, :, None], axis=1)
    return mixed.astype(jnp.bfloat16)


def solution(mesh):
    in_specs = (
        P("ep", "tp"),
        P("tp"),
        P("ep", None),
        P("ep", None),
        P("ep", None, "tp"),
        P("ep", None, "tp"),
        P("ep", None, "tp"),
    )
    out_specs = P("ep", "tp")
    return jax.shard_map(body, mesh=mesh, in_specs=in_specs, out_specs=out_specs, check_vma=False)
```

profile of v0, /device:TPU:1, one launch (start us, length us, event | category | flops | bytes accessed | tf_op | source)
XLA Modules:
  0.0 235.0 jit_solution(7820353611331967869)
XLA Ops:
  6.5 1.2 fusion.14
  7.7 0.6 broadcast_in_dim.5
  8.3 13.8 %all-to-all-start = ((f32[16,1,256]{2,1,0:T(1,128)}), f32[16,1,256]{2,1,0:T(1,128)S(1)}, u32[]{:S(2)}, u32[]{:S(2)}) async-start(f32[16,1,256]{2,1,0:T(1,128)} %broadcast_in_dim.5), calls=%async_computation | async-start | bytes 32768 | tf_op jit(solution)/shard_map/all_to_all | solution.py:9
  22.1 0.8 copy.37
  23.2 0.7 broadcast_multiply_fusion
  24.0 1.2 reduce-window.6
  25.9 3.6 %all-to-all-done = f32[16,1,256]{2,1,0:T(1,128)S(1)} async-done(((f32[16,1,256]{2,1,0:T(1,128)}), f32[16,1,256]{2,1,0:T(1,128)S(1)}, u32[]{:S(2)}, u32[]{:S(2)}) %all-to-all-start) | async-done | bytes 16416 | tf_op jit(solution)/shard_map/all_to_all | solution.py:9
  29.5 1.0 fusion.16
  30.5 3.9 %scatter_custom_fusion = bf16[768,256]{1,0:T(8,128)(2,1)S(1)} fusion(s32[512]{0:T(512)S(1)} %bitcast.61, bf16[256,256]{1,0:T(8,128)(2,1)S(1)} %fusion.16, s32[1024]{0:T(1024)S(1)} %pad_clamp_fusion.1, bf16[]{:T(256)} %constant.49.clone.1), kind=kCustom, calls=%fused_computation.21 | custom fusion | bytes 393218 | tf_op jit(solution)/shard_map/scatter | solution.py:43
  34.4 0.6 copy.54
  35.5 3.1 %reduce.3 = bf16[768,256]{1,0:T(8,128)(2,1)S(1)} reduce(bf16[768,1,256]{2,1,0:T(2,128)(2,1)S(1)} %bitcast.56, bf16[]{:T(256)} %broadcast.166), dimensions={1}, to_apply=%bitcast.54.reduce_sub_computation | reduce | bytes 786434
  38.7 32.5 %all_to_all.16 = bf16[48,2,2048]{2,1,0:T(2,128)(2,1)S(1)} all-to-all(bf16[48,2,2048]{2,1,0:T(2,128)(2,1)S(1)} %reshape.182), channel_id=1, replica_groups=mesh['ep'=48,'tp'=16] {'ep'}, dimensions={0} | all-to-all | bytes 786432 | tf_op jit(solution)/shard_map/all_to_all | solution.py:46
  71.6 0.8 copy.42
  72.7 54.5 %all-gather.4.cloned.1.call-done = bf16[1,768,4096]{2,1,0:T(8,128)(2,1)} async-done(((bf16[1,768,256]{2,1,0:T(8,128)(2,1)}), bf16[1,768,4096]{2,1,0:T(8,128)(2,1)}) %all-gather.4.cloned.1.call-update) | async-done | bytes 6291472 | tf_op jit(solution)/shard_map/all_gather | solution.py:47
  127.2 4.7 %fusion.2 = f32[768,128]{1,0:T(8,128)S(1)} fusion(bf16[1,768,4096]{2,1,0:T(8,128)(2,1)} %all-gather.4.cloned.1.call-done, bf16[1,4096,128]{2,1,0:T(8,128)(2,1)S(1)} %copy-done.3), kind=kOutput, calls=%fused_computation.5 | convolution fusion | flops 805306368 | bytes 7733248 | tf_op jit(solution)/shard_map/erd,edf->erf/dot_general | solution.py:48
  132.0 2.5 %fusion.8 = bf16[768,128]{1,0:T(8,128)(2,1)} fusion(bf16[1,768,4096]{2,1,0:T(8,128)(2,1)S(1)} %copy-done.2, bf16[1,4096,128]{2,1,0:T(8,128)(2,1)S(1)} %copy-done.4, f32[768,128]{1,0:T(8,128)S(1)} %fusion.2), kind=kOutput, calls=%fused_computation.10 | convolution fusion | flops 805896192 | bytes 7929856 | tf_op jit(solution)/shard_map/erd,edf->erf/dot_general | solution.py:51
  134.5 49.9 %all-gather.6.cloned.1.call-done = bf16[768,2048]{1,0:T(8,128)(2,1)} async-done(((bf16[768,128]{1,0:T(8,128)(2,1)}), bf16[768,2048]{1,0:T(8,128)(2,1)}) %all-gather.6.cloned.1.call-update) | async-done | bytes 3145744 | tf_op jit(solution)/shard_map/all_gather | solution.py:55
  184.4 2.9 %fusion.4 = bf16[1,768,256]{2,1,0:T(8,128)(2,1)S(1)} fusion(bf16[768,2048]{1,0:T(8,128)(2,1)} %all-gather.6.cloned.1.call-done, bf16[1,2048,256]{2,1,0:T(8,128)(2,1)S(1)} %copy-done), kind=kOutput, calls=%fused_computation.8 | convolution fusion | flops 805502976 | bytes 4587520 | tf_op jit(solution)/shard_map/erf,efd->erd/dot_general | solution.py:53
  187.9 3.1 %reduce.4 = bf16[768,256]{1,0:T(8,128)(2,1)S(1)} reduce(bf16[768,1,256]{2,1,0:T(2,128)(2,1)S(1)} %bitcast.57, bf16[]{:T(256)} %broadcast.166), dimensions={1}, to_apply=%bitcast.53.reduce_sub_computation | reduce | bytes 786434
  191.0 0.8 reshape.184
  191.8 12.4 %all-to-all-start.2 = ((bf16[48,2,2048]{2,1,0:T(2,128)(2,1)}), bf16[48,2,2048]{2,1,0:T(2,128)(2,1)S(1)}, u32[]{:S(2)}, u32[]{:S(2)}) async-start(bf16[48,2,2048]{2,1,0:T(2,128)(2,1)} %reshape.184), calls=%async_computation.2 | async-start | bytes 786432 | tf_op jit(solution)/shard_map/all_to_all | solution.py:59
  204.4 19.7 %all-to-all-done.2 = bf16[48,2,2048]{2,1,0:T(2,128)(2,1)S(1)} async-done(((bf16[48,2,2048]{2,1,0:T(2,128)(2,1)}), bf16[48,2,2048]{2,1,0:T(2,128)(2,1)S(1)}, u32[]{:S(2)}, u32[]{:S(2)}) %all-to-all-start.2) | async-done | bytes 393248 | tf_op jit(solution)/shard_map/all_to_all | solution.py:59
  224.5 2.0 gather_fusion
  226.8 1.4 multiply_reduce_fusion
  (37 shorter events, 3.8 us)
Async XLA Ops:
  6.5 177.8 %copy-start = (bf16[1,2048,256]{2,1,0:T(8,128)(2,1)S(1)}, bf16[1,2048,256]{2,1,0:T(8,128)(2,1)}, u32[]{:S(2)}) copy-start(bf16[1,2048,256]{2,1,0:T(8,128)(2,1)} %param.13) | copy-start | bytes 3145732
  6.5 120.7 %copy-start.3 = (bf16[1,4096,128]{2,1,0:T(8,128)(2,1)S(1)}, bf16[1,4096,128]{2,1,0:T(8,128)(2,1)}, u32[]{:S(2)}) copy-start(bf16[1,4096,128]{2,1,0:T(8,128)(2,1)} %param.11) | copy-start | bytes 3145732
  8.3 21.1 %all-to-all-start = ((f32[16,1,256]{2,1,0:T(1,128)}), f32[16,1,256]{2,1,0:T(1,128)S(1)}, u32[]{:S(2)}, u32[]{:S(2)}) async-start(f32[16,1,256]{2,1,0:T(1,128)} %broadcast_in_dim.5), calls=%async_computation | async-start | bytes 32768 | tf_op jit(solution)/shard_map/all_to_all | solution.py:9
  22.1 105.1 %all-gather.4.cloned.1.call-start = ((), (), s32[]{:S(2)}) async-start(), calls=%async_computation.3 | async-start | bytes 6684672 | tf_op jit(solution)/shard_map/all_gather | solution.py:47
  72.4 59.5 %copy-start.4 = (bf16[1,4096,128]{2,1,0:T(8,128)(2,1)S(1)}, bf16[1,4096,128]{2,1,0:T(8,128)(2,1)}, u32[]{:S(2)}) copy-start(bf16[1,4096,128]{2,1,0:T(8,128)(2,1)} %param.12) | copy-start | bytes 3145732
  72.5 111.9 %all-gather.6.cloned.1.call-start = ((), (), s32[]{:S(2)}) async-start(), calls=%async_computation.4 | async-start | bytes 3342336 | tf_op jit(solution)/shard_map/all_gather | solution.py:55
  127.2 4.7 %copy-start.2 = (bf16[1,768,4096]{2,1,0:T(8,128)(2,1)S(1)}, bf16[1,768,4096]{2,1,0:T(8,128)(2,1)}, u32[]{:S(2)}) copy-start(bf16[1,768,4096]{2,1,0:T(8,128)(2,1)} %all-gather.4.cloned.1.call-done) | copy-start | bytes 18874372
  134.5 69.7 %copy-start.1 = (f32[256,2]{0,1:T(2,128)S(1)}, f32[256,2]{0,1:T(2,128)}, u32[]{:S(2)}) copy-start(f32[256,2]{0,1:T(2,128)} %param.10) | copy-start | bytes 6148
  191.8 32.2 %all-to-all-start.2 = ((bf16[48,2,2048]{2,1,0:T(2,128)(2,1)}), bf16[48,2,2048]{2,1,0:T(2,128)(2,1)S(1)}, u32[]{:S(2)}, u32[]{:S(2)}) async-start(bf16[48,2,2048]{2,1,0:T(2,128)(2,1)} %reshape.184), calls=%async_computation.2 | async-start | bytes 786432 | tf_op jit(solution)/shard_map/all_to_all | solution.py:59
Sparse Core Ops, SparseCore 0:
  72.6 54.6 all-gather.3
  134.6 49.7 all-gather.5
where the time goes:
time: 237 us; the launch traced here: 235 us
  waiting for transfers between devices  128 us (54%)
  blocking collectives  32.5 us (14%)
  starting transfers between devices  26.4 us (11%)
  between operations  13.6 us (6%)
  local copies, waits for them, and re-layouts  12.8 us (5%)
  other arithmetic  11.9 us (5%)
  matrix products  10.1 us (4%)
    all_gather x1, waiting for transfers between devices, body(): block_part = lax.all_gather(arrived, 'tp', axis=2, tiled=True)  54.5 us
    all_gather x1, waiting for transfers between devices, body(): lax.all_gather(hidden, 'tp', axis=2, tiled=True)  49.9 us
    all_to_all x1, blocking collectives, body(): lax.all_to_all(outgoing, 'ep', split_axis=1, concat_axis=1, tiled=True)  32.5 us
    all_to_all x1, waiting for transfers between devices, body(): lax.all_to_all(produced.astype(jnp.bfloat16), 'ep', split_axis=1, concat_...  19.7 us
    all_to_all x1, starting transfers between devices, copy_for_each(): lax.all_to_all(jnp.broadcast_to(value[None], (devices, *value.shape)), ax...  13.8 us
    all_to_all x1, starting transfers between devices, body(): lax.all_to_all(produced.astype(jnp.bfloat16), 'ep', split_axis=1, concat_...  12.4 us
    unnamed x2, other arithmetic  6.23 us
  transfers between devices with their start and end apart: 4, of which 4 were waited for; matrix products, arithmetic and copies ran while one was open for 2% of the time, Pallas kernels for 0%

commit v1 on v0

v1 whole, which is shorter than its diff:
```python
import functools

import jax
import jax.numpy as jnp
from jax import lax
from jax.experimental import pallas as pl
from jax.experimental.pallas import tpu as pltpu
from jax.sharding import Mesh, PartitionSpec as P

BF = jnp.bfloat16
F32 = jnp.float32
VM = pl.BlockSpec(memory_space=pltpu.VMEM)
SM = pl.BlockSpec(memory_space=pltpu.SMEM)
STEPS = (0, 1, -1, 2, -2, 3, -3, 4)
PAD = 8


def dot(a, b):
    return jnp.dot(a, b, preferred_element_type=F32)


def dispatch_kernel(experts, cap, ids_ref, tok_ref, out_ref, pick_ref):
    rows = tok_ref.shape[0]
    expert = lax.broadcasted_iota(jnp.int32, (experts, rows), 0)
    named = (expert == ids_ref[0:1, :]) | (expert == ids_ref[1:2, :])
    before = lax.broadcasted_iota(jnp.int32, (rows, rows), 0) < lax.broadcasted_iota(
        jnp.int32, (rows, rows), 1
    )
    rank = dot(named.astype(F32).astype(BF), before.astype(F32).astype(BF))
    rank = jnp.where(named, rank, -1.0)
    slot = lax.broadcasted_iota(jnp.int32, (cap, rows), 0).astype(F32)
    for e in range(experts):
        pick_ref[e * cap : (e + 1) * cap, :] = (
            (rank[e : e + 1, :] == slot).astype(F32).astype(BF)
        )
    out_ref[...] = dot(pick_ref[...], tok_ref[...]).astype(BF)


def combine_kernel(experts, cap, ids_ref, weight_ref, back_ref, out_ref):
    rows = out_ref.shape[0]
    line = lax.broadcasted_iota(jnp.int32, (8, rows), 0)
    table = jnp.where(line == 0, ids_ref[0:1, :].astype(F32), 0.0)
    table = jnp.where(line == 1, ids_ref[1:2, :].astype(F32), table)
    table = jnp.where(line == 2, weight_ref[0:1, :], table)
    table = jnp.where(line == 3, weight_ref[1:2, :], table)
    column = table.T
    first, second = column[:, 0:1], column[:, 1:2]
    lanes = lax.broadcasted_iota(jnp.int32, (rows, 128), 1).astype(F32)
    named = (lanes == first) | (lanes == second)
    after = lax.broadcasted_iota(jnp.int32, (rows, rows), 1) < lax.broadcasted_iota(
        jnp.int32, (rows, rows), 0
    )
    rank = dot(after.astype(F32).astype(BF), named.astype(F32).astype(BF))
    place = lax.broadcasted_iota(jnp.int32, (rows, experts * cap), 1).astype(F32)
    total = None
    for k, name in enumerate((first, second)):
        mine = jnp.sum(jnp.where(lanes == name, rank, 0.0), axis=1, keepdims=True)
        pick = (place == name * cap + mine).astype(F32).astype(BF)
        term = dot(pick, back_ref[...]) * column[:, 2 + k : 3 + k]
        total = term if total is None else total + term
    out_ref[...] = total.astype(BF)


def pack_kernel(where_ref, came_ref, gain_ref, peer_gain_ref, out_ref):
    sources = came_ref.shape[0] // 2
    width = came_ref.shape[2]
    for s in range(sources):
        for c in range(2):
            out_ref[s * 8 : s * 8 + 8, c * width : (c + 1) * width] = came_ref[2 * s + c]
    core = where_ref[1]
    mine, other = gain_ref[...], peer_gain_ref[...]
    gain = jnp.concatenate(
        [jnp.where(core == 0, mine, other), jnp.where(core == 0, other, mine)], axis=1
    )
    top = gain.astype(BF).astype(F32)
    mid = (gain - top).astype(BF).astype(F32)
    low = gain - top - mid
    line = lax.broadcasted_iota(jnp.int32, (PAD, 2 * width), 0)
    split = jnp.where(line == 0, top, jnp.where(line == 1, mid, jnp.where(line == 2, low, 0.0)))
    out_ref[sources * 8 : sources * 8 + PAD, :] = split.astype(BF)


def source_of(where_ref, step, count):
    turn = 1 - 2 * where_ref[1]
    return lax.rem(where_ref[0] - step * turn + 2 * count, count)


def hidden_kernel(count, where_ref, *refs):
    blocks, (gate_ref, gate2_ref, up_ref, up2_ref, out_ref, gsum, usum, square) = refs[:8], refs[8:]
    rows, half = out_ref.shape[0], gate_ref.shape[1]
    depth = blocks[0].shape[1]
    for number, (step, block) in enumerate(zip(STEPS, blocks)):
        start = pl.multiple_of(source_of(where_ref, step, count) * depth, depth)
        gain = jnp.sum(block[rows : rows + PAD, :].astype(F32), axis=0, keepdims=True)
        raw = block[0:rows, :].astype(F32)
        squares = raw * raw
        part = squares[:, 0:128]
        for lane in range(128, depth, 128):
            part = part + squares[:, lane : lane + 128]
        scaled = (raw * gain).astype(BF)
        gate = jnp.concatenate([gate_ref[pl.ds(start, depth), :], gate2_ref[pl.ds(start, depth), :]], axis=1)
        up = jnp.concatenate([up_ref[pl.ds(start, depth), :], up2_ref[pl.ds(start, depth), :]], axis=1)
        if number == 0:
            square[...] = part
            gsum[...] = dot(scaled, gate)
            usum[...] = dot(scaled, up)
        else:
            square[...] += part
            gsum[...] += dot(scaled, gate)
            usum[...] += dot(scaled, up)
    mean = jnp.sum(square[...], axis=1, keepdims=True) / (depth * count)
    scale = lax.rsqrt(mean + 1e-06)
    gate, up = gsum[...] * scale, usum[...] * scale
    hidden = (gate / (1.0 + jnp.exp(-gate)) * up).astype(BF)
    core = where_ref[1]
    out_ref[:, pl.ds(pl.multiple_of(core * half, half), half)] = hidden[:, :half]
    out_ref[:, pl.ds(pl.multiple_of((1 - core) * half, half), half)] = hidden[:, half:]


def down_kernel(count, where_ref, *refs):
    blocks, (down_ref, down2_ref, out_ref, mine, other) = refs[:8], refs[8:]
    depth = blocks[0].shape[1]
    for number, (step, block) in enumerate(zip(STEPS, blocks)):
        start = pl.multiple_of(source_of(where_ref, step, count) * depth, depth)
        first = dot(block[...], down_ref[pl.ds(start, depth), :])
        second = dot(block[...], down2_ref[pl.ds(start, depth), :])
        if number == 0:
            mine[...] = first
            other[...] = second
        else:
            mine[...] += first
            other[...] += second
    core = where_ref[1]
    for s in range(out_ref.shape[0]):
        out_ref[s, core] = mine[s * 8 : s * 8 + 8, :].astype(BF)
        out_ref[s, 1 - core] = other[s * 8 : s * 8 + 8, :].astype(BF)


def ring(block, count):
    def perm(sign):
        return [
            (y * 2 + c, (y + sign * (1 - 2 * c)) % count * 2 + c) for y in range(count) for c in range(2)
        ]

    main = other = block
    found = [block]
    for k in range(3):
        main = lax.ppermute(main, ("y", "c"), perm(1))
        other = lax.ppermute(other, ("y", "c"), perm(-1))
        found += [main, other]
    found.append(lax.ppermute(main, ("y", "c"), perm(1)))
    return found


def swap(value):
    return lax.ppermute(value, "c", [(0, 1), (1, 0)])


def body(tokens, norm_gain, expert_ids, expert_weights, gate_weight, up_weight, down_weight):
    count = lax.axis_size("y")
    experts = lax.axis_size("z") * lax.axis_size("x")
    rows, width = tokens.shape
    cap = 3 * rows * expert_ids.shape[1] // (2 * experts)
    half = experts * cap // 2
    where = jnp.stack([lax.axis_index("y"), lax.axis_index("c")]).astype(jnp.int32)
    ids = expert_ids.T
    call = functools.partial(pl.pallas_call)

    outgoing = call(
        functools.partial(dispatch_kernel, experts, cap),
        out_shape=jax.ShapeDtypeStruct((experts * cap, width), BF),
        in_specs=[VM, VM],
        out_specs=VM,
        scratch_shapes=[pltpu.VMEM((experts * cap, rows), BF)],
        name="dispatch",
    )(ids, tokens)
    came = lax.all_to_all(outgoing.reshape(2 * experts, 8, width), ("z", "x", "c"), 0, 0, tiled=True)

    gain = norm_gain[None, :]
    block = call(
        pack_kernel,
        out_shape=jax.ShapeDtypeStruct((half + PAD, 2 * width), BF),
        in_specs=[SM, VM, VM, VM],
        out_specs=VM,
        name="pack",
    )(where, came, gain, swap(gain))
    found = ring(block, count)

    gate, up, down = gate_weight[0], up_weight[0], down_weight[0]
    ff = gate.shape[1]
    hidden = call(
        functools.partial(hidden_kernel, count),
        out_shape=jax.ShapeDtypeStruct((half, 2 * ff), BF),
        in_specs=[SM] + [VM] * 12,
        out_specs=VM,
        scratch_shapes=[
            pltpu.VMEM((half, 2 * ff), F32),
            pltpu.VMEM((half, 2 * ff), F32),
            pltpu.VMEM((half, 128), F32),
        ],
        compiler_params=pltpu.CompilerParams(vmem_limit_bytes=40 << 20),
        name="hidden",
    )(where, *found, gate, swap(gate), up, swap(up))
    found = ring(hidden, count)

    made = call(
        functools.partial(down_kernel, count),
        out_shape=jax.ShapeDtypeStruct((experts, 2, 8, width), BF),
        in_specs=[SM] + [VM] * 10,
        out_specs=VM,
        scratch_shapes=[pltpu.VMEM((half, width), F32), pltpu.VMEM((half, width), F32)],
        compiler_params=pltpu.CompilerParams(vmem_limit_bytes=40 << 20),
        name="down",
    )(where, *found, down, swap(down))
    back = lax.all_to_all(made.reshape(2 * experts, 8, width), ("z", "x", "c"), 0, 0, tiled=True)

    return call(
        functools.partial(combine_kernel, experts, cap),
        out_shape=jax.ShapeDtypeStruct((rows, width), BF),
        in_specs=[VM, VM, VM],
        out_specs=VM,
        name="combine",
    )(ids, expert_weights.T, back.reshape(experts * cap, width))


def solution(mesh):
    split = Mesh(mesh.devices.reshape(12, 4, 8, 2), ("z", "x", "y", "c"))
    ep, tp = ("z", "x"), ("y", "c")
    in_specs = (
        P(ep, tp),
        P(tp),
        P(ep, None),
        P(ep, None),
        P(ep, None, tp),
        P(ep, None, tp),
        P(ep, None, tp),
    )
    return jax.shard_map(body, mesh=split, in_specs=in_specs, out_specs=P(ep, tp), check_vma=False)
```

time: 237 us -> 172 us (0.73)
  waiting for transfers between devices: 128 us -> 41.1 us
  starting transfers between devices: 26.4 us -> 84 us
  between operations: 13.6 us -> 0.26 us
  other arithmetic: 11.9 us -> 0.58 us
  local copies, waits for them, and re-layouts: 12.8 us -> 1.76 us
  Pallas kernels: 0 us -> 10.8 us
  matrix products: 10.1 us -> 0 us
    all_gather x2 -> x0, waiting for transfers between devices: 104 us -> none  [the longest x1 54.5 us: body(): block_part = lax.all_gather(arrived, 'tp', axis=2, tiled=True)]
    ppermute x0 -> x18, starting transfers between devices: none -> 64 us  [the longest x6 25.8 us: ring(): main = lax.ppermute(main, ('y', 'c'), perm(1))]
    ppermute x0 -> x18, waiting for transfers between devices: none -> 23.2 us  [the longest x2 10.6 us: ring(): found.append(lax.ppermute(main, ('y', 'c'), perm(1)))]
    pallas_call x0 -> x5, Pallas kernels: none -> 10.8 us  [the longest x1 2.69 us: body(): call(functools.partial(combine_kernel, experts, cap), out_shape=jax.Shape...]
    dot_general x3 -> x0, matrix products: 10.1 us -> none  [the longest x1 4.72 us: body(): jnp.einsum('erd,edf->erf', block_part, gate_weight, preferred_element_typ...]
    unnamed x2 -> x0, other arithmetic: 6.23 us -> none
    all_to_all x2 -> x1, starting transfers between devices: 26.1 us -> 20 us  [body(): lax.all_to_all(outgoing.reshape(2 * experts, 8, width), ('z', 'x', 'c'),...]
    all_to_all x2 -> x1, waiting for transfers between devices: 23.3 us -> 17.9 us  [body(): lax.all_to_all(outgoing.reshape(2 * experts, 8, width), ('z', 'x', 'c'),...]
  transfers between devices with their start and end apart: 4 -> 19, of which waited for: 4 -> 12; matrix products, arithmetic and copies ran while one was open for 2% -> 0% of each run, Pallas kernels for 0% -> 2%
where the time goes in v1:
time: 172 us; the launch traced here: 170 us
  starting transfers between devices  84 us (49%)
  waiting for transfers between devices  41.1 us (24%)
  blocking collectives  31.4 us (18%)
  Pallas kernels  10.8 us (6%)
  local copies, waits for them, and re-layouts  1.76 us (1%)
    all_to_all x1, blocking collectives, body(): lax.all_to_all(made.reshape(2 * experts, 8, width), ('z', 'x', 'c'), 0, 0...  31.4 us
    ppermute x6, starting transfers between devices, ring(): main = lax.ppermute(main, ('y', 'c'), perm(1))  25.8 us
    ppermute x6, starting transfers between devices, ring(): other = lax.ppermute(other, ('y', 'c'), perm(-1))  20.7 us
    all_to_all x1, starting transfers between devices, body(): lax.all_to_all(outgoing.reshape(2 * experts, 8, width), ('z', 'x', 'c'),...  20 us
    all_to_all x1, waiting for transfers between devices, body(): lax.all_to_all(outgoing.reshape(2 * experts, 8, width), ('z', 'x', 'c'),...  17.9 us
    ppermute x4, starting transfers between devices, swap(): return lax.ppermute(value, 'c', [(0, 1), (1, 0)])  11.6 us
    ppermute x2, waiting for transfers between devices, ring(): found.append(lax.ppermute(main, ('y', 'c'), perm(1)))  10.6 us
    ppermute x6, waiting for transfers between devices, ring(): other = lax.ppermute(other, ('y', 'c'), perm(-1))  6.39 us
  transfers between devices with their start and end apart: 19, of which 12 were waited for; matrix products, arithmetic and copies ran while one was open for 0% of the time, Pallas kernels for 2%

profile of v1, /device:TPU:1, one launch (start us, length us, event | category | flops | bytes accessed | tf_op | source)
XLA Modules:
  0.0 169.9 jit_solution(15029643221463603077)
XLA Ops:
  0.0 2.2 %dispatch.1 = bf16[768,256]{1,0:T(8,128)(2,1)} custom-call(s32[2,256]{1,0:T(2,128)} %bitcast.20, bf16[256,256]{1,0:T(8,128)(2,1)} %tok_ref.1), custom_call_target="tpu_custom_call" | custom-call | tf_op jit(solution)/shard_map/dispatch/pallas_call | solution.py:169
  2.2 20.0 %all-to-all-start = ((bf16[96,8,256]{2,1,0:T(8,128)(2,1)}), bf16[96,8,256]{2,1,0:T(8,128)(2,1)S(1)}, u32[]{:S(2)}, u32[]{:S(2)}) async-start(bf16[96,8,256]{2,1,0:T(8,128)(2,1)} %bitcast.18), calls=%async_computation | async-start | bytes 786432 | tf_op jit(solution)/shard_map/all_to_all | solution.py:177
  22.3 2.6 %collective-permute-start = (f32[1,256]{1,0:T(1,128)}, f32[1,256]{1,0:T(1,128)S(1)}, u32[]{:S(2)}, u32[]{:S(2)}) collective-permute-start(f32[1,256]{1,0:T(1,128)} %bitcast.23), channel_id=1, source_target_pairs={{0,1},{1,0},{2,3},{3,2},{4,5},{5,4},{6,7},{7,6},{8,9},{9,8},{10,11... | collective-permute-start | bytes 3080 | tf_op jit(solution)/shard_map/ppermute | solution.py:156
  25.9 17.9 %all-to-all-done.came_ref = bf16[96,8,256]{2,1,0:T(8,128)(2,1)S(1)} async-done(((bf16[96,8,256]{2,1,0:T(8,128)(2,1)}), bf16[96,8,256]{2,1,0:T(8,128)(2,1)S(1)}, u32[]{:S(2)}, u32[]{:S(2)}) %all-to-all-start) | async-done | bytes 393248 | tf_op jit(solution)/shard_map/all_to_all | solution.py:177
  46.3 5.1 %collective-permute-start.1 = (bf16[392,512]{1,0:T(8,128)(2,1)}, bf16[392,512]{1,0:T(8,128)(2,1)S(1)}, u32[]{:S(2)}, u32[]{:S(2)}) collective-permute-start(bf16[392,512]{1,0:T(8,128)(2,1)} %pack.1.refs_0_), channel_id=1, source_target_pairs={{0,2},{1,15},{2,4},{3,1},{4,6},{5,3},{6,8},{7,5},{8,10},{9,7},{10,... | collective-permute-start | bytes 1204232 | tf_op jit(solution)/shard_map/ppermute | solution.py:148
  53.3 3.6 %collective-permute-done.1.refs_1_ = bf16[392,512]{1,0:T(8,128)(2,1)S(1)} collective-permute-done((bf16[392,512]{1,0:T(8,128)(2,1)}, bf16[392,512]{1,0:T(8,128)(2,1)S(1)}, u32[]{:S(2)}, u32[]{:S(2)}) %collective-permute-start.1) | collective-permute-done | bytes 401440 | tf_op jit(solution)/shard_map/ppermute | solution.py:148
  56.9 5.2 %collective-permute-start.3 = (bf16[392,512]{1,0:T(8,128)(2,1)S(1)}, bf16[392,512]{1,0:T(8,128)(2,1)S(1)}, u32[]{:S(2)}, u32[]{:S(2)}) collective-permute-start(bf16[392,512]{1,0:T(8,128)(2,1)S(1)} %collective-permute-done.1.refs_1_), channel_id=1, source_target_pairs={{0,2},{1,15},{2,4},{3,1},{4,6},{5,3},{6,8},{7,5},{8,10},{9,7},{10,... | collective-permute-start | bytes 1204232 | tf_op jit(solution)/shard_map/ppermute | solution.py:148
  62.1 4.4 %collective-permute-start.8 = (bf16[4096,128]{1,0:T(8,128)(2,1)S(1)}, bf16[4096,128]{1,0:T(8,128)(2,1)S(1)}, u32[]{:S(2)}, u32[]{:S(2)}) collective-permute-start(bf16[4096,128]{1,0:T(8,128)(2,1)S(1)} %bitcast.12), channel_id=1, source_target_pairs={{0,1},{1,0},{2,3},{3,2},{4,5},{5,4},{6,7},{7,6},{8,9},{9,8},{10,11... | collective-permute-start | bytes 3145736 | tf_op jit(solution)/shard_map/ppermute | solution.py:156
  68.5 4.0 %collective-permute-start.4 = (bf16[392,512]{1,0:T(8,128)(2,1)S(1)}, bf16[392,512]{1,0:T(8,128)(2,1)S(1)}, u32[]{:S(2)}, u32[]{:S(2)}) collective-permute-start(bf16[392,512]{1,0:T(8,128)(2,1)S(1)} %collective-permute-done.2.refs_2_), channel_id=1, source_target_pairs={{0,14},{1,3},{2,0},{3,5},{4,2},{5,7},{6,4},{7,9},{8,6},{9,11},{10,... | collective-permute-start | bytes 1204232 | tf_op jit(solution)/shard_map/ppermute | solution.py:149
  72.5 2.5 %collective-permute-start.5 = (bf16[392,512]{1,0:T(8,128)(2,1)S(1)}, bf16[392,512]{1,0:T(8,128)(2,1)S(1)}, u32[]{:S(2)}, u32[]{:S(2)}) collective-permute-start(bf16[392,512]{1,0:T(8,128)(2,1)S(1)} %collective-permute-done.3.refs_3_), channel_id=1, source_target_pairs={{0,2},{1,15},{2,4},{3,1},{4,6},{5,3},{6,8},{7,5},{8,10},{9,7},{10,... | collective-permute-start | bytes 1204232 | tf_op jit(solution)/shard_map/ppermute | solution.py:148
  75.0 3.7 %collective-permute-done.4.refs_4_ = bf16[392,512]{1,0:T(8,128)(2,1)S(1)} collective-permute-done((bf16[392,512]{1,0:T(8,128)(2,1)S(1)}, bf16[392,512]{1,0:T(8,128)(2,1)S(1)}, u32[]{:S(2)}, u32[]{:S(2)}) %collective-permute-start.4) | collective-permute-done | bytes 401440 | tf_op jit(solution)/shard_map/ppermute | solution.py:149
  78.7 4.1 %collective-permute-start.6 = (bf16[392,512]{1,0:T(8,128)(2,1)S(1)}, bf16[392,512]{1,0:T(8,128)(2,1)S(1)}, u32[]{:S(2)}, u32[]{:S(2)}) collective-permute-start(bf16[392,512]{1,0:T(8,128)(2,1)S(1)} %collective-permute-done.4.refs_4_), channel_id=1, source_target_pairs={{0,14},{1,3},{2,0},{3,5},{4,2},{5,7},{6,4},{7,9},{8,6},{9,11},{10,... | collective-permute-start | bytes 1204232 | tf_op jit(solution)/shard_map/ppermute | solution.py:149
  83.0 4.0 %collective-permute-start.7 = (bf16[392,512]{1,0:T(8,128)(2,1)S(1)}, bf16[392,512]{1,0:T(8,128)(2,1)S(1)}, u32[]{:S(2)}, u32[]{:S(2)}) collective-permute-start(bf16[392,512]{1,0:T(8,128)(2,1)S(1)} %collective-permute-done.5.refs_5_), channel_id=1, source_target_pairs={{0,2},{1,15},{2,4},{3,1},{4,6},{5,3},{6,8},{7,5},{8,10},{9,7},{10,... | collective-permute-start | bytes 1204232 | tf_op jit(solution)/shard_map/ppermute | solution.py:151
  87.0 2.7 %collective-permute-start.17 = (bf16[2048,256]{1,0:T(8,128)(2,1)}, bf16[2048,256]{1,0:T(8,128)(2,1)S(1)}, u32[]{:S(2)}, u32[]{:S(2)}) collective-permute-start(bf16[2048,256]{1,0:T(8,128)(2,1)} %bitcast.16), channel_id=1, source_target_pairs={{0,1},{1,0},{2,3},{3,2},{4,5},{5,4},{6,7},{7,6},{8,9},{9,8},{10,11... | collective-permute-start | bytes 3145736 | tf_op jit(solution)/shard_map/ppermute | solution.py:156
  89.7 5.4 %collective-permute-done.7.refs_7_ = bf16[392,512]{1,0:T(8,128)(2,1)S(1)} collective-permute-done((bf16[392,512]{1,0:T(8,128)(2,1)S(1)}, bf16[392,512]{1,0:T(8,128)(2,1)S(1)}, u32[]{:S(2)}, u32[]{:S(2)}) %collective-permute-start.7) | collective-permute-done | bytes 401440 | tf_op jit(solution)/shard_map/ppermute | solution.py:151
  96.1 2.6 %hidden.1.refs_0_ = bf16[384,256]{1,0:T(8,128)(2,1)S(1)} custom-call(s32[2]{0:T(128)S(1)} %copy-done.4, bf16[392,512]{1,0:T(8,128)(2,1)S(1)} %copy-done, bf16[392,512]{1,0:T(8,128)(2,1)S(1)} %collective-permute-done.1.refs_1_, bf16[392,512]{1,0:T(8,128)(2,1)S(1)} %collective-permute-done.2.refs_2_, bf16[392,512]{1,0:T(8,128)(2,1)S(1)} %collective-permute-done.3.refs_3_, ...), custom_call_target="tpu_custom_call" | custom-call | tf_op jit(solution)/shard_map/hidden/pallas_call | solution.py:191
  98.7 5.0 %collective-permute-start.10 = (bf16[384,256]{1,0:T(8,128)(2,1)S(1)}, bf16[384,256]{1,0:T(8,128)(2,1)S(1)}, u32[]{:S(2)}, u32[]{:S(2)}) collective-permute-start(bf16[384,256]{1,0:T(8,128)(2,1)S(1)} %hidden.1.refs_0_), channel_id=1, source_target_pairs={{0,2},{1,15},{2,4},{3,1},{4,6},{5,3},{6,8},{7,5},{8,10},{9,7},{10,... | collective-permute-start | bytes 589832 | tf_op jit(solution)/shard_map/ppermute | solution.py:148
  106.3 5.0 %collective-permute-start.12 = (bf16[384,256]{1,0:T(8,128)(2,1)S(1)}, bf16[384,256]{1,0:T(8,128)(2,1)S(1)}, u32[]{:S(2)}, u32[]{:S(2)}) collective-permute-start(bf16[384,256]{1,0:T(8,128)(2,1)S(1)} %collective-permute-done.10.refs_1_), channel_id=1, source_target_pairs={{0,2},{1,15},{2,4},{3,1},{4,6},{5,3},{6,8},{7,5},{8,10},{9,7},{10,... | collective-permute-start | bytes 589832 | tf_op jit(solution)/shard_map/ppermute | solution.py:148
  111.4 3.8 %collective-permute-start.13 = (bf16[384,256]{1,0:T(8,128)(2,1)S(1)}, bf16[384,256]{1,0:T(8,128)(2,1)S(1)}, u32[]{:S(2)}, u32[]{:S(2)}) collective-permute-start(bf16[384,256]{1,0:T(8,128)(2,1)S(1)} %collective-permute-done.11.refs_2_), channel_id=1, source_target_pairs={{0,14},{1,3},{2,0},{3,5},{4,2},{5,7},{6,4},{7,9},{8,6},{9,11},{10,... | collective-permute-start | bytes 589832 | tf_op jit(solution)/shard_map/ppermute | solution.py:149
  116.0 3.0 %collective-permute-start.14 = (bf16[384,256]{1,0:T(8,128)(2,1)S(1)}, bf16[384,256]{1,0:T(8,128)(2,1)S(1)}, u32[]{:S(2)}, u32[]{:S(2)}) collective-permute-start(bf16[384,256]{1,0:T(8,128)(2,1)S(1)} %collective-permute-done.12.refs_3_), channel_id=1, source_target_pairs={{0,2},{1,15},{2,4},{3,1},{4,6},{5,3},{6,8},{7,5},{8,10},{9,7},{10,... | collective-permute-start | bytes 589832 | tf_op jit(solution)/shard_map/ppermute | solution.py:148
  119.7 5.0 %collective-permute-start.15 = (bf16[384,256]{1,0:T(8,128)(2,1)S(1)}, bf16[384,256]{1,0:T(8,128)(2,1)S(1)}, u32[]{:S(2)}, u32[]{:S(2)}) collective-permute-start(bf16[384,256]{1,0:T(8,128)(2,1)S(1)} %collective-permute-done.13.refs_4_), channel_id=1, source_target_pairs={{0,14},{1,3},{2,0},{3,5},{4,2},{5,7},{6,4},{7,9},{8,6},{9,11},{10,... | collective-permute-start | bytes 589832 | tf_op jit(solution)/shard_map/ppermute | solution.py:149
  129.0 5.3 %collective-permute-done.16.refs_7_ = bf16[384,256]{1,0:T(8,128)(2,1)S(1)} collective-permute-done((bf16[384,256]{1,0:T(8,128)(2,1)S(1)}, bf16[384,256]{1,0:T(8,128)(2,1)S(1)}, u32[]{:S(2)}, u32[]{:S(2)}) %collective-permute-start.16) | collective-permute-done | bytes 196640 | tf_op jit(solution)/shard_map/ppermute | solution.py:151
  135.8 31.4 %all_to_all.10 = bf16[96,8,256]{2,1,0:T(8,128)(2,1)} all-to-all(bf16[96,8,256]{2,1,0:T(8,128)(2,1)S(1)} %bitcast.11), channel_id=1, replica_groups=mesh['z'=12,'x'=4,'y'=8,'c'=2] {'z','x','c'}, dimensions={0} | all-to-all | bytes 786432 | tf_op jit(solution)/shard_map/all_to_all | solution.py:215
  167.2 2.7 %combine.1 = bf16[256,256]{1,0:T(8,128)(2,1)} custom-call(s32[2,256]{1,0:T(2,128)} %bitcast.21, f32[2,256]{1,0:T(2,128)} %bitcast.22, bf16[768,256]{1,0:T(8,128)(2,1)} %bitcast.19), custom_call_target="tpu_custom_call" | custom-call | tf_op jit(solution)/shard_map/combine/pallas_call | solution.py:217
  (35 shorter events, 18.6 us)
Async XLA Ops:
  0.0 62.1 %copy-start.1 = (bf16[1,4096,128]{2,1,0:T(8,128)(2,1)S(1)}, bf16[1,4096,128]{2,1,0:T(8,128)(2,1)}, u32[]{:S(2)}) copy-start(bf16[1,4096,128]{2,1,0:T(8,128)(2,1)} %param.11) | copy-start | bytes 3145732
  0.0 66.5 %copy-start.2 = (bf16[1,4096,128]{2,1,0:T(8,128)(2,1)S(1)}, bf16[1,4096,128]{2,1,0:T(8,128)(2,1)}, u32[]{:S(2)}) copy-start(bf16[1,4096,128]{2,1,0:T(8,128)(2,1)} %param.12) | copy-start | bytes 3145732
  2.2 41.5 %all-to-all-start = ((bf16[96,8,256]{2,1,0:T(8,128)(2,1)}), bf16[96,8,256]{2,1,0:T(8,128)(2,1)S(1)}, u32[]{:S(2)}, u32[]{:S(2)}) async-start(bf16[96,8,256]{2,1,0:T(8,128)(2,1)} %bitcast.18), calls=%async_computation | async-start | bytes 786432 | tf_op jit(solution)/shard_map/all_to_all | solution.py:177
  22.3 3.6 %collective-permute-start = (f32[1,256]{1,0:T(1,128)}, f32[1,256]{1,0:T(1,128)S(1)}, u32[]{:S(2)}, u32[]{:S(2)}) collective-permute-start(f32[1,256]{1,0:T(1,128)} %bitcast.23), channel_id=1, source_target_pairs={{0,1},{1,0},{2,3},{3,2},{4,5},{5,4},{6,7},{7,6},{8,9},{9,8},{10,11... | collective-permute-start | bytes 3080 | tf_op jit(solution)/shard_map/ppermute | solution.py:156
  25.9 17.9 %copy-start.6 = (f32[1,256]{1,0:T(1,128)}, f32[1,256]{1,0:T(1,128)S(1)}, u32[]{:S(2)}) copy-start(f32[1,256]{1,0:T(1,128)S(1)} %collective-permute-done.peer_gain_ref) | copy-start | bytes 3076
  46.3 10.6 %collective-permute-start.1 = (bf16[392,512]{1,0:T(8,128)(2,1)}, bf16[392,512]{1,0:T(8,128)(2,1)S(1)}, u32[]{:S(2)}, u32[]{:S(2)}) collective-permute-start(bf16[392,512]{1,0:T(8,128)(2,1)} %pack.1.refs_0_), channel_id=1, source_target_pairs={{0,2},{1,15},{2,4},{3,1},{4,6},{5,3},{6,8},{7,5},{8,10},{9,7},{10,... | collective-permute-start | bytes 1204232 | tf_op jit(solution)/shard_map/ppermute | solution.py:148
  51.4 17.1 %collective-permute-start.2 = (bf16[392,512]{1,0:T(8,128)(2,1)}, bf16[392,512]{1,0:T(8,128)(2,1)S(1)}, u32[]{:S(2)}, u32[]{:S(2)}) collective-permute-start(bf16[392,512]{1,0:T(8,128)(2,1)} %pack.1.refs_0_), channel_id=1, source_target_pairs={{0,14},{1,3},{2,0},{3,5},{4,2},{5,7},{6,4},{7,9},{8,6},{9,11},{10,... | collective-permute-start | bytes 1204232 | tf_op jit(solution)/shard_map/ppermute | solution.py:149
  56.9 15.6 %collective-permute-start.3 = (bf16[392,512]{1,0:T(8,128)(2,1)S(1)}, bf16[392,512]{1,0:T(8,128)(2,1)S(1)}, u32[]{:S(2)}, u32[]{:S(2)}) collective-permute-start(bf16[392,512]{1,0:T(8,128)(2,1)S(1)} %collective-permute-done.1.refs_1_), channel_id=1, source_target_pairs={{0,2},{1,15},{2,4},{3,1},{4,6},{5,3},{6,8},{7,5},{8,10},{9,7},{10,... | collective-permute-start | bytes 1204232 | tf_op jit(solution)/shard_map/ppermute | solution.py:148
  62.1 27.6 %collective-permute-start.8 = (bf16[4096,128]{1,0:T(8,128)(2,1)S(1)}, bf16[4096,128]{1,0:T(8,128)(2,1)S(1)}, u32[]{:S(2)}, u32[]{:S(2)}) collective-permute-start(bf16[4096,128]{1,0:T(8,128)(2,1)S(1)} %bitcast.12), channel_id=1, source_target_pairs={{0,1},{1,0},{2,3},{3,2},{4,5},{5,4},{6,7},{7,6},{8,9},{9,8},{10,11... | collective-permute-start | bytes 3145736 | tf_op jit(solution)/shard_map/ppermute | solution.py:156
  66.5 28.6 %copy-start.4 = (s32[2]{0:T(128)S(1)}, s32[2]{0:T(128)}, u32[]{:S(2)}) copy-start(s32[2]{0:T(128)} %pad_add_fusion.where_ref) | copy-start | bytes 28
  66.5 23.2 %collective-permute-start.9 = (bf16[4096,128]{1,0:T(8,128)(2,1)S(1)}, bf16[4096,128]{1,0:T(8,128)(2,1)S(1)}, u32[]{:S(2)}, u32[]{:S(2)}) collective-permute-start(bf16[4096,128]{1,0:T(8,128)(2,1)S(1)} %bitcast.14), channel_id=1, source_target_pairs={{0,1},{1,0},{2,3},{3,2},{4,5},{5,4},{6,7},{7,6},{8,9},{9,8},{10,11... | collective-permute-start | bytes 3145736 | tf_op jit(solution)/shard_map/ppermute | solution.py:156
  68.5 10.2 %collective-permute-start.4 = (bf16[392,512]{1,0:T(8,128)(2,1)S(1)}, bf16[392,512]{1,0:T(8,128)(2,1)S(1)}, u32[]{:S(2)}, u32[]{:S(2)}) collective-permute-start(bf16[392,512]{1,0:T(8,128)(2,1)S(1)} %collective-permute-done.2.refs_2_), channel_id=1, source_target_pairs={{0,14},{1,3},{2,0},{3,5},{4,2},{5,7},{6,4},{7,9},{8,6},{9,11},{10,... | collective-permute-start | bytes 1204232 | tf_op jit(solution)/shard_map/ppermute | solution.py:149
  72.5 10.5 %collective-permute-start.5 = (bf16[392,512]{1,0:T(8,128)(2,1)S(1)}, bf16[392,512]{1,0:T(8,128)(2,1)S(1)}, u32[]{:S(2)}, u32[]{:S(2)}) collective-permute-start(bf16[392,512]{1,0:T(8,128)(2,1)S(1)} %collective-permute-done.3.refs_3_), channel_id=1, source_target_pairs={{0,2},{1,15},{2,4},{3,1},{4,6},{5,3},{6,8},{7,5},{8,10},{9,7},{10,... | collective-permute-start | bytes 1204232 | tf_op jit(solution)/shard_map/ppermute | solution.py:148
  78.7 11.0 %collective-permute-start.6 = (bf16[392,512]{1,0:T(8,128)(2,1)S(1)}, bf16[392,512]{1,0:T(8,128)(2,1)S(1)}, u32[]{:S(2)}, u32[]{:S(2)}) collective-permute-start(bf16[392,512]{1,0:T(8,128)(2,1)S(1)} %collective-permute-done.4.refs_4_), channel_id=1, source_target_pairs={{0,14},{1,3},{2,0},{3,5},{4,2},{5,7},{6,4},{7,9},{8,6},{9,11},{10,... | collective-permute-start | bytes 1204232 | tf_op jit(solution)/shard_map/ppermute | solution.py:149
  83.0 12.1 %collective-permute-start.7 = (bf16[392,512]{1,0:T(8,128)(2,1)S(1)}, bf16[392,512]{1,0:T(8,128)(2,1)S(1)}, u32[]{:S(2)}, u32[]{:S(2)}) collective-permute-start(bf16[392,512]{1,0:T(8,128)(2,1)S(1)} %collective-permute-done.5.refs_5_), channel_id=1, source_target_pairs={{0,2},{1,15},{2,4},{3,1},{4,6},{5,3},{6,8},{7,5},{8,10},{9,7},{10,... | collective-permute-start | bytes 1204232 | tf_op jit(solution)/shard_map/ppermute | solution.py:151
  87.0 40.0 %collective-permute-start.17 = (bf16[2048,256]{1,0:T(8,128)(2,1)}, bf16[2048,256]{1,0:T(8,128)(2,1)S(1)}, u32[]{:S(2)}, u32[]{:S(2)}) collective-permute-start(bf16[2048,256]{1,0:T(8,128)(2,1)} %bitcast.16), channel_id=1, source_target_pairs={{0,1},{1,0},{2,3},{3,2},{4,5},{5,4},{6,7},{7,6},{8,9},{9,8},{10,11... | collective-permute-start | bytes 3145736 | tf_op jit(solution)/shard_map/ppermute | solution.py:156
  96.1 38.2 %copy-start.3 = (bf16[1,2048,256]{2,1,0:T(8,128)(2,1)S(1)}, bf16[1,2048,256]{2,1,0:T(8,128)(2,1)}, u32[]{:S(2)}) copy-start(bf16[1,2048,256]{2,1,0:T(8,128)(2,1)} %param.13) | copy-start | bytes 3145732
  98.7 7.6 %collective-permute-start.10 = (bf16[384,256]{1,0:T(8,128)(2,1)S(1)}, bf16[384,256]{1,0:T(8,128)(2,1)S(1)}, u32[]{:S(2)}, u32[]{:S(2)}) collective-permute-start(bf16[384,256]{1,0:T(8,128)(2,1)S(1)} %hidden.1.refs_0_), channel_id=1, source_target_pairs={{0,2},{1,15},{2,4},{3,1},{4,6},{5,3},{6,8},{7,5},{8,10},{9,7},{10,... | collective-permute-start | bytes 589832 | tf_op jit(solution)/shard_map/ppermute | solution.py:148
  103.8 7.6 %collective-permute-start.11 = (bf16[384,256]{1,0:T(8,128)(2,1)S(1)}, bf16[384,256]{1,0:T(8,128)(2,1)S(1)}, u32[]{:S(2)}, u32[]{:S(2)}) collective-permute-start(bf16[384,256]{1,0:T(8,128)(2,1)S(1)} %hidden.1.refs_0_), channel_id=1, source_target_pairs={{0,14},{1,3},{2,0},{3,5},{4,2},{5,7},{6,4},{7,9},{8,6},{9,11},{10,... | collective-permute-start | bytes 589832 | tf_op jit(solution)/shard_map/ppermute | solution.py:149
  106.3 9.7 %collective-permute-start.12 = (bf16[384,256]{1,0:T(8,128)(2,1)S(1)}, bf16[384,256]{1,0:T(8,128)(2,1)S(1)}, u32[]{:S(2)}, u32[]{:S(2)}) collective-permute-start(bf16[384,256]{1,0:T(8,128)(2,1)S(1)} %collective-permute-done.10.refs_1_), channel_id=1, source_target_pairs={{0,2},{1,15},{2,4},{3,1},{4,6},{5,3},{6,8},{7,5},{8,10},{9,7},{10,... | collective-permute-start | bytes 589832 | tf_op jit(solution)/shard_map/ppermute | solution.py:148
  111.4 8.3 %collective-permute-start.13 = (bf16[384,256]{1,0:T(8,128)(2,1)S(1)}, bf16[384,256]{1,0:T(8,128)(2,1)S(1)}, u32[]{:S(2)}, u32[]{:S(2)}) collective-permute-start(bf16[384,256]{1,0:T(8,128)(2,1)S(1)} %collective-permute-done.11.refs_2_), channel_id=1, source_target_pairs={{0,14},{1,3},{2,0},{3,5},{4,2},{5,7},{6,4},{7,9},{8,6},{9,11},{10,... | collective-permute-start | bytes 589832 | tf_op jit(solution)/shard_map/ppermute | solution.py:149
  116.0 9.1 %collective-permute-start.14 = (bf16[384,256]{1,0:T(8,128)(2,1)S(1)}, bf16[384,256]{1,0:T(8,128)(2,1)S(1)}, u32[]{:S(2)}, u32[]{:S(2)}) collective-permute-start(bf16[384,256]{1,0:T(8,128)(2,1)S(1)} %collective-permute-done.12.refs_3_), channel_id=1, source_target_pairs={{0,2},{1,15},{2,4},{3,1},{4,6},{5,3},{6,8},{7,5},{8,10},{9,7},{10,... | collective-permute-start | bytes 589832 | tf_op jit(solution)/shard_map/ppermute | solution.py:148
  119.7 9.4 %collective-permute-start.15 = (bf16[384,256]{1,0:T(8,128)(2,1)S(1)}, bf16[384,256]{1,0:T(8,128)(2,1)S(1)}, u32[]{:S(2)}, u32[]{:S(2)}) collective-permute-start(bf16[384,256]{1,0:T(8,128)(2,1)S(1)} %collective-permute-done.13.refs_4_), channel_id=1, source_target_pairs={{0,14},{1,3},{2,0},{3,5},{4,2},{5,7},{6,4},{7,9},{8,6},{9,11},{10,... | collective-permute-start | bytes 589832 | tf_op jit(solution)/shard_map/ppermute | solution.py:149
  125.1 9.2 %collective-permute-start.16 = (bf16[384,256]{1,0:T(8,128)(2,1)S(1)}, bf16[384,256]{1,0:T(8,128)(2,1)S(1)}, u32[]{:S(2)}, u32[]{:S(2)}) collective-permute-start(bf16[384,256]{1,0:T(8,128)(2,1)S(1)} %collective-permute-done.14.refs_5_), channel_id=1, source_target_pairs={{0,2},{1,15},{2,4},{3,1},{4,6},{5,3},{6,8},{7,5},{8,10},{9,7},{10,... | collective-permute-start | bytes 589832 | tf_op jit(solution)/shard_map/ppermute | solution.py:151
  (2 other events, 1.7 us)

commit v2 on v1

--- a/solution.py
+++ b/solution.py
@@ -11,8 +11,8 @@
 F32 = jnp.float32
 VM = pl.BlockSpec(memory_space=pltpu.VMEM)
 SM = pl.BlockSpec(memory_space=pltpu.SMEM)
-STEPS = (0, 1, -1, 2, -2, 3, -3, 4)
 PAD = 8
+CHUNKS = 2
 
 
 def dot(a, b):
@@ -61,12 +61,9 @@
     out_ref[...] = total.astype(BF)
 
 
-def pack_kernel(where_ref, came_ref, gain_ref, peer_gain_ref, out_ref):
-    sources = came_ref.shape[0] // 2
+def pack_kernel(where_ref, came_ref, gain_ref, peer_gain_ref, *out_refs):
     width = came_ref.shape[2]
-    for s in range(sources):
-        for c in range(2):
-            out_ref[s * 8 : s * 8 + 8, c * width : (c + 1) * width] = came_ref[2 * s + c]
+    sources = came_ref.shape[0] // 2 // len(out_refs)
     core = where_ref[1]
     mine, other = gain_ref[...], peer_gain_ref[...]
     gain = jnp.concatenate(
@@ -77,19 +74,25 @@
     low = gain - top - mid
     line = lax.broadcasted_iota(jnp.int32, (PAD, 2 * width), 0)
     split = jnp.where(line == 0, top, jnp.where(line == 1, mid, jnp.where(line == 2, low, 0.0)))
-    out_ref[sources * 8 : sources * 8 + PAD, :] = split.astype(BF)
+    for number, out_ref in enumerate(out_refs):
+        for s in range(sources):
+            for c in range(2):
+                out_ref[s * 8 : s * 8 + 8, c * width : (c + 1) * width] = came_ref[
+                    2 * (number * sources + s) + c
+                ]
+        out_ref[sources * 8 : sources * 8 + PAD, :] = split.astype(BF)
 
 
 def source_of(where_ref, step, count):
     turn = 1 - 2 * where_ref[1]
-    return lax.rem(where_ref[0] - step * turn + 2 * count, count)
+    return lax.rem(where_ref[0] - step * turn + count, count)
 
 
 def hidden_kernel(count, where_ref, *refs):
-    blocks, (gate_ref, gate2_ref, up_ref, up2_ref, out_ref, gsum, usum, square) = refs[:8], refs[8:]
+    blocks, (gate_ref, gate2_ref, up_ref, up2_ref, out_ref, gsum, usum, square) = refs[:count], refs[count:]
     rows, half = out_ref.shape[0], gate_ref.shape[1]
     depth = blocks[0].shape[1]
-    for number, (step, block) in enumerate(zip(STEPS, blocks)):
+    for step, block in enumerate(blocks):
         start = pl.multiple_of(source_of(where_ref, step, count) * depth, depth)
         gain = jnp.sum(block[rows : rows + PAD, :].astype(F32), axis=0, keepdims=True)
         raw = block[0:rows, :].astype(F32)
@@ -100,7 +103,7 @@
         scaled = (raw * gain).astype(BF)
         gate = jnp.concatenate([gate_ref[pl.ds(start, depth), :], gate2_ref[pl.ds(start, depth), :]], axis=1)
         up = jnp.concatenate([up_ref[pl.ds(start, depth), :], up2_ref[pl.ds(start, depth), :]], axis=1)
-        if number == 0:
+        if step == 0:
             square[...] = part
             gsum[...] = dot(scaled, gate)
             usum[...] = dot(scaled, up)
@@ -118,37 +121,27 @@
 
 
 def down_kernel(count, where_ref, *refs):
-    blocks, (down_ref, down2_ref, out_ref, mine, other) = refs[:8], refs[8:]
-    depth = blocks[0].shape[1]
-    for number, (step, block) in enumerate(zip(STEPS, blocks)):
-        start = pl.multiple_of(source_of(where_ref, step, count) * depth, depth)
-        first = dot(block[...], down_ref[pl.ds(start, depth), :])
-        second = dot(block[...], down2_ref[pl.ds(start, depth), :])
-        if number == 0:
-            mine[...] = first
-            other[...] = second
-        else:
-            mine[...] += first
-            other[...] += second
+    blocks, (down_ref, down2_ref, out_ref) = refs[: CHUNKS * count], refs[CHUNKS * count :]
+    rows, depth = blocks[0].shape
     core = where_ref[1]
-    for s in range(out_ref.shape[0]):
-        out_ref[s, core] = mine[s * 8 : s * 8 + 8, :].astype(BF)
-        out_ref[s, 1 - core] = other[s * 8 : s * 8 + 8, :].astype(BF)
+    for number in range(CHUNKS):
+        mine = other = None
+        for step, block in enumerate(blocks[number * count : (number + 1) * count]):
+            start = pl.multiple_of(source_of(where_ref, step, count) * depth, depth)
+            first = dot(block[...], down_ref[pl.ds(start, depth), :])
+            second = dot(block[...], down2_ref[pl.ds(start, depth), :])
+            mine = first if step == 0 else mine + first
+            other = second if step == 0 else other + second
+        for s in range(rows // 8):
+            out_ref[number * rows // 8 + s, core] = mine[s * 8 : s * 8 + 8, :].astype(BF)
+            out_ref[number * rows // 8 + s, 1 - core] = other[s * 8 : s * 8 + 8, :].astype(BF)
 
 
 def ring(block, count):
-    def perm(sign):
-        return [
-            (y * 2 + c, (y + sign * (1 - 2 * c)) % count * 2 + c) for y in range(count) for c in range(2)
-        ]
-
-    main = other = block
+    perm = [(y * 2 + c, (y + 1 - 2 * c) % count * 2 + c) for y in range(count) for c in range(2)]
     found = [block]
-    for k in range(3):
-        main = lax.ppermute(main, ("y", "c"), perm(1))
-        other = lax.ppermute(other, ("y", "c"), perm(-1))
-        found += [main, other]
-    found.append(lax.ppermute(main, ("y", "c"), perm(1)))
+    for _ in range(count - 1):
+        found.append(lax.ppermute(found[-1], ("y", "c"), perm))
     return found
 
 
@@ -164,7 +157,7 @@
     half = experts * cap // 2
     where = jnp.stack([lax.axis_index("y"), lax.axis_index("c")]).astype(jnp.int32)
     ids = expert_ids.T
-    call = functools.partial(pl.pallas_call)
+    call = pl.pallas_call
 
     outgoing = call(
         functools.partial(dispatch_kernel, experts, cap),
@@ -172,46 +165,54 @@
         in_specs=[VM, VM],
         out_specs=VM,
         scratch_shapes=[pltpu.VMEM((experts * cap, rows), BF)],
+        compiler_params=pltpu.CompilerParams(vmem_limit_bytes=8 << 20),
         name="dispatch",
     )(ids, tokens)
     came = lax.all_to_all(outgoing.reshape(2 * experts, 8, width), ("z", "x", "c"), 0, 0, tiled=True)
 
     gain = norm_gain[None, :]
-    block = call(
+    gate, up, down = gate_weight[0], up_weight[0], down_weight[0]
+    came, gain2, gate2, up2, down2 = lax.optimization_barrier(
+        (came, swap(gain), swap(gate), swap(up), swap(down))
+    )
+    rows_each = half // CHUNKS
+    blocks = call(
         pack_kernel,
-        out_shape=jax.ShapeDtypeStruct((half + PAD, 2 * width), BF),
+        out_shape=[jax.ShapeDtypeStruct((rows_each + PAD, 2 * width), BF)] * CHUNKS,
         in_specs=[SM, VM, VM, VM],
-        out_specs=VM,
+        out_specs=[VM] * CHUNKS,
+        compiler_params=pltpu.CompilerParams(vmem_limit_bytes=8 << 20),
         name="pack",
-    )(where, came, gain, swap(gain))
-    found = ring(block, count)
-
-    gate, up, down = gate_weight[0], up_weight[0], down_weight[0]
+    )(where, came, gain, gain2)
+
     ff = gate.shape[1]
-    hidden = call(
-        functools.partial(hidden_kernel, count),
-        out_shape=jax.ShapeDtypeStruct((half, 2 * ff), BF),
-        in_specs=[SM] + [VM] * 12,
-        out_specs=VM,
-        scratch_shapes=[
-            pltpu.VMEM((half, 2 * ff), F32),
-            pltpu.VMEM((half, 2 * ff), F32),
-            pltpu.VMEM((half, 128), F32),
-        ],
-        compiler_params=pltpu.CompilerParams(vmem_limit_bytes=40 << 20),
-        name="hidden",
-    )(where, *found, gate, swap(gate), up, swap(up))
-    found = ring(hidden, count)
+    wide = [ring(block, count) for block in blocks]
+    hidden = [
+        call(
+            functools.partial(hidden_kernel, count),
+            out_shape=jax.ShapeDtypeStruct((rows_each, 2 * ff), BF),
+            in_specs=[SM] + [VM] * (count + 4),
+            out_specs=VM,
+            scratch_shapes=[
+                pltpu.VMEM((rows_each, 2 * ff), F32),
+                pltpu.VMEM((rows_each, 2 * ff), F32),
+                pltpu.VMEM((rows_each, 128), F32),
+            ],
+            compiler_params=pltpu.CompilerParams(vmem_limit_bytes=24 << 20),
+            name="hidden",
+        )(where, *found, gate, gate2, up, up2)
+        for found in wide
+    ]
+    wide = [ring(block, count) for block in hidden]
 
     made = call(
         functools.partial(down_kernel, count),
         out_shape=jax.ShapeDtypeStruct((experts, 2, 8, width), BF),
-        in_specs=[SM] + [VM] * 10,
+        in_specs=[SM] + [VM] * (CHUNKS * count + 2),
         out_specs=VM,
-        scratch_shapes=[pltpu.VMEM((half, width), F32), pltpu.VMEM((half, width), F32)],
-        compiler_params=pltpu.CompilerParams(vmem_limit_bytes=40 << 20),
+        compiler_params=pltpu.CompilerParams(vmem_limit_bytes=24 << 20),
         name="down",
-    )(where, *found, down, swap(down))
+    )(where, *(block for found in wide for block in found), down, down2)
     back = lax.all_to_all(made.reshape(2 * experts, 8, width), ("z", "x", "c"), 0, 0, tiled=True)
 
     return call(
@@ -219,6 +220,7 @@
         out_shape=jax.ShapeDtypeStruct((rows, width), BF),
         in_specs=[VM, VM, VM],
         out_specs=VM,
+        compiler_params=pltpu.CompilerParams(vmem_limit_bytes=8 << 20),
         name="combine",
     )(ids, expert_weights.T, back.reshape(experts * cap, width))
 

time: 172 us -> 201 us (1.17)
  starting transfers between devices: 84 us -> 128 us
  waiting for transfers between devices: 41.1 us -> 14.8 us
  blocking collectives: 31.4 us -> 43.6 us
    ppermute x14 -> x28, starting transfers between devices: 52.4 us -> 99.5 us  [ring(): found.append(lax.ppermute(found[-1], ('y', 'c'), perm))]
    ppermute x14 -> x28, waiting for transfers between devices: 22.8 us -> 2.29 us  [ring(): found.append(lax.ppermute(found[-1], ('y', 'c'), perm))]
    all_to_all x1, blocking collectives: 31.4 us -> 43.6 us  [body(): lax.all_to_all(made.reshape(2 * experts, 8, width), ('z', 'x', 'c'), 0, 0...]
    all_to_all x1, waiting for transfers between devices: 17.9 us -> 11.5 us  [body(): lax.all_to_all(outgoing.reshape(2 * experts, 8, width), ('z', 'x', 'c'),...]
    ppermute x4, starting transfers between devices: 11.6 us -> 8.84 us  [swap(): return lax.ppermute(value, 'c', [(0, 1), (1, 0)])]
  transfers between devices with their start and end apart: 19 -> 33, of which waited for: 12 -> 4; matrix products, arithmetic and copies ran while one was open for 0% -> 0% of each run, Pallas kernels for 2% -> 2%
where the time goes in v2:
time: 201 us; the launch traced here: 200 us
  starting transfers between devices  128 us (64%)
  blocking collectives  43.6 us (22%)
  waiting for transfers between devices  14.8 us (7%)
  Pallas kernels  8.86 us (4%)
  local copies, waits for them, and re-layouts  3.6 us (2%)
    ppermute x28, starting transfers between devices, ring(): found.append(lax.ppermute(found[-1], ('y', 'c'), perm))  99.5 us
    all_to_all x1, blocking collectives, body(): lax.all_to_all(made.reshape(2 * experts, 8, width), ('z', 'x', 'c'), 0, 0...  43.6 us
    all_to_all x1, starting transfers between devices, body(): lax.all_to_all(outgoing.reshape(2 * experts, 8, width), ('z', 'x', 'c'),...  20 us
    all_to_all x1, waiting for transfers between devices, body(): lax.all_to_all(outgoing.reshape(2 * experts, 8, width), ('z', 'x', 'c'),...  11.5 us
    ppermute x4, starting transfers between devices, swap(): return lax.ppermute(value, 'c', [(0, 1), (1, 0)])  8.84 us
  transfers between devices with their start and end apart: 33, of which 4 were waited for; matrix products, arithmetic and copies ran while one was open for 0% of the time, Pallas kernels for 2%

profile of v2, /device:TPU:1, one launch (start us, length us, event | category | flops | bytes accessed | tf_op | source)
XLA Modules:
  0.0 199.9 jit_solution(3500422172740948294)
XLA Ops:
  2.8 20.0 %all-to-all-start = ((bf16[96,8,256]{2,1,0:T(8,128)(2,1)}), bf16[96,8,256]{2,1,0:T(8,128)(2,1)S(1)}, u32[]{:S(2)}, u32[]{:S(2)}) async-start(bf16[96,8,256]{2,1,0:T(8,128)(2,1)} %bitcast.4), calls=%async_computation | async-start | bytes 786432 | tf_op jit(solution)/shard_map/all_to_all | solution.py:171
  32.9 11.5 %all-to-all-done.came_ref = bf16[96,8,256]{2,1,0:T(8,128)(2,1)S(1)} async-done(((bf16[96,8,256]{2,1,0:T(8,128)(2,1)}), bf16[96,8,256]{2,1,0:T(8,128)(2,1)S(1)}, u32[]{:S(2)}, u32[]{:S(2)}) %all-to-all-start) | async-done | bytes 393248 | tf_op jit(solution)/shard_map/all_to_all | solution.py:171
  44.9 5.1 %collective-permute-start.4 = (bf16[200,512]{1,0:T(8,128)(2,1)S(1)}, bf16[200,512]{1,0:T(8,128)(2,1)S(1)}, u32[]{:S(2)}, u32[]{:S(2)}) collective-permute-start(bf16[200,512]{1,0:T(8,128)(2,1)S(1)} %get-tuple-element.14.refs_0_), channel_id=1, source_target_pairs={{0,2},{1,15},{2,4},{3,1},{4,6},{5,3},{6,8},{7,5},{8,10},{9,7},{10,... | collective-permute-start | bytes 614408 | tf_op jit(solution)/shard_map/ppermute | solution.py:144
  50.0 3.0 %collective-permute-start.18 = (bf16[200,512]{1,0:T(8,128)(2,1)S(1)}, bf16[200,512]{1,0:T(8,128)(2,1)S(1)}, u32[]{:S(2)}, u32[]{:S(2)}) collective-permute-start(bf16[200,512]{1,0:T(8,128)(2,1)S(1)} %get-tuple-element.17.refs_0_), channel_id=1, source_target_pairs={{0,2},{1,15},{2,4},{3,1},{4,6},{5,3},{6,8},{7,5},{8,10},{9,7},{10,... | collective-permute-start | bytes 614408 | tf_op jit(solution)/shard_map/ppermute | solution.py:144
  53.0 4.7 %collective-permute-start.5 = (bf16[200,512]{1,0:T(8,128)(2,1)S(1)}, bf16[200,512]{1,0:T(8,128)(2,1)S(1)}, u32[]{:S(2)}, u32[]{:S(2)}) collective-permute-start(bf16[200,512]{1,0:T(8,128)(2,1)S(1)} %collective-permute-done.4.refs_1_), channel_id=1, source_target_pairs={{0,2},{1,15},{2,4},{3,1},{4,6},{5,3},{6,8},{7,5},{8,10},{9,7},{10,... | collective-permute-start | bytes 614408 | tf_op jit(solution)/shard_map/ppermute | solution.py:144
  57.7 3.0 %collective-permute-start.19 = (bf16[200,512]{1,0:T(8,128)(2,1)S(1)}, bf16[200,512]{1,0:T(8,128)(2,1)S(1)}, u32[]{:S(2)}, u32[]{:S(2)}) collective-permute-start(bf16[200,512]{1,0:T(8,128)(2,1)S(1)} %collective-permute-done.18.refs_1_), channel_id=1, source_target_pairs={{0,2},{1,15},{2,4},{3,1},{4,6},{5,3},{6,8},{7,5},{8,10},{9,7},{10,... | collective-permute-start | bytes 614408 | tf_op jit(solution)/shard_map/ppermute | solution.py:144
  60.7 4.7 %collective-permute-start.6 = (bf16[200,512]{1,0:T(8,128)(2,1)S(1)}, bf16[200,512]{1,0:T(8,128)(2,1)S(1)}, u32[]{:S(2)}, u32[]{:S(2)}) collective-permute-start(bf16[200,512]{1,0:T(8,128)(2,1)S(1)} %collective-permute-done.5.refs_2_), channel_id=1, source_target_pairs={{0,2},{1,15},{2,4},{3,1},{4,6},{5,3},{6,8},{7,5},{8,10},{9,7},{10,... | collective-permute-start | bytes 614408 | tf_op jit(solution)/shard_map/ppermute | solution.py:144
  65.4 3.0 %collective-permute-start.20 = (bf16[200,512]{1,0:T(8,128)(2,1)S(1)}, bf16[200,512]{1,0:T(8,128)(2,1)S(1)}, u32[]{:S(2)}, u32[]{:S(2)}) collective-permute-start(bf16[200,512]{1,0:T(8,128)(2,1)S(1)} %collective-permute-done.19.refs_2_), channel_id=1, source_target_pairs={{0,2},{1,15},{2,4},{3,1},{4,6},{5,3},{6,8},{7,5},{8,10},{9,7},{10,... | collective-permute-start | bytes 614408 | tf_op jit(solution)/shard_map/ppermute | solution.py:144
  68.4 4.7 %collective-permute-start.7 = (bf16[200,512]{1,0:T(8,128)(2,1)S(1)}, bf16[200,512]{1,0:T(8,128)(2,1)S(1)}, u32[]{:S(2)}, u32[]{:S(2)}) collective-permute-start(bf16[200,512]{1,0:T(8,128)(2,1)S(1)} %collective-permute-done.6.refs_3_), channel_id=1, source_target_pairs={{0,2},{1,15},{2,4},{3,1},{4,6},{5,3},{6,8},{7,5},{8,10},{9,7},{10,... | collective-permute-start | bytes 614408 | tf_op jit(solution)/shard_map/ppermute | solution.py:144
  73.1 3.0 %collective-permute-start.21 = (bf16[200,512]{1,0:T(8,128)(2,1)S(1)}, bf16[200,512]{1,0:T(8,128)(2,1)S(1)}, u32[]{:S(2)}, u32[]{:S(2)}) collective-permute-start(bf16[200,512]{1,0:T(8,128)(2,1)S(1)} %collective-permute-done.20.refs_3_), channel_id=1, source_target_pairs={{0,2},{1,15},{2,4},{3,1},{4,6},{5,3},{6,8},{7,5},{8,10},{9,7},{10,... | collective-permute-start | bytes 614408 | tf_op jit(solution)/shard_map/ppermute | solution.py:144
  76.1 4.7 %collective-permute-start.8 = (bf16[200,512]{1,0:T(8,128)(2,1)S(1)}, bf16[200,512]{1,0:T(8,128)(2,1)S(1)}, u32[]{:S(2)}, u32[]{:S(2)}) collective-permute-start(bf16[200,512]{1,0:T(8,128)(2,1)S(1)} %collective-permute-done.7.refs_4_), channel_id=1, source_target_pairs={{0,2},{1,15},{2,4},{3,1},{4,6},{5,3},{6,8},{7,5},{8,10},{9,7},{10,... | collective-permute-start | bytes 614408 | tf_op jit(solution)/shard_map/ppermute | solution.py:144
  80.8 3.0 %collective-permute-start.22 = (bf16[200,512]{1,0:T(8,128)(2,1)S(1)}, bf16[200,512]{1,0:T(8,128)(2,1)S(1)}, u32[]{:S(2)}, u32[]{:S(2)}) collective-permute-start(bf16[200,512]{1,0:T(8,128)(2,1)S(1)} %collective-permute-done.21.refs_4_), channel_id=1, source_target_pairs={{0,2},{1,15},{2,4},{3,1},{4,6},{5,3},{6,8},{7,5},{8,10},{9,7},{10,... | collective-permute-start | bytes 614408 | tf_op jit(solution)/shard_map/ppermute | solution.py:144
  83.8 4.7 %collective-permute-start.9 = (bf16[200,512]{1,0:T(8,128)(2,1)S(1)}, bf16[200,512]{1,0:T(8,128)(2,1)S(1)}, u32[]{:S(2)}, u32[]{:S(2)}) collective-permute-start(bf16[200,512]{1,0:T(8,128)(2,1)S(1)} %collective-permute-done.8.refs_5_), channel_id=1, source_target_pairs={{0,2},{1,15},{2,4},{3,1},{4,6},{5,3},{6,8},{7,5},{8,10},{9,7},{10,... | collective-permute-start | bytes 614408 | tf_op jit(solution)/shard_map/ppermute | solution.py:144
  88.6 3.0 %collective-permute-start.23 = (bf16[200,512]{1,0:T(8,128)(2,1)S(1)}, bf16[200,512]{1,0:T(8,128)(2,1)S(1)}, u32[]{:S(2)}, u32[]{:S(2)}) collective-permute-start(bf16[200,512]{1,0:T(8,128)(2,1)S(1)} %collective-permute-done.22.refs_5_), channel_id=1, source_target_pairs={{0,2},{1,15},{2,4},{3,1},{4,6},{5,3},{6,8},{7,5},{8,10},{9,7},{10,... | collective-permute-start | bytes 614408 | tf_op jit(solution)/shard_map/ppermute | solution.py:144
  91.5 4.7 %collective-permute-start.10 = (bf16[200,512]{1,0:T(8,128)(2,1)S(1)}, bf16[200,512]{1,0:T(8,128)(2,1)S(1)}, u32[]{:S(2)}, u32[]{:S(2)}) collective-permute-start(bf16[200,512]{1,0:T(8,128)(2,1)S(1)} %collective-permute-done.9.refs_6_), channel_id=1, source_target_pairs={{0,2},{1,15},{2,4},{3,1},{4,6},{5,3},{6,8},{7,5},{8,10},{9,7},{10,... | collective-permute-start | bytes 614408 | tf_op jit(solution)/shard_map/ppermute | solution.py:144
  96.3 3.0 %collective-permute-start.24 = (bf16[200,512]{1,0:T(8,128)(2,1)S(1)}, bf16[200,512]{1,0:T(8,128)(2,1)S(1)}, u32[]{:S(2)}, u32[]{:S(2)}) collective-permute-start(bf16[200,512]{1,0:T(8,128)(2,1)S(1)} %collective-permute-done.23.refs_6_), channel_id=1, source_target_pairs={{0,2},{1,15},{2,4},{3,1},{4,6},{5,3},{6,8},{7,5},{8,10},{9,7},{10,... | collective-permute-start | bytes 614408 | tf_op jit(solution)/shard_map/ppermute | solution.py:144
  102.1 4.8 %collective-permute-start.11 = (bf16[192,256]{1,0:T(8,128)(2,1)S(1)}, bf16[192,256]{1,0:T(8,128)(2,1)S(1)}, u32[]{:S(2)}, u32[]{:S(2)}) collective-permute-start(bf16[192,256]{1,0:T(8,128)(2,1)S(1)} %hidden.2.refs_0_), channel_id=1, source_target_pairs={{0,2},{1,15},{2,4},{3,1},{4,6},{5,3},{6,8},{7,5},{8,10},{9,7},{10,... | collective-permute-start | bytes 294920 | tf_op jit(solution)/shard_map/ppermute | solution.py:144
  114.0 3.1 %collective-permute-start.26 = (bf16[192,256]{1,0:T(8,128)(2,1)S(1)}, bf16[192,256]{1,0:T(8,128)(2,1)S(1)}, u32[]{:S(2)}, u32[]{:S(2)}) collective-permute-start(bf16[192,256]{1,0:T(8,128)(2,1)S(1)} %collective-permute-done.25.refs_9_), channel_id=1, source_target_pairs={{0,2},{1,15},{2,4},{3,1},{4,6},{5,3},{6,8},{7,5},{8,10},{9,7},{10,... | collective-permute-start | bytes 294920 | tf_op jit(solution)/shard_map/ppermute | solution.py:144
  120.1 3.6 %collective-permute-start.27 = (bf16[192,256]{1,0:T(8,128)(2,1)S(1)}, bf16[192,256]{1,0:T(8,128)(2,1)S(1)}, u32[]{:S(2)}, u32[]{:S(2)}) collective-permute-start(bf16[192,256]{1,0:T(8,128)(2,1)S(1)} %collective-permute-done.26.refs_10_), channel_id=1, source_target_pairs={{0,2},{1,15},{2,4},{3,1},{4,6},{5,3},{6,8},{7,5},{8,10},{9,7},{10,... | collective-permute-start | bytes 294920 | tf_op jit(solution)/shard_map/ppermute | solution.py:144
  126.6 3.6 %collective-permute-start.28 = (bf16[192,256]{1,0:T(8,128)(2,1)S(1)}, bf16[192,256]{1,0:T(8,128)(2,1)S(1)}, u32[]{:S(2)}, u32[]{:S(2)}) collective-permute-start(bf16[192,256]{1,0:T(8,128)(2,1)S(1)} %collective-permute-done.27.refs_11_), channel_id=1, source_target_pairs={{0,2},{1,15},{2,4},{3,1},{4,6},{5,3},{6,8},{7,5},{8,10},{9,7},{10,... | collective-permute-start | bytes 294920 | tf_op jit(solution)/shard_map/ppermute | solution.py:144
  133.2 3.6 %collective-permute-start.29 = (bf16[192,256]{1,0:T(8,128)(2,1)S(1)}, bf16[192,256]{1,0:T(8,128)(2,1)S(1)}, u32[]{:S(2)}, u32[]{:S(2)}) collective-permute-start(bf16[192,256]{1,0:T(8,128)(2,1)S(1)} %collective-permute-done.28.refs_12_), channel_id=1, source_target_pairs={{0,2},{1,15},{2,4},{3,1},{4,6},{5,3},{6,8},{7,5},{8,10},{9,7},{10,... | collective-permute-start | bytes 294920 | tf_op jit(solution)/shard_map/ppermute | solution.py:144
  139.8 3.6 %collective-permute-start.30 = (bf16[192,256]{1,0:T(8,128)(2,1)S(1)}, bf16[192,256]{1,0:T(8,128)(2,1)S(1)}, u32[]{:S(2)}, u32[]{:S(2)}) collective-permute-start(bf16[192,256]{1,0:T(8,128)(2,1)S(1)} %collective-permute-done.29.refs_13_), channel_id=1, source_target_pairs={{0,2},{1,15},{2,4},{3,1},{4,6},{5,3},{6,8},{7,5},{8,10},{9,7},{10,... | collective-permute-start | bytes 294920 | tf_op jit(solution)/shard_map/ppermute | solution.py:144
  146.3 3.6 %collective-permute-start.31 = (bf16[192,256]{1,0:T(8,128)(2,1)S(1)}, bf16[192,256]{1,0:T(8,128)(2,1)S(1)}, u32[]{:S(2)}, u32[]{:S(2)}) collective-permute-start(bf16[192,256]{1,0:T(8,128)(2,1)S(1)} %collective-permute-done.30.refs_14_), channel_id=1, source_target_pairs={{0,2},{1,15},{2,4},{3,1},{4,6},{5,3},{6,8},{7,5},{8,10},{9,7},{10,... | collective-permute-start | bytes 294920 | tf_op jit(solution)/shard_map/ppermute | solution.py:144
  153.9 43.6 %all_to_all.10 = bf16[96,8,256]{2,1,0:T(8,128)(2,1)S(1)} all-to-all(bf16[96,8,256]{2,1,0:T(8,128)(2,1)S(1)} %bitcast.17), channel_id=1, replica_groups=mesh['z'=12,'x'=4,'y'=8,'c'=2] {'z','x','c'}, dimensions={0} | all-to-all | bytes 786432 | tf_op jit(solution)/shard_map/all_to_all | solution.py:216
  (68 shorter events, 44.4 us)
Async XLA Ops:
  2.8 41.5 %all-to-all-start = ((bf16[96,8,256]{2,1,0:T(8,128)(2,1)}), bf16[96,8,256]{2,1,0:T(8,128)(2,1)S(1)}, u32[]{:S(2)}, u32[]{:S(2)}) async-start(bf16[96,8,256]{2,1,0:T(8,128)(2,1)} %bitcast.4), calls=%async_computation | async-start | bytes 786432 | tf_op jit(solution)/shard_map/all_to_all | solution.py:171
  22.9 10.0 %collective-permute-start.1 = (bf16[4096,128]{1,0:T(8,128)(2,1)S(1)}, bf16[4096,128]{1,0:T(8,128)(2,1)S(1)}, u32[]{:S(2)}, u32[]{:S(2)}) collective-permute-start(bf16[4096,128]{1,0:T(8,128)(2,1)S(1)} %bitcast.11), channel_id=1, source_target_pairs={{0,1},{1,0},{2,3},{3,2},{4,5},{5,4},{6,7},{7,6},{8,9},{9,8},{10,11... | collective-permute-start | bytes 3145736 | tf_op jit(solution)/shard_map/ppermute | solution.py:149
  25.5 7.4 %collective-permute-start.2 = (bf16[4096,128]{1,0:T(8,128)(2,1)}, bf16[4096,128]{1,0:T(8,128)(2,1)S(1)}, u32[]{:S(2)}, u32[]{:S(2)}) collective-permute-start(bf16[4096,128]{1,0:T(8,128)(2,1)} %bitcast.14), channel_id=1, source_target_pairs={{0,1},{1,0},{2,3},{3,2},{4,5},{5,4},{6,7},{7,6},{8,9},{9,8},{10,11... | collective-permute-start | bytes 3145736 | tf_op jit(solution)/shard_map/ppermute | solution.py:149
  44.9 8.1 %collective-permute-start.4 = (bf16[200,512]{1,0:T(8,128)(2,1)S(1)}, bf16[200,512]{1,0:T(8,128)(2,1)S(1)}, u32[]{:S(2)}, u32[]{:S(2)}) collective-permute-start(bf16[200,512]{1,0:T(8,128)(2,1)S(1)} %get-tuple-element.14.refs_0_), channel_id=1, source_target_pairs={{0,2},{1,15},{2,4},{3,1},{4,6},{5,3},{6,8},{7,5},{8,10},{9,7},{10,... | collective-permute-start | bytes 614408 | tf_op jit(solution)/shard_map/ppermute | solution.py:144
  50.0 7.7 %collective-permute-start.18 = (bf16[200,512]{1,0:T(8,128)(2,1)S(1)}, bf16[200,512]{1,0:T(8,128)(2,1)S(1)}, u32[]{:S(2)}, u32[]{:S(2)}) collective-permute-start(bf16[200,512]{1,0:T(8,128)(2,1)S(1)} %get-tuple-element.17.refs_0_), channel_id=1, source_target_pairs={{0,2},{1,15},{2,4},{3,1},{4,6},{5,3},{6,8},{7,5},{8,10},{9,7},{10,... | collective-permute-start | bytes 614408 | tf_op jit(solution)/shard_map/ppermute | solution.py:144
  53.0 7.7 %collective-permute-start.5 = (bf16[200,512]{1,0:T(8,128)(2,1)S(1)}, bf16[200,512]{1,0:T(8,128)(2,1)S(1)}, u32[]{:S(2)}, u32[]{:S(2)}) collective-permute-start(bf16[200,512]{1,0:T(8,128)(2,1)S(1)} %collective-permute-done.4.refs_1_), channel_id=1, source_target_pairs={{0,2},{1,15},{2,4},{3,1},{4,6},{5,3},{6,8},{7,5},{8,10},{9,7},{10,... | collective-permute-start | bytes 614408 | tf_op jit(solution)/shard_map/ppermute | solution.py:144
  57.7 7.7 %collective-permute-start.19 = (bf16[200,512]{1,0:T(8,128)(2,1)S(1)}, bf16[200,512]{1,0:T(8,128)(2,1)S(1)}, u32[]{:S(2)}, u32[]{:S(2)}) collective-permute-start(bf16[200,512]{1,0:T(8,128)(2,1)S(1)} %collective-permute-done.18.refs_1_), channel_id=1, source_target_pairs={{0,2},{1,15},{2,4},{3,1},{4,6},{5,3},{6,8},{7,5},{8,10},{9,7},{10,... | collective-permute-start | bytes 614408 | tf_op jit(solution)/shard_map/ppermute | solution.py:144
  60.7 7.7 %collective-permute-start.6 = (bf16[200,512]{1,0:T(8,128)(2,1)S(1)}, bf16[200,512]{1,0:T(8,128)(2,1)S(1)}, u32[]{:S(2)}, u32[]{:S(2)}) collective-permute-start(bf16[200,512]{1,0:T(8,128)(2,1)S(1)} %collective-permute-done.5.refs_2_), channel_id=1, source_target_pairs={{0,2},{1,15},{2,4},{3,1},{4,6},{5,3},{6,8},{7,5},{8,10},{9,7},{10,... | collective-permute-start | bytes 614408 | tf_op jit(solution)/shard_map/ppermute | solution.py:144
  65.4 7.7 %collective-permute-start.20 = (bf16[200,512]{1,0:T(8,128)(2,1)S(1)}, bf16[200,512]{1,0:T(8,128)(2,1)S(1)}, u32[]{:S(2)}, u32[]{:S(2)}) collective-permute-start(bf16[200,512]{1,0:T(8,128)(2,1)S(1)} %collective-permute-done.19.refs_2_), channel_id=1, source_target_pairs={{0,2},{1,15},{2,4},{3,1},{4,6},{5,3},{6,8},{7,5},{8,10},{9,7},{10,... | collective-permute-start | bytes 614408 | tf_op jit(solution)/shard_map/ppermute | solution.py:144
  68.4 7.7 %collective-permute-start.7 = (bf16[200,512]{1,0:T(8,128)(2,1)S(1)}, bf16[200,512]{1,0:T(8,128)(2,1)S(1)}, u32[]{:S(2)}, u32[]{:S(2)}) collective-permute-start(bf16[200,512]{1,0:T(8,128)(2,1)S(1)} %collective-permute-done.6.refs_3_), channel_id=1, source_target_pairs={{0,2},{1,15},{2,4},{3,1},{4,6},{5,3},{6,8},{7,5},{8,10},{9,7},{10,... | collective-permute-start | bytes 614408 | tf_op jit(solution)/shard_map/ppermute | solution.py:144
  73.1 7.7 %collective-permute-start.21 = (bf16[200,512]{1,0:T(8,128)(2,1)S(1)}, bf16[200,512]{1,0:T(8,128)(2,1)S(1)}, u32[]{:S(2)}, u32[]{:S(2)}) collective-permute-start(bf16[200,512]{1,0:T(8,128)(2,1)S(1)} %collective-permute-done.20.refs_3_), channel_id=1, source_target_pairs={{0,2},{1,15},{2,4},{3,1},{4,6},{5,3},{6,8},{7,5},{8,10},{9,7},{10,... | collective-permute-start | bytes 614408 | tf_op jit(solution)/shard_map/ppermute | solution.py:144
  76.1 7.7 %collective-permute-start.8 = (bf16[200,512]{1,0:T(8,128)(2,1)S(1)}, bf16[200,512]{1,0:T(8,128)(2,1)S(1)}, u32[]{:S(2)}, u32[]{:S(2)}) collective-permute-start(bf16[200,512]{1,0:T(8,128)(2,1)S(1)} %collective-permute-done.7.refs_4_), channel_id=1, source_target_pairs={{0,2},{1,15},{2,4},{3,1},{4,6},{5,3},{6,8},{7,5},{8,10},{9,7},{10,... | collective-permute-start | bytes 614408 | tf_op jit(solution)/shard_map/ppermute | solution.py:144
  80.8 7.7 %collective-permute-start.22 = (bf16[200,512]{1,0:T(8,128)(2,1)S(1)}, bf16[200,512]{1,0:T(8,128)(2,1)S(1)}, u32[]{:S(2)}, u32[]{:S(2)}) collective-permute-start(bf16[200,512]{1,0:T(8,128)(2,1)S(1)} %collective-permute-done.21.refs_4_), channel_id=1, source_target_pairs={{0,2},{1,15},{2,4},{3,1},{4,6},{5,3},{6,8},{7,5},{8,10},{9,7},{10,... | collective-permute-start | bytes 614408 | tf_op jit(solution)/shard_map/ppermute | solution.py:144
  83.8 7.7 %collective-permute-start.9 = (bf16[200,512]{1,0:T(8,128)(2,1)S(1)}, bf16[200,512]{1,0:T(8,128)(2,1)S(1)}, u32[]{:S(2)}, u32[]{:S(2)}) collective-permute-start(bf16[200,512]{1,0:T(8,128)(2,1)S(1)} %collective-permute-done.8.refs_5_), channel_id=1, source_target_pairs={{0,2},{1,15},{2,4},{3,1},{4,6},{5,3},{6,8},{7,5},{8,10},{9,7},{10,... | collective-permute-start | bytes 614408 | tf_op jit(solution)/shard_map/ppermute | solution.py:144
  88.6 7.7 %collective-permute-start.23 = (bf16[200,512]{1,0:T(8,128)(2,1)S(1)}, bf16[200,512]{1,0:T(8,128)(2,1)S(1)}, u32[]{:S(2)}, u32[]{:S(2)}) collective-permute-start(bf16[200,512]{1,0:T(8,128)(2,1)S(1)} %collective-permute-done.22.refs_5_), channel_id=1, source_target_pairs={{0,2},{1,15},{2,4},{3,1},{4,6},{5,3},{6,8},{7,5},{8,10},{9,7},{10,... | collective-permute-start | bytes 614408 | tf_op jit(solution)/shard_map/ppermute | solution.py:144
  91.5 7.7 %collective-permute-start.10 = (bf16[200,512]{1,0:T(8,128)(2,1)S(1)}, bf16[200,512]{1,0:T(8,128)(2,1)S(1)}, u32[]{:S(2)}, u32[]{:S(2)}) collective-permute-start(bf16[200,512]{1,0:T(8,128)(2,1)S(1)} %collective-permute-done.9.refs_6_), channel_id=1, source_target_pairs={{0,2},{1,15},{2,4},{3,1},{4,6},{5,3},{6,8},{7,5},{8,10},{9,7},{10,... | collective-permute-start | bytes 614408 | tf_op jit(solution)/shard_map/ppermute | solution.py:144
  96.3 10.7 %collective-permute-start.24 = (bf16[200,512]{1,0:T(8,128)(2,1)S(1)}, bf16[200,512]{1,0:T(8,128)(2,1)S(1)}, u32[]{:S(2)}, u32[]{:S(2)}) collective-permute-start(bf16[200,512]{1,0:T(8,128)(2,1)S(1)} %collective-permute-done.23.refs_6_), channel_id=1, source_target_pairs={{0,2},{1,15},{2,4},{3,1},{4,6},{5,3},{6,8},{7,5},{8,10},{9,7},{10,... | collective-permute-start | bytes 614408 | tf_op jit(solution)/shard_map/ppermute | solution.py:144
  102.1 8.4 %collective-permute-start.11 = (bf16[192,256]{1,0:T(8,128)(2,1)S(1)}, bf16[192,256]{1,0:T(8,128)(2,1)S(1)}, u32[]{:S(2)}, u32[]{:S(2)}) collective-permute-start(bf16[192,256]{1,0:T(8,128)(2,1)S(1)} %hidden.2.refs_0_), channel_id=1, source_target_pairs={{0,2},{1,15},{2,4},{3,1},{4,6},{5,3},{6,8},{7,5},{8,10},{9,7},{10,... | collective-permute-start | bytes 294920 | tf_op jit(solution)/shard_map/ppermute | solution.py:144
  110.6 6.6 %collective-permute-start.12 = (bf16[192,256]{1,0:T(8,128)(2,1)S(1)}, bf16[192,256]{1,0:T(8,128)(2,1)S(1)}, u32[]{:S(2)}, u32[]{:S(2)}) collective-permute-start(bf16[192,256]{1,0:T(8,128)(2,1)S(1)} %collective-permute-done.11.refs_1_), channel_id=1, source_target_pairs={{0,2},{1,15},{2,4},{3,1},{4,6},{5,3},{6,8},{7,5},{8,10},{9,7},{10,... | collective-permute-start | bytes 294920 | tf_op jit(solution)/shard_map/ppermute | solution.py:144
  117.1 6.6 %collective-permute-start.13 = (bf16[192,256]{1,0:T(8,128)(2,1)S(1)}, bf16[192,256]{1,0:T(8,128)(2,1)S(1)}, u32[]{:S(2)}, u32[]{:S(2)}) collective-permute-start(bf16[192,256]{1,0:T(8,128)(2,1)S(1)} %collective-permute-done.12.refs_2_), channel_id=1, source_target_pairs={{0,2},{1,15},{2,4},{3,1},{4,6},{5,3},{6,8},{7,5},{8,10},{9,7},{10,... | collective-permute-start | bytes 294920 | tf_op jit(solution)/shard_map/ppermute | solution.py:144
  126.6 6.6 %collective-permute-start.28 = (bf16[192,256]{1,0:T(8,128)(2,1)S(1)}, bf16[192,256]{1,0:T(8,128)(2,1)S(1)}, u32[]{:S(2)}, u32[]{:S(2)}) collective-permute-start(bf16[192,256]{1,0:T(8,128)(2,1)S(1)} %collective-permute-done.27.refs_11_), channel_id=1, source_target_pairs={{0,2},{1,15},{2,4},{3,1},{4,6},{5,3},{6,8},{7,5},{8,10},{9,7},{10,... | collective-permute-start | bytes 294920 | tf_op jit(solution)/shard_map/ppermute | solution.py:144
  130.2 6.6 %collective-permute-start.15 = (bf16[192,256]{1,0:T(8,128)(2,1)S(1)}, bf16[192,256]{1,0:T(8,128)(2,1)S(1)}, u32[]{:S(2)}, u32[]{:S(2)}) collective-permute-start(bf16[192,256]{1,0:T(8,128)(2,1)S(1)} %collective-permute-done.14.refs_4_), channel_id=1, source_target_pairs={{0,2},{1,15},{2,4},{3,1},{4,6},{5,3},{6,8},{7,5},{8,10},{9,7},{10,... | collective-permute-start | bytes 294920 | tf_op jit(solution)/shard_map/ppermute | solution.py:144
  133.2 6.6 %collective-permute-start.29 = (bf16[192,256]{1,0:T(8,128)(2,1)S(1)}, bf16[192,256]{1,0:T(8,128)(2,1)S(1)}, u32[]{:S(2)}, u32[]{:S(2)}) collective-permute-start(bf16[192,256]{1,0:T(8,128)(2,1)S(1)} %collective-permute-done.28.refs_12_), channel_id=1, source_target_pairs={{0,2},{1,15},{2,4},{3,1},{4,6},{5,3},{6,8},{7,5},{8,10},{9,7},{10,... | collective-permute-start | bytes 294920 | tf_op jit(solution)/shard_map/ppermute | solution.py:144
  136.8 6.6 %collective-permute-start.16 = (bf16[192,256]{1,0:T(8,128)(2,1)S(1)}, bf16[192,256]{1,0:T(8,128)(2,1)S(1)}, u32[]{:S(2)}, u32[]{:S(2)}) collective-permute-start(bf16[192,256]{1,0:T(8,128)(2,1)S(1)} %collective-permute-done.15.refs_5_), channel_id=1, source_target_pairs={{0,2},{1,15},{2,4},{3,1},{4,6},{5,3},{6,8},{7,5},{8,10},{9,7},{10,... | collective-permute-start | bytes 294920 | tf_op jit(solution)/shard_map/ppermute | solution.py:144
  (18 other events, 180.2 us)

commit v3 on v2

v3 whole, which is shorter than its diff:
```python
import functools

import jax
import jax.numpy as jnp
from jax import lax
from jax.experimental import pallas as pl
from jax.experimental.pallas import tpu as pltpu
from jax.sharding import Mesh, PartitionSpec as P

BF = jnp.bfloat16
F32 = jnp.float32
VM = pl.BlockSpec(memory_space=pltpu.VMEM)
SM = pl.BlockSpec(memory_space=pltpu.SMEM)
PAD = 8


def dot(a, b):
    return jnp.dot(a, b, preferred_element_type=F32)


def dispatch_kernel(experts, cap, ids_ref, tok_ref, out_ref, pick_ref):
    rows = tok_ref.shape[0]
    expert = lax.broadcasted_iota(jnp.int32, (experts, rows), 0)
    named = (expert == ids_ref[0:1, :]) | (expert == ids_ref[1:2, :])
    before = lax.broadcasted_iota(jnp.int32, (rows, rows), 0) < lax.broadcasted_iota(
        jnp.int32, (rows, rows), 1
    )
    rank = dot(named.astype(F32).astype(BF), before.astype(F32).astype(BF))
    rank = jnp.where(named, rank, -1.0)
    slot = lax.broadcasted_iota(jnp.int32, (cap, rows), 0).astype(F32)
    for e in range(experts):
        pick_ref[e * cap : (e + 1) * cap, :] = (
            (rank[e : e + 1, :] == slot).astype(F32).astype(BF)
        )
    out_ref[...] = dot(pick_ref[...], tok_ref[...]).astype(BF)


def combine_kernel(experts, cap, ids_ref, weight_ref, back_ref, out_ref):
    rows = out_ref.shape[0]
    line = lax.broadcasted_iota(jnp.int32, (8, rows), 0)
    table = jnp.where(line == 0, ids_ref[0:1, :].astype(F32), 0.0)
    table = jnp.where(line == 1, ids_ref[1:2, :].astype(F32), table)
    table = jnp.where(line == 2, weight_ref[0:1, :], table)
    table = jnp.where(line == 3, weight_ref[1:2, :], table)
    column = table.T
    first, second = column[:, 0:1], column[:, 1:2]
    lanes = lax.broadcasted_iota(jnp.int32, (rows, 128), 1).astype(F32)
    named = (lanes == first) | (lanes == second)
    after = lax.broadcasted_iota(jnp.int32, (rows, rows), 1) < lax.broadcasted_iota(
        jnp.int32, (rows, rows), 0
    )
    rank = dot(after.astype(F32).astype(BF), named.astype(F32).astype(BF))
    place = lax.broadcasted_iota(jnp.int32, (rows, experts * cap), 1).astype(F32)
    total = None
    for k, name in enumerate((first, second)):
        mine = jnp.sum(jnp.where(lanes == name, rank, 0.0), axis=1, keepdims=True)
        pick = (place == name * cap + mine).astype(F32).astype(BF)
        term = dot(pick, back_ref[...]) * column[:, 2 + k : 3 + k]
        total = term if total is None else total + term
    out_ref[...] = total.astype(BF)


def pack_kernel(where_ref, came_ref, gain_ref, peer_gain_ref, own_ref, pair_ref):
    width = came_ref.shape[2]
    sources = came_ref.shape[0] // 2
    core = where_ref[1]
    mine, other = gain_ref[...], peer_gain_ref[...]
    gain = jnp.concatenate(
        [jnp.where(core == 0, mine, other), jnp.where(core == 0, other, mine)], axis=1
    )
    top = gain.astype(BF).astype(F32)
    mid = (gain - top).astype(BF).astype(F32)
    low = gain - top - mid
    line = lax.broadcasted_iota(jnp.int32, (PAD, 2 * width), 0)
    split = jnp.where(line == 0, top, jnp.where(line == 1, mid, jnp.where(line == 2, low, 0.0)))
    for out_ref in (own_ref, pair_ref.at[0]):
        for s in range(sources):
            for c in range(2):
                out_ref[s * 8 : s * 8 + 8, c * width : (c + 1) * width] = came_ref[2 * s + c]
        out_ref[sources * 8 : sources * 8 + PAD, :] = split.astype(BF)


def origins(where_ref, count):
    here, core = where_ref[0], where_ref[1]

    def partner(y, odd):
        return lax.rem(((y + odd) ^ 1) - odd + count, count)

    def first(y):
        return partner(y, core)

    def second(y):
        return partner(y, 1 - core)

    found = [here, first(here)]
    base = second(here)
    found += [base, first(base)]
    base = second(first(here))
    found += [base, first(base)]
    base = second(first(second(here)))
    found += [base, first(base)]
    return found


def take(refs, sizes):
    parts, at = [], 0
    for size in sizes:
        parts.append(refs[at : at + size])
        at += size
    return parts


def blocks_of(refs):
    return [ref if len(ref.shape) == 2 else ref.at[i] for ref in refs for i in range(1 if len(ref.shape) == 2 else 2)]


def hidden_kernel(count, skip, inputs, last, where_ref, *refs):
    kept = 3 if skip else 0
    blocks, weights, before, outs = take(refs, (inputs, 4, kept, len(refs) - inputs - 4 - kept))
    gate_ref, gate2_ref, up_ref, up2_ref = weights
    blocks = blocks_of(blocks)
    depth = blocks[0].shape[1]
    rows, half = blocks[0].shape[0] - PAD, gate_ref.shape[1]
    total = [ref[...] for ref in before] if skip else None
    places = origins(where_ref, count)[skip : skip + len(blocks)]
    for place, block in zip(places, blocks):
        start = pl.multiple_of(place * depth, depth)
        gain = jnp.sum(block[rows : rows + PAD, :].astype(F32), axis=0, keepdims=True)
        raw = block[0:rows, :].astype(F32)
        squares = raw * raw
        part = squares[:, 0:128]
        for lane in range(128, depth, 128):
            part = part + squares[:, lane : lane + 128]
        scaled = (raw * gain).astype(BF)
        gate = jnp.concatenate([gate_ref[pl.ds(start, depth), :], gate2_ref[pl.ds(start, depth), :]], axis=1)
        up = jnp.concatenate([up_ref[pl.ds(start, depth), :], up2_ref[pl.ds(start, depth), :]], axis=1)
        new = [dot(scaled, gate), dot(scaled, up), part]
        total = new if total is None else [t + n for t, n in zip(total, new)]
    if not last:
        for ref, value in zip(outs, total):
            ref[...] = value
        return
    mean = jnp.sum(total[2], axis=1, keepdims=True) / (depth * count)
    scale = lax.rsqrt(mean + 1e-06)
    gate, up = total[0] * scale, total[1] * scale
    hidden = (gate / (1.0 + jnp.exp(-gate)) * up).astype(BF)
    core = where_ref[1]
    for ref in (outs[0], outs[1].at[0]):
        ref[:, pl.ds(pl.multiple_of(core * half, half), half)] = hidden[:, :half]
        ref[:, pl.ds(pl.multiple_of((1 - core) * half, half), half)] = hidden[:, half:]


def down_kernel(count, skip, inputs, last, where_ref, *refs):
    kept = 2 if skip else 0
    blocks, weights, before, outs = take(refs, (inputs, 2, kept, len(refs) - inputs - 2 - kept))
    blocks = blocks_of(blocks)
    rows, depth = blocks[0].shape
    total = [ref[...] for ref in before] if skip else None
    places = origins(where_ref, count)[skip : skip + len(blocks)]
    for place, block in zip(places, blocks):
        start = pl.multiple_of(place * depth, depth)
        new = [dot(block[...], ref[pl.ds(start, depth), :]) for ref in weights]
        total = new if total is None else [t + n for t, n in zip(total, new)]
    if not last:
        for ref, value in zip(outs, total):
            ref[...] = value
        return
    core = where_ref[1]
    for s in range(rows // 8):
        outs[0][s, core] = total[0][s * 8 : s * 8 + 8, :].astype(BF)
        outs[0][s, 1 - core] = total[1][s * 8 : s * 8 + 8, :].astype(BF)


def gather(own, pair, count):
    def exchange(value, turn):
        perm = []
        for y in range(count):
            for c in range(2):
                odd = (turn + c) % 2
                perm.append((y * 2 + c, (((y + odd) ^ 1) - odd + count) % count * 2 + c))
        return lax.ppermute(value, ("y", "c"), perm)

    got = exchange(own, 0)
    pair = pair.at[1].set(got)
    second = exchange(pair, 1)
    third = exchange(second, 0)
    return [own, got, second], [third], [exchange(third, 1)]


def swap(value):
    return lax.ppermute(value, "c", [(0, 1), (1, 0)])


def body(tokens, norm_gain, expert_ids, expert_weights, gate_weight, up_weight, down_weight):
    count = lax.axis_size("y")
    experts = lax.axis_size("z") * lax.axis_size("x")
    rows, width = tokens.shape
    cap = 3 * rows * expert_ids.shape[1] // (2 * experts)
    half = experts * cap // 2
    where = jnp.stack([lax.axis_index("y"), lax.axis_index("c")]).astype(jnp.int32)
    ids = expert_ids.T
    call = pl.pallas_call

    outgoing = call(
        functools.partial(dispatch_kernel, experts, cap),
        out_shape=jax.ShapeDtypeStruct((experts * cap, width), BF),
        in_specs=[VM, VM],
        out_specs=VM,
        scratch_shapes=[pltpu.VMEM((experts * cap, rows), BF)],
        name="dispatch",
    )(ids, tokens)
    came = lax.all_to_all(outgoing.reshape(2 * experts, 8, width), ("z", "x", "c"), 0, 0, tiled=True)

    gain = norm_gain[None, :]
    gate, up, down = gate_weight[0], up_weight[0], down_weight[0]
    came, gain2, gate2, up2, down2 = lax.optimization_barrier(
        (came, swap(gain), swap(gate), swap(up), swap(down))
    )
    packed = (half + PAD, 2 * width)
    own, pair = call(
        pack_kernel,
        out_shape=[jax.ShapeDtypeStruct(packed, BF), jax.ShapeDtypeStruct((2, *packed), BF)],
        in_specs=[SM, VM, VM, VM],
        out_specs=[VM, VM],
        compiler_params=pltpu.CompilerParams(vmem_limit_bytes=8 << 20),
        name="pack",
    )(where, came, gain, gain2)

    def product(kernel, name, groups, weights, sums, outs, each):
        total, skip = [], 0
        for number, group in enumerate(groups):
            last = number == len(groups) - 1
            blocks = sum(1 if block.ndim == 2 else 2 for block in group)
            shapes = outs if last else sums
            total = call(
                functools.partial(kernel, count, skip, len(group), last),
                out_shape=shapes,
                in_specs=[SM] + [VM] * (len(group) + len(weights) + len(total)),
                out_specs=[VM] * len(shapes),
                compiler_params=pltpu.CompilerParams(vmem_limit_bytes=16 << 20),
                cost_estimate=pl.CostEstimate(
                    flops=blocks * each, bytes_accessed=blocks * each // 512, transcendentals=0
                ),
                name=name,
            )(where, *group, *weights, *total)
            skip += blocks
        return total

    ff = gate.shape[1]
    own, pair = product(
        hidden_kernel,
        "hidden",
        gather(own, pair, count),
        (gate, gate2, up, up2),
        [jax.ShapeDtypeStruct((half, 2 * ff), F32)] * 2 + [jax.ShapeDtypeStruct((half, 128), F32)],
        [jax.ShapeDtypeStruct((half, 2 * ff), BF), jax.ShapeDtypeStruct((2, half, 2 * ff), BF)],
        2 * half * 2 * width * 4 * ff,
    )
    (made,) = product(
        down_kernel,
        "down",
        gather(own, pair, count),
        (down, down2),
        [jax.ShapeDtypeStruct((half, width), F32)] * 2,
        [jax.ShapeDtypeStruct((experts, 2, 8, width), BF)],
        2 * half * 2 * ff * 2 * width,
    )
    back = lax.all_to_all(made.reshape(2 * experts, 8, width), ("z", "x", "c"), 0, 0, tiled=True)

    return call(
        functools.partial(combine_kernel, experts, cap),
        out_shape=jax.ShapeDtypeStruct((rows, width), BF),
        in_specs=[VM, VM, VM],
        out_specs=VM,
        compiler_params=pltpu.CompilerParams(vmem_limit_bytes=8 << 20),
        name="combine",
    )(ids, expert_weights.T, back.reshape(experts * cap, width))


def solution(mesh):
    split = Mesh(mesh.devices.reshape(12, 4, 8, 2), ("z", "x", "y", "c"))
    ep, tp = ("z", "x"), ("y", "c")
    in_specs = (
        P(ep, tp),
        P(tp),
        P(ep, None),
        P(ep, None),
        P(ep, None, tp),
        P(ep, None, tp),
        P(ep, None, tp),
    )
    return jax.shard_map(body, mesh=split, in_specs=in_specs, out_specs=P(ep, tp), check_vma=False)
```

time: 201 us -> 180 us (0.90)
  starting transfers between devices: 128 us -> 55.7 us
  waiting for transfers between devices: 14.8 us -> 67 us
  Pallas kernels: 8.86 us -> 14.5 us
  blocking collectives: 43.6 us -> 40 us
    ppermute x28 -> x8, starting transfers between devices: 99.5 us -> 26.7 us  [exchange(): return lax.ppermute(value, ('y', 'c'), perm)]
    ppermute x28 -> x8, waiting for transfers between devices: 2.29 us -> 54.5 us  [exchange(): return lax.ppermute(value, ('y', 'c'), perm)]
    pallas_call x4 -> x7, Pallas kernels: 6.05 us -> 10.7 us  [the longest x6 10.1 us: product(): call(functools.partial(kernel, count, skip, len(group), last), out_shape=...]
    all_to_all x1, blocking collectives: 43.6 us -> 40 us  [body(): lax.all_to_all(made.reshape(2 * experts, 8, width), ('z', 'x', 'c'), 0, 0...]
  transfers between devices with their start and end apart: 33 -> 13, of which waited for: 4 -> 10; matrix products, arithmetic and copies ran while one was open for 0% -> 0% of each run, Pallas kernels for 2% -> 4%
where the time goes in v3:
time: 180 us
  waiting for transfers between devices  67 us (37%)
  starting transfers between devices  55.7 us (31%)
  blocking collectives  40 us (22%)
  Pallas kernels  14.5 us (8%)
  local copies, waits for them, and re-layouts  1.96 us (1%)
    ppermute x8, waiting for transfers between devices, exchange(): return lax.ppermute(value, ('y', 'c'), perm)  54.5 us
    all_to_all x1, blocking collectives, body(): lax.all_to_all(made.reshape(2 * experts, 8, width), ('z', 'x', 'c'), 0, 0...  40 us
    ppermute x8, starting transfers between devices, exchange(): return lax.ppermute(value, ('y', 'c'), perm)  26.7 us
    all_to_all x1, starting transfers between devices, body(): lax.all_to_all(outgoing.reshape(2 * experts, 8, width), ('z', 'x', 'c'),...  20.1 us
    all_to_all x1, waiting for transfers between devices, body(): lax.all_to_all(outgoing.reshape(2 * experts, 8, width), ('z', 'x', 'c'),...  11.5 us
    pallas_call x6, Pallas kernels, product(): call(functools.partial(kernel, count, skip, len(group), last), out_shape=...  10.1 us
    ppermute x4, starting transfers between devices, swap(): return lax.ppermute(value, 'c', [(0, 1), (1, 0)])  8.84 us
  transfers between devices with their start and end apart: 13, of which 10 were waited for; matrix products, arithmetic and copies ran while one was open for 0% of the time, Pallas kernels for 4%

profile of v3, /device:TPU:1, one launch (start us, length us, event | category | flops | bytes accessed | tf_op | source)
XLA Modules:
  0.0 179.5 jit_solution(17403489272113115781)
XLA Ops:
  0.0 2.2 %dispatch.1 = bf16[768,256]{1,0:T(8,128)(2,1)} custom-call(s32[2,256]{1,0:T(2,128)} %bitcast.29, bf16[256,256]{1,0:T(8,128)(2,1)} %tok_ref.1), custom_call_target="tpu_custom_call" | custom-call | tf_op jit(solution)/shard_map/dispatch/pallas_call | solution.py:204
  2.2 20.1 %all-to-all-start = ((bf16[96,8,256]{2,1,0:T(8,128)(2,1)}), bf16[96,8,256]{2,1,0:T(8,128)(2,1)S(1)}, u32[]{:S(2)}, u32[]{:S(2)}) async-start(bf16[96,8,256]{2,1,0:T(8,128)(2,1)} %bitcast.34), calls=%async_computation | async-start | bytes 786432 | tf_op jit(solution)/shard_map/all_to_all | solution.py:212
  22.3 2.6 %collective-permute-start.1 = (bf16[4096,128]{1,0:T(8,128)(2,1)}, bf16[4096,128]{1,0:T(8,128)(2,1)}, u32[]{:S(2)}, u32[]{:S(2)}) collective-permute-start(bf16[4096,128]{1,0:T(8,128)(2,1)} %bitcast.19), channel_id=1, source_target_pairs={{0,1},{1,0},{2,3},{3,2},{4,5},{5,4},{6,7},{7,6},{8,9},{9,8},{10,11... | collective-permute-start | bytes 3145736 | tf_op jit(solution)/shard_map/ppermute | solution.py:191
  24.9 1.9 %collective-permute-start.2 = (bf16[4096,128]{1,0:T(8,128)(2,1)}, bf16[4096,128]{1,0:T(8,128)(2,1)}, u32[]{:S(2)}, u32[]{:S(2)}) collective-permute-start(bf16[4096,128]{1,0:T(8,128)(2,1)} %bitcast.23), channel_id=1, source_target_pairs={{0,1},{1,0},{2,3},{3,2},{4,5},{5,4},{6,7},{7,6},{8,9},{9,8},{10,11... | collective-permute-start | bytes 3145736 | tf_op jit(solution)/shard_map/ppermute | solution.py:191
  26.9 2.4 %collective-permute-start.3 = (bf16[2048,256]{1,0:T(8,128)(2,1)S(1)}, bf16[2048,256]{1,0:T(8,128)(2,1)S(1)}, u32[]{:S(2)}, u32[]{:S(2)}) collective-permute-start(bf16[2048,256]{1,0:T(8,128)(2,1)S(1)} %bitcast.15), channel_id=1, source_target_pairs={{0,1},{1,0},{2,3},{3,2},{4,5},{5,4},{6,7},{7,6},{8,9},{9,8},{10,11... | collective-permute-start | bytes 3145736 | tf_op jit(solution)/shard_map/ppermute | solution.py:191
  29.3 1.9 %collective-permute-start = (f32[1,256]{1,0:T(1,128)S(1)}, f32[1,256]{1,0:T(1,128)S(1)}, u32[]{:S(2)}, u32[]{:S(2)}) collective-permute-start(f32[1,256]{1,0:T(1,128)S(1)} %bitcast.32), channel_id=1, source_target_pairs={{0,1},{1,0},{2,3},{3,2},{4,5},{5,4},{6,7},{7,6},{8,9},{9,8},{10,11... | collective-permute-start | bytes 3080 | tf_op jit(solution)/shard_map/ppermute | solution.py:191
  32.4 11.5 %all-to-all-done.came_ref = bf16[96,8,256]{2,1,0:T(8,128)(2,1)S(1)} async-done(((bf16[96,8,256]{2,1,0:T(8,128)(2,1)}), bf16[96,8,256]{2,1,0:T(8,128)(2,1)S(1)}, u32[]{:S(2)}, u32[]{:S(2)}) %all-to-all-start) | async-done | bytes 393248 | tf_op jit(solution)/shard_map/all_to_all | solution.py:212
  44.4 5.1 %collective-permute-start.4 = (bf16[392,512]{1,0:T(8,128)(2,1)S(1)}, bf16[392,512]{1,0:T(8,128)(2,1)S(1)}, u32[]{:S(2)}, u32[]{:S(2)}) collective-permute-start(bf16[392,512]{1,0:T(8,128)(2,1)S(1)} %get-tuple-element.51.refs_0_), channel_id=1, source_target_pairs={{0,2},{1,15},{2,0},{3,5},{4,6},{5,3},{6,4},{7,9},{8,10},{9,7},{10,... | collective-permute-start | bytes 1204232 | tf_op jit(solution)/shard_map/ppermute | solution.py:181
  49.5 5.2 %collective-permute-done.4.refs_1_ = bf16[392,512]{1,0:T(8,128)(2,1)S(1)} collective-permute-done((bf16[392,512]{1,0:T(8,128)(2,1)S(1)}, bf16[392,512]{1,0:T(8,128)(2,1)S(1)}, u32[]{:S(2)}, u32[]{:S(2)}) %collective-permute-start.4) | collective-permute-done | bytes 401440 | tf_op jit(solution)/shard_map/ppermute | solution.py:181
  56.7 11.3 %collective-permute-done.5.refs_2_ = bf16[2,392,512]{2,1,0:T(8,128)(2,1)S(1)} collective-permute-done((bf16[2,392,512]{2,1,0:T(8,128)(2,1)S(1)}, bf16[2,392,512]{2,1,0:T(8,128)(2,1)S(1)}, u32[]{:S(2)}, u32[]{:S(2)}) %collective-permute-start.5) | collective-permute-done | bytes 802848 | tf_op jit(solution)/shard_map/ppermute | solution.py:181
  68.0 4.6 %collective-permute-start.6 = (bf16[2,392,512]{2,1,0:T(8,128)(2,1)S(1)}, bf16[2,392,512]{2,1,0:T(8,128)(2,1)S(1)}, u32[]{:S(2)}, u32[]{:S(2)}) collective-permute-start(bf16[2,392,512]{2,1,0:T(8,128)(2,1)S(1)} %collective-permute-done.5.refs_2_), channel_id=1, source_target_pairs={{0,2},{1,15},{2,0},{3,5},{4,6},{5,3},{6,4},{7,9},{8,10},{9,7},{10,... | collective-permute-start | bytes 2408456 | tf_op jit(solution)/shard_map/ppermute | solution.py:181
  72.6 9.5 %collective-permute-done.6.refs_0_ = bf16[2,392,512]{2,1,0:T(8,128)(2,1)S(1)} collective-permute-done((bf16[2,392,512]{2,1,0:T(8,128)(2,1)S(1)}, bf16[2,392,512]{2,1,0:T(8,128)(2,1)S(1)}, u32[]{:S(2)}, u32[]{:S(2)}) %collective-permute-start.6) | collective-permute-done | bytes 802848 | tf_op jit(solution)/shard_map/ppermute | solution.py:181
  85.3 2.7 %hidden.3 = (f32[384,256]{1,0:T(8,128)S(1)}, f32[384,256]{1,0:T(8,128)S(1)}, f32[384,128]{1,0:T(8,128)S(1)}) custom-call(s32[2]{0:T(128)S(1)} %pad_add_fusion.where_ref, bf16[392,512]{1,0:T(8,128)(2,1)S(1)} %get-tuple-element.51.refs_0_, bf16[392,512]{1,0:T(8,128)(2,1)S(1)} %collective-permute-done.4.refs_1_, ...), custom_call_target="tpu_custom_call" | custom-call | flops 805306368 | bytes 1572864 | tf_op jit(solution)/shard_map/hidden/pallas_call | solution.py:235
  87.9 2.2 %hidden.4 = (f32[384,256]{1,0:T(8,128)S(1)}, f32[384,256]{1,0:T(8,128)S(1)}, f32[384,128]{1,0:T(8,128)S(1)}) custom-call(s32[2]{0:T(128)S(1)} %pad_add_fusion.where_ref, bf16[2,392,512]{2,1,0:T(8,128)(2,1)S(1)} %collective-permute-done.6.refs_0_, bf16[4096,128]{1,0:T(8,128)(2,1)S(1)} %bitcast.21, bf16[4096,128]{1,0:T(8,128)(2,1)} %collective-permute-done.1.refs_4_.refs_2_, ...), custom_call_target="tpu_custom_call" | custom-call | flops 402653184 | bytes 786432 | tf_op jit(solution)/shard_map/hidden/pallas_call | solution.py:235
  90.1 5.2 %collective-permute-done.7.refs_0_ = bf16[2,392,512]{2,1,0:T(8,128)(2,1)S(1)} collective-permute-done((bf16[2,392,512]{2,1,0:T(8,128)(2,1)S(1)}, bf16[2,392,512]{2,1,0:T(8,128)(2,1)S(1)}, u32[]{:S(2)}, u32[]{:S(2)}) %collective-permute-start.7) | collective-permute-done | bytes 802848 | tf_op jit(solution)/shard_map/ppermute | solution.py:181
  95.3 2.3 %hidden.5 = (bf16[384,256]{1,0:T(8,128)(2,1)S(1)}, bf16[2,384,256]{2,1,0:T(8,128)(2,1)S(1)}) custom-call(s32[2]{0:T(128)S(1)} %pad_add_fusion.where_ref, bf16[2,392,512]{2,1,0:T(8,128)(2,1)S(1)} %collective-permute-done.7.refs_0_, bf16[4096,128]{1,0:T(8,128)(2,1)S(1)} %bitcast.22, bf16[4096,128]{1,0:T(8,128)(2,1)} %collective-permute-done.1.refs_4_.refs_2_, ...), custom_call_target="tpu_custom_call" | custom-call | flops 402653184 | bytes 786432 | tf_op jit(solution)/shard_map/hidden/pallas_call | solution.py:235
  97.6 4.6 %collective-permute-start.8 = (bf16[384,256]{1,0:T(8,128)(2,1)S(1)}, bf16[384,256]{1,0:T(8,128)(2,1)S(1)}, u32[]{:S(2)}, u32[]{:S(2)}) collective-permute-start(bf16[384,256]{1,0:T(8,128)(2,1)S(1)} %get-tuple-element.61.refs_0_), channel_id=1, source_target_pairs={{0,2},{1,15},{2,0},{3,5},{4,6},{5,3},{6,4},{7,9},{8,10},{9,7},{10,... | collective-permute-start | bytes 589832 | tf_op jit(solution)/shard_map/ppermute | solution.py:181
  102.2 3.0 %collective-permute-done.8.refs_1_ = bf16[384,256]{1,0:T(8,128)(2,1)S(1)} collective-permute-done((bf16[384,256]{1,0:T(8,128)(2,1)S(1)}, bf16[384,256]{1,0:T(8,128)(2,1)S(1)}, u32[]{:S(2)}, u32[]{:S(2)}) %collective-permute-start.8) | collective-permute-done | bytes 196640 | tf_op jit(solution)/shard_map/ppermute | solution.py:181
  105.2 1.9 %collective-permute-start.9 = (bf16[2,384,256]{2,1,0:T(8,128)(2,1)S(1)}, bf16[2,384,256]{2,1,0:T(8,128)(2,1)S(1)}, u32[]{:S(2)}, u32[]{:S(2)}) collective-permute-start(bf16[2,384,256]{2,1,0:T(8,128)(2,1)S(1)} %bitcast_dynamic-update-slice_fusion.1), channel_id=1, source_target_pairs={{0,14},{1,3},{2,4},{3,1},{4,2},{5,7},{6,8},{7,5},{8,6},{9,11},{10,... | collective-permute-start | bytes 1179656 | tf_op jit(solution)/shard_map/ppermute | solution.py:181
  107.2 6.7 %collective-permute-done.9.refs_2_ = bf16[2,384,256]{2,1,0:T(8,128)(2,1)S(1)} collective-permute-done((bf16[2,384,256]{2,1,0:T(8,128)(2,1)S(1)}, bf16[2,384,256]{2,1,0:T(8,128)(2,1)S(1)}, u32[]{:S(2)}, u32[]{:S(2)}) %collective-permute-start.9) | collective-permute-done | bytes 393248 | tf_op jit(solution)/shard_map/ppermute | solution.py:181
  113.9 4.8 %collective-permute-start.10 = (bf16[2,384,256]{2,1,0:T(8,128)(2,1)S(1)}, bf16[2,384,256]{2,1,0:T(8,128)(2,1)S(1)}, u32[]{:S(2)}, u32[]{:S(2)}) collective-permute-start(bf16[2,384,256]{2,1,0:T(8,128)(2,1)S(1)} %collective-permute-done.9.refs_2_), channel_id=1, source_target_pairs={{0,2},{1,15},{2,0},{3,5},{4,6},{5,3},{6,4},{7,9},{8,10},{9,7},{10,... | collective-permute-start | bytes 1179656 | tf_op jit(solution)/shard_map/ppermute | solution.py:181
  118.8 6.5 %collective-permute-done.10.refs_0_ = bf16[2,384,256]{2,1,0:T(8,128)(2,1)S(1)} collective-permute-done((bf16[2,384,256]{2,1,0:T(8,128)(2,1)S(1)}, bf16[2,384,256]{2,1,0:T(8,128)(2,1)S(1)}, u32[]{:S(2)}, u32[]{:S(2)}) %collective-permute-start.10) | collective-permute-done | bytes 393248 | tf_op jit(solution)/shard_map/ppermute | solution.py:181
  129.2 7.0 %collective-permute-done.11.refs_0_ = bf16[2,384,256]{2,1,0:T(8,128)(2,1)S(1)} collective-permute-done((bf16[2,384,256]{2,1,0:T(8,128)(2,1)S(1)}, bf16[2,384,256]{2,1,0:T(8,128)(2,1)S(1)}, u32[]{:S(2)}, u32[]{:S(2)}) %collective-permute-start.11) | collective-permute-done | bytes 393248 | tf_op jit(solution)/shard_map/ppermute | solution.py:181
  137.2 40.0 %all_to_all.10 = bf16[96,8,256]{2,1,0:T(8,128)(2,1)S(1)} all-to-all(bf16[96,8,256]{2,1,0:T(8,128)(2,1)S(1)} %bitcast.28), channel_id=1, replica_groups=mesh['z'=12,'x'=4,'y'=8,'c'=2] {'z','x','c'}, dimensions={0} | all-to-all | bytes 786432 | tf_op jit(solution)/shard_map/all_to_all | solution.py:268
  (29 shorter events, 14.1 us)
Async XLA Ops:
  0.0 26.9 %copy-start = (bf16[1,2048,256]{2,1,0:T(8,128)(2,1)S(1)}, bf16[1,2048,256]{2,1,0:T(8,128)(2,1)}, u32[]{:S(2)}) copy-start(bf16[1,2048,256]{2,1,0:T(8,128)(2,1)} %param.17) | copy-start | bytes 3145732
  0.0 29.3 %copy-start.6 = (f32[256]{0:T(256)S(1)}, f32[256]{0:T(256)}, u32[]{:S(2)}) copy-start(f32[256]{0:T(256)} %param.12) | copy-start | bytes 3076
  2.2 81.9 %copy-start.1 = (bf16[1,4096,128]{2,1,0:T(8,128)(2,1)S(1)}, bf16[1,4096,128]{2,1,0:T(8,128)(2,1)}, u32[]{:S(2)}) copy-start(bf16[1,4096,128]{2,1,0:T(8,128)(2,1)} %param.15) | copy-start | bytes 3145732
  2.2 41.7 %all-to-all-start = ((bf16[96,8,256]{2,1,0:T(8,128)(2,1)}), bf16[96,8,256]{2,1,0:T(8,128)(2,1)S(1)}, u32[]{:S(2)}, u32[]{:S(2)}) async-start(bf16[96,8,256]{2,1,0:T(8,128)(2,1)} %bitcast.34), calls=%async_computation | async-start | bytes 786432 | tf_op jit(solution)/shard_map/all_to_all | solution.py:212
  22.3 10.0 %collective-permute-start.1 = (bf16[4096,128]{1,0:T(8,128)(2,1)}, bf16[4096,128]{1,0:T(8,128)(2,1)}, u32[]{:S(2)}, u32[]{:S(2)}) collective-permute-start(bf16[4096,128]{1,0:T(8,128)(2,1)} %bitcast.19), channel_id=1, source_target_pairs={{0,1},{1,0},{2,3},{3,2},{4,5},{5,4},{6,7},{7,6},{8,9},{9,8},{10,11... | collective-permute-start | bytes 3145736 | tf_op jit(solution)/shard_map/ppermute | solution.py:191
  24.9 7.4 %collective-permute-start.2 = (bf16[4096,128]{1,0:T(8,128)(2,1)}, bf16[4096,128]{1,0:T(8,128)(2,1)}, u32[]{:S(2)}, u32[]{:S(2)}) collective-permute-start(bf16[4096,128]{1,0:T(8,128)(2,1)} %bitcast.23), channel_id=1, source_target_pairs={{0,1},{1,0},{2,3},{3,2},{4,5},{5,4},{6,7},{7,6},{8,9},{9,8},{10,11... | collective-permute-start | bytes 3145736 | tf_op jit(solution)/shard_map/ppermute | solution.py:191
  26.9 5.5 %collective-permute-start.3 = (bf16[2048,256]{1,0:T(8,128)(2,1)S(1)}, bf16[2048,256]{1,0:T(8,128)(2,1)S(1)}, u32[]{:S(2)}, u32[]{:S(2)}) collective-permute-start(bf16[2048,256]{1,0:T(8,128)(2,1)S(1)} %bitcast.15), channel_id=1, source_target_pairs={{0,1},{1,0},{2,3},{3,2},{4,5},{5,4},{6,7},{7,6},{8,9},{9,8},{10,11... | collective-permute-start | bytes 3145736 | tf_op jit(solution)/shard_map/ppermute | solution.py:191
  29.3 3.1 %collective-permute-start = (f32[1,256]{1,0:T(1,128)S(1)}, f32[1,256]{1,0:T(1,128)S(1)}, u32[]{:S(2)}, u32[]{:S(2)}) collective-permute-start(f32[1,256]{1,0:T(1,128)S(1)} %bitcast.32), channel_id=1, source_target_pairs={{0,1},{1,0},{2,3},{3,2},{4,5},{5,4},{6,7},{7,6},{8,9},{9,8},{10,11... | collective-permute-start | bytes 3080 | tf_op jit(solution)/shard_map/ppermute | solution.py:191
  44.4 10.3 %collective-permute-start.4 = (bf16[392,512]{1,0:T(8,128)(2,1)S(1)}, bf16[392,512]{1,0:T(8,128)(2,1)S(1)}, u32[]{:S(2)}, u32[]{:S(2)}) collective-permute-start(bf16[392,512]{1,0:T(8,128)(2,1)S(1)} %get-tuple-element.51.refs_0_), channel_id=1, source_target_pairs={{0,2},{1,15},{2,0},{3,5},{4,6},{5,3},{6,4},{7,9},{8,10},{9,7},{10,... | collective-permute-start | bytes 1204232 | tf_op jit(solution)/shard_map/ppermute | solution.py:181
  54.8 13.2 %collective-permute-start.5 = (bf16[2,392,512]{2,1,0:T(8,128)(2,1)S(1)}, bf16[2,392,512]{2,1,0:T(8,128)(2,1)S(1)}, u32[]{:S(2)}, u32[]{:S(2)}) collective-permute-start(bf16[2,392,512]{2,1,0:T(8,128)(2,1)S(1)} %bitcast_dynamic-update-slice_fusion), channel_id=1, source_target_pairs={{0,14},{1,3},{2,4},{3,1},{4,2},{5,7},{6,8},{7,5},{8,6},{9,11},{10,... | collective-permute-start | bytes 2408456 | tf_op jit(solution)/shard_map/ppermute | solution.py:181
  68.0 14.1 %collective-permute-start.6 = (bf16[2,392,512]{2,1,0:T(8,128)(2,1)S(1)}, bf16[2,392,512]{2,1,0:T(8,128)(2,1)S(1)}, u32[]{:S(2)}, u32[]{:S(2)}) collective-permute-start(bf16[2,392,512]{2,1,0:T(8,128)(2,1)S(1)} %collective-permute-done.5.refs_2_), channel_id=1, source_target_pairs={{0,2},{1,15},{2,0},{3,5},{4,6},{5,3},{6,4},{7,9},{8,10},{9,7},{10,... | collective-permute-start | bytes 2408456 | tf_op jit(solution)/shard_map/ppermute | solution.py:181
  82.1 13.2 %collective-permute-start.7 = (bf16[2,392,512]{2,1,0:T(8,128)(2,1)S(1)}, bf16[2,392,512]{2,1,0:T(8,128)(2,1)S(1)}, u32[]{:S(2)}, u32[]{:S(2)}) collective-permute-start(bf16[2,392,512]{2,1,0:T(8,128)(2,1)S(1)} %collective-permute-done.6.refs_0_), channel_id=1, source_target_pairs={{0,14},{1,3},{2,4},{3,1},{4,2},{5,7},{6,8},{7,5},{8,6},{9,11},{10,... | collective-permute-start | bytes 2408456 | tf_op jit(solution)/shard_map/ppermute | solution.py:181
  84.0 1.2 copy-start.2
  85.3 2.7 %copy-start.3 = (bf16[1,4096,128]{2,1,0:T(8,128)(2,1)S(1)}, bf16[1,4096,128]{2,1,0:T(8,128)(2,1)}, u32[]{:S(2)}) copy-start(bf16[1,4096,128]{2,1,0:T(8,128)(2,1)} %param.16) | copy-start | bytes 3145732
  97.6 7.6 %collective-permute-start.8 = (bf16[384,256]{1,0:T(8,128)(2,1)S(1)}, bf16[384,256]{1,0:T(8,128)(2,1)S(1)}, u32[]{:S(2)}, u32[]{:S(2)}) collective-permute-start(bf16[384,256]{1,0:T(8,128)(2,1)S(1)} %get-tuple-element.61.refs_0_), channel_id=1, source_target_pairs={{0,2},{1,15},{2,0},{3,5},{4,6},{5,3},{6,4},{7,9},{8,10},{9,7},{10,... | collective-permute-start | bytes 589832 | tf_op jit(solution)/shard_map/ppermute | solution.py:181
  105.2 8.7 %collective-permute-start.9 = (bf16[2,384,256]{2,1,0:T(8,128)(2,1)S(1)}, bf16[2,384,256]{2,1,0:T(8,128)(2,1)S(1)}, u32[]{:S(2)}, u32[]{:S(2)}) collective-permute-start(bf16[2,384,256]{2,1,0:T(8,128)(2,1)S(1)} %bitcast_dynamic-update-slice_fusion.1), channel_id=1, source_target_pairs={{0,14},{1,3},{2,4},{3,1},{4,2},{5,7},{6,8},{7,5},{8,6},{9,11},{10,... | collective-permute-start | bytes 1179656 | tf_op jit(solution)/shard_map/ppermute | solution.py:181
  113.9 11.3 %collective-permute-start.10 = (bf16[2,384,256]{2,1,0:T(8,128)(2,1)S(1)}, bf16[2,384,256]{2,1,0:T(8,128)(2,1)S(1)}, u32[]{:S(2)}, u32[]{:S(2)}) collective-permute-start(bf16[2,384,256]{2,1,0:T(8,128)(2,1)S(1)} %collective-permute-done.9.refs_2_), channel_id=1, source_target_pairs={{0,2},{1,15},{2,0},{3,5},{4,6},{5,3},{6,4},{7,9},{8,10},{9,7},{10,... | collective-permute-start | bytes 1179656 | tf_op jit(solution)/shard_map/ppermute | solution.py:181
  125.2 11.0 %collective-permute-start.11 = (bf16[2,384,256]{2,1,0:T(8,128)(2,1)S(1)}, bf16[2,384,256]{2,1,0:T(8,128)(2,1)S(1)}, u32[]{:S(2)}, u32[]{:S(2)}) collective-permute-start(bf16[2,384,256]{2,1,0:T(8,128)(2,1)S(1)} %collective-permute-done.10.refs_0_), channel_id=1, source_target_pairs={{0,14},{1,3},{2,4},{3,1},{4,2},{5,7},{6,8},{7,5},{8,6},{9,11},{10,... | collective-permute-start | bytes 1179656 | tf_op jit(solution)/shard_map/ppermute | solution.py:181
  137.1 40.1 %copy-start.5 = (f32[256,2]{0,1:T(2,128)S(1)}, f32[256,2]{0,1:T(2,128)}, u32[]{:S(2)}) copy-start(f32[256,2]{0,1:T(2,128)} %param.14) | copy-start | bytes 6148
  177.2 0.7 copy-start.4

commit v4 on v0

v4 whole, which is shorter than its diff:
```python
import functools

import jax
import jax.numpy as jnp
from jax import lax
from jax.experimental import pallas as pl
from jax.experimental.pallas import tpu as pltpu
from jax.sharding import Mesh, PartitionSpec as P

BF = jnp.bfloat16
F32 = jnp.float32
VM = pl.BlockSpec(memory_space=pltpu.VMEM)
SM = pl.BlockSpec(memory_space=pltpu.SMEM)
PAD = 8
LANES = 128
QUART = 4


def dot(a, b):
    return jnp.dot(a, b, preferred_element_type=F32)


def ones_where(mask):
    return mask.astype(F32).astype(BF)


def dispatch_kernel(experts, cap, ids_ref, tok_ref, out_ref, pick_ref):
    rows = tok_ref.shape[0]
    expert = lax.broadcasted_iota(jnp.int32, (experts, rows), 0)
    named = (expert == ids_ref[0:1, :]) | (expert == ids_ref[1:2, :])
    before = lax.broadcasted_iota(jnp.int32, (rows, rows), 0) < lax.broadcasted_iota(
        jnp.int32, (rows, rows), 1
    )
    rank = jnp.where(named, dot(ones_where(named), ones_where(before)), -1.0)
    line = lax.broadcasted_iota(jnp.int32, (2 * cap, 2 * rows), 0)
    column = lax.broadcasted_iota(jnp.int32, (2 * cap, 2 * rows), 1)
    slot = line // 8 * QUART + line % QUART
    wanted = jnp.where(line % 8 // QUART == column // rows, slot, -2).astype(F32)
    rank2 = jnp.concatenate([rank, rank], axis=1)
    for e in range(experts):
        pick_ref[e * 2 * cap : (e + 1) * 2 * cap, :] = ones_where(rank2[e : e + 1, :] == wanted)
    halves = jnp.concatenate([tok_ref[:, :LANES], tok_ref[:, LANES:]], axis=0)
    out_ref[...] = dot(pick_ref[...], halves).astype(BF)


def combine_kernel(experts, cap, ids_ref, weight_ref, back_ref, out_ref):
    rows = out_ref.shape[0]
    line = lax.broadcasted_iota(jnp.int32, (8, rows), 0)
    table = jnp.where(line == 0, ids_ref[0:1, :].astype(F32), 0.0)
    table = jnp.where(line == 1, ids_ref[1:2, :].astype(F32), table)
    table = jnp.where(line == 2, weight_ref[0:1, :], table)
    table = jnp.where(line == 3, weight_ref[1:2, :], table)
    column = table.T
    first, second = column[:, 0:1], column[:, 1:2]
    lanes = lax.broadcasted_iota(jnp.int32, (rows, LANES), 1).astype(F32)
    named = (lanes == first) | (lanes == second)
    after = lax.broadcasted_iota(jnp.int32, (rows, rows), 1) < lax.broadcasted_iota(
        jnp.int32, (rows, rows), 0
    )
    rank = dot(ones_where(after), ones_where(named))
    place = lax.broadcasted_iota(jnp.int32, (rows, experts * 2 * cap), 1).astype(F32)
    total = [None, None]
    for k, name in enumerate((first, second)):
        mine = jnp.sum(jnp.where(lanes == name, rank, 0.0), axis=1, keepdims=True)
        at = name * (2 * cap) + jnp.floor(mine / QUART) * QUART + mine
        for half in range(2):
            pick = ones_where(place == at + half * QUART)
            term = dot(pick, back_ref[...]) * column[:, 2 + k : 3 + k]
            total[half] = term if k == 0 else total[half] + term
    out_ref[:, :LANES] = total[0].astype(BF)
    out_ref[:, LANES:] = total[1].astype(BF)


def trade(a, b):
    top = lax.broadcasted_iota(jnp.int32, a.shape, 0) < QUART
    return jnp.where(top, a, pltpu.roll(b, QUART, 0)), jnp.where(top, pltpu.roll(a, QUART, 0), b)


def pack_kernel(came_ref, gain_ref, *out_refs):
    sources = came_ref.shape[0] // len(out_refs)
    parts = came_ref.shape[1]
    for number, out_ref in enumerate(out_refs):
        for s in range(0, sources, 2):
            for part in range(parts):
                a = came_ref[number * sources + s, part].astype(F32)
                b = came_ref[number * sources + s + 1, part].astype(F32)
                for half, tile in enumerate(trade(a, b)):
                    at = (2 * part + half) * LANES
                    out_ref[s * QUART : s * QUART + 8, at : at + LANES] = tile.astype(BF)
    gain = jnp.concatenate([gain_ref[i : i + 1, :] for i in range(parts)], axis=1)
    top = gain.astype(BF).astype(F32)
    mid = (gain - top).astype(BF).astype(F32)
    low = gain - top - mid
    line = lax.broadcasted_iota(jnp.int32, (PAD, gain.shape[1]), 0)
    split = jnp.where(line == 0, top, jnp.where(line == 1, mid, jnp.where(line == 2, low, 0.0)))
    out_refs[0][sources * QUART :, :] = split.astype(BF)


def positions(where_ref):
    chip, core = where_ref[0], where_ref[1]
    return [chip * 2 + core, chip * 2 + 1 - core, (1 - chip) * 2 + core, (1 - chip) * 2 + 1 - core]


def hidden_kernel(where_ref, a_ref, b_ref, *refs):
    gates, ups, out_ref = refs[:4], refs[4:8], refs[8]
    blocks, _, depth = a_ref.shape
    half, piece = b_ref.shape[1], gates[0].shape[1]
    square, sums = None, [None] * 4
    for q in range(blocks):
        gain = jnp.sum(a_ref[q, half:, :].astype(F32), axis=0, keepdims=True)
        raw = jnp.concatenate([a_ref[q, :half, :].astype(F32), b_ref[q].astype(F32)], axis=0)
        squares = raw * raw
        part = squares[:, :LANES]
        for lane in range(LANES, depth, LANES):
            part = part + squares[:, lane : lane + LANES]
        square = part if q == 0 else square + part
        scaled = (raw * gain).astype(BF)
        for i, (first, second) in enumerate((gates[:2], ups[:2], gates[2:], ups[2:])):
            span = slice(q * depth, (q + 1) * depth)
            new = dot(scaled, jnp.concatenate([first[span, :], second[span, :]], axis=1))
            sums[i] = new if q == 0 else sums[i] + new
    mean = jnp.sum(square, axis=1, keepdims=True) / (depth * blocks)
    scale = lax.rsqrt(mean + 1e-06)
    place = positions(where_ref)
    for i in range(2):
        gate, up = sums[2 * i] * scale, sums[2 * i + 1] * scale
        hidden = (gate / (1.0 + jnp.exp(-gate)) * up).astype(BF)
        for j in range(2):
            at = pl.multiple_of(place[2 * i + j] * piece, piece)
            out_ref[:, pl.ds(at, piece)] = hidden[:, j * piece : (j + 1) * piece]


def down_kernel(where_ref, hidden_ref, *refs):
    downs, out_ref = refs[:4], refs[4]
    blocks, rows, depth = hidden_ref.shape
    for place, down in zip(positions(where_ref), downs):
        total = None
        for q in range(blocks):
            new = dot(hidden_ref[q], down[q * depth : (q + 1) * depth, :])
            total = new if q == 0 else total + new
        for s in range(0, rows // QUART, 2):
            at = s * QUART
            first, second = trade(total[at : at + 8, :LANES], total[at : at + 8, LANES:])
            out_ref[s, place] = first.astype(BF)
            out_ref[s + 1, place] = second.astype(BF)


def body(tokens, norm_gain, expert_ids, expert_weights, gate_weight, up_weight, down_weight):
    experts = lax.axis_size("z") * lax.axis_size("x")
    parts = lax.axis_size("p") * lax.axis_size("c")
    rows, width = tokens.shape
    cap = 3 * rows * expert_ids.shape[1] // (2 * experts)
    quarter = experts * cap // parts
    where = jnp.stack([lax.axis_index("p"), lax.axis_index("c")]).astype(jnp.int32)
    ids = expert_ids.T
    wide = ("z", "x", "p", "c")

    def params(mib, flops=0):
        return dict(
            compiler_params=pltpu.CompilerParams(vmem_limit_bytes=mib << 20),
            cost_estimate=pl.CostEstimate(flops=flops, bytes_accessed=1 << 20, transcendentals=0),
        )

    def swap(value, axis):
        return lax.ppermute(value, axis, [(0, 1), (1, 0)])

    outgoing = pl.pallas_call(
        functools.partial(dispatch_kernel, experts, cap),
        out_shape=jax.ShapeDtypeStruct((experts * 2 * cap, LANES), BF),
        in_specs=[VM, VM],
        out_specs=VM,
        scratch_shapes=[pltpu.VMEM((experts * 2 * cap, 2 * rows), BF)],
        name="dispatch",
    )(ids, tokens)
    came = lax.all_to_all(outgoing.reshape(experts * parts, 8, LANES), wide, 0, 0, tiled=True)

    own = [gate_weight[0], up_weight[0], down_weight[0]]
    over = [swap(w, "p") for w in own]
    side = [swap(w, "c") for w in own]
    gains = lax.all_gather(norm_gain, ("p", "c"), axis=0)
    came, gains, side = lax.optimization_barrier((came, gains, side))

    one, two = pl.pallas_call(
        pack_kernel,
        out_shape=[
            jax.ShapeDtypeStruct((quarter // 2 + PAD, parts * width), BF),
            jax.ShapeDtypeStruct((quarter // 2, parts * width), BF),
        ],
        in_specs=[VM, VM],
        out_specs=[VM, VM],
        name="pack",
        **params(8),
    )(came.reshape(experts, parts, 8, LANES), gains)
    one = lax.all_gather(one, "q", axis=0)
    one, over[0], over[1] = lax.optimization_barrier((one, over[0], over[1]))
    far = [swap(w, "c") for w in over[:2]]
    two = lax.all_gather(two, "q", axis=0)

    piece = gate_weight.shape[2]
    hidden = pl.pallas_call(
        hidden_kernel,
        out_shape=jax.ShapeDtypeStruct((quarter, parts * piece), BF),
        in_specs=[SM] + [VM] * 10,
        out_specs=VM,
        name="hidden",
        **params(24, 1 << 31),
    )(where, one, two, own[0], side[0], over[0], far[0], own[1], side[1], over[1], far[1])
    hidden, over[2] = lax.optimization_barrier((hidden, over[2]))
    far.append(swap(over[2], "c"))
    hidden = lax.all_gather(hidden, "q", axis=0)

    made = pl.pallas_call(
        down_kernel,
        out_shape=jax.ShapeDtypeStruct((experts, parts, 8, LANES), BF),
        in_specs=[SM] + [VM] * 5,
        out_specs=VM,
        name="down",
        **params(16, 1 << 30),
    )(where, hidden, own[2], side[2], over[2], far[2])
    back = lax.all_to_all(made.reshape(experts * parts, 8, LANES), wide, 0, 0, tiled=True)

    return pl.pallas_call(
        functools.partial(combine_kernel, experts, cap),
        out_shape=jax.ShapeDtypeStruct((rows, width), BF),
        in_specs=[VM, VM, VM],
        out_specs=VM,
        name="combine",
        **params(16),
    )(ids, expert_weights.T, back.reshape(experts * 2 * cap, LANES))


def solution(mesh):
    split = Mesh(mesh.devices.reshape(12, 4, 4, 2, 2), ("z", "x", "q", "p", "c"))
    ep, tp = ("z", "x"), ("q", "p", "c")
    in_specs = (
        P(ep, tp),
        P(tp),
        P(ep, None),
        P(ep, None),
        P(ep, None, tp),
        P(ep, None, tp),
        P(ep, None, tp),
    )
    return jax.shard_map(body, mesh=split, in_specs=in_specs, out_specs=P(ep, tp), check_vma=False)
```

time: 237 us -> 227 us (0.958)
  waiting for transfers between devices: 128 us -> 0.03 us
  blocking collectives: 32.5 us -> 160 us
  starting transfers between devices: 26.4 us -> 47.7 us
  between operations: 13.6 us -> 0.18 us
  other arithmetic: 11.9 us -> 0.08 us
  Pallas kernels: 0 us -> 11.4 us
  matrix products: 10.1 us -> 0 us
  local copies, waits for them, and re-layouts: 12.8 us -> 6.09 us
    all_gather x0 -> x4, blocking collectives: none -> 121 us  [the longest x1 46.7 us: body(): gains = lax.all_gather(norm_gain, ('p', 'c'), axis=0)]
    all_gather x2 -> x0, waiting for transfers between devices: 104 us -> none  [the longest x1 54.5 us: body(): block_part = lax.all_gather(arrived, 'tp', axis=2, tiled=True)]
    ppermute x0 -> x9, starting transfers between devices: none -> 25.5 us  [swap(): return lax.ppermute(value, axis, [(0, 1), (1, 0)])]
    all_to_all x2 -> x1, waiting for transfers between devices: 23.3 us -> 0.01 us  [body(): lax.all_to_all(outgoing.reshape(experts * parts, 8, LANES), wide, 0, 0, t...]
    pallas_call x0 -> x5, Pallas kernels: none -> 11.4 us  [the longest x1 4.26 us: body(): pl.pallas_call(hidden_kernel, out_shape=jax.ShapeDtypeStruct((quarter, pa...]
    dot_general x3 -> x0, matrix products: 10.1 us -> none  [the longest x1 4.72 us: body(): jnp.einsum('erd,edf->erf', block_part, gate_weight, preferred_element_typ...]
    all_to_all x1, blocking collectives: 32.5 us -> 39.3 us  [body(): lax.all_to_all(made.reshape(experts * parts, 8, LANES), wide, 0, 0, tiled...]
    unnamed x2 -> x0, other arithmetic: 6.23 us -> none
  transfers between devices with their start and end apart: 4 -> 10, of which waited for: 4 -> 0; matrix products, arithmetic and copies ran while one was open for 2% -> 0% of each run, Pallas kernels for 0% -> 2%
where the time goes in v4:
time: 227 us; the launch traced here: 226 us
  blocking collectives  160 us (70%)
  starting transfers between devices  47.7 us (21%)
  Pallas kernels  11.4 us (5%)
  local copies, waits for them, and re-layouts  6.09 us (3%)
    all_gather x1, blocking collectives, body(): gains = lax.all_gather(norm_gain, ('p', 'c'), axis=0)  46.7 us
    all_to_all x1, blocking collectives, body(): lax.all_to_all(made.reshape(experts * parts, 8, LANES), wide, 0, 0, tiled...  39.3 us
    all_gather x1, blocking collectives, body(): two = lax.all_gather(two, 'q', axis=0)  37.7 us
    ppermute x9, starting transfers between devices, swap(): return lax.ppermute(value, axis, [(0, 1), (1, 0)])  25.5 us
    all_to_all x1, starting transfers between devices, body(): lax.all_to_all(outgoing.reshape(experts * parts, 8, LANES), wide, 0, 0, t...  22.2 us
    all_gather x1, blocking collectives, body(): one = lax.all_gather(one, 'q', axis=0)  21 us
    all_gather x1, blocking collectives, body(): hidden = lax.all_gather(hidden, 'q', axis=0)  15.4 us
    unnamed x25, local copies, waits for them, and re-layouts  6.09 us
  transfers between devices with their start and end apart: 10, of which 0 were waited for; matrix products, arithmetic and copies ran while one was open for 0% of the time, Pallas kernels for 2%

profile of v4, /device:TPU:1, one launch (start us, length us, event | category | flops | bytes accessed | tf_op | source)
XLA Modules:
  0.0 225.6 jit_solution(7981243778453618498)
XLA Ops:
  0.0 2.5 %dispatch.1 = bf16[1536,128]{1,0:T(8,128)(2,1)} custom-call(s32[2,256]{1,0:T(2,128)} %bitcast.34, bf16[256,256]{1,0:T(8,128)(2,1)} %tok_ref.1), custom_call_target="tpu_custom_call" | custom-call | tf_op jit(solution)/shard_map/dispatch/pallas_call | solution.py:167
  2.5 22.2 %all-to-all-start = ((bf16[192,8,128]{2,1,0:T(8,128)(2,1)}), bf16[192,8,128]{2,1,0:T(8,128)(2,1)S(1)}, u32[]{:S(2)}, u32[]{:S(2)}) async-start(bf16[192,8,128]{2,1,0:T(8,128)(2,1)} %bitcast.37), calls=%async_computation | async-start | bytes 786432 | tf_op jit(solution)/shard_map/all_to_all | solution.py:175
  24.7 3.2 %collective-permute-start = (bf16[4096,128]{1,0:T(8,128)(2,1)S(1)}, bf16[4096,128]{1,0:T(8,128)(2,1)S(1)}, u32[]{:S(2)}, u32[]{:S(2)}) collective-permute-start(bf16[4096,128]{1,0:T(8,128)(2,1)S(1)} %bitcast.24), channel_id=1, source_target_pairs={{0,1},{1,0},{2,3},{3,2},{4,5},{5,4},{6,7},{7,6},{8,9},{9,8},{10,11... | collective-permute-start | bytes 3145736 | tf_op jit(solution)/shard_map/ppermute | solution.py:165
  27.9 1.9 collective-permute-start.1
  29.9 2.4 %collective-permute-start.2 = (bf16[2048,256]{1,0:T(8,128)(2,1)}, bf16[2048,256]{1,0:T(8,128)(2,1)S(1)}, u32[]{:S(2)}, u32[]{:S(2)}) collective-permute-start(bf16[2048,256]{1,0:T(8,128)(2,1)} %bitcast.30), channel_id=1, source_target_pairs={{0,1},{1,0},{2,3},{3,2},{4,5},{5,4},{6,7},{7,6},{8,9},{9,8},{10,11... | collective-permute-start | bytes 3145736 | tf_op jit(solution)/shard_map/ppermute | solution.py:165
  32.3 2.3 %collective-permute-start.3 = (bf16[4096,128]{1,0:T(8,128)(2,1)S(1)}, bf16[4096,128]{1,0:T(8,128)(2,1)}, u32[]{:S(2)}, u32[]{:S(2)}) collective-permute-start(bf16[4096,128]{1,0:T(8,128)(2,1)S(1)} %bitcast.25), channel_id=1, source_target_pairs={{0,2},{2,0},{1,3},{3,1},{4,6},{6,4},{5,7},{7,5},{8,10},{10,8},{9,1... | collective-permute-start | bytes 3145736 | tf_op jit(solution)/shard_map/ppermute | solution.py:165
  34.6 3.0 %collective-permute-start.4 = (bf16[4096,128]{1,0:T(8,128)(2,1)}, bf16[4096,128]{1,0:T(8,128)(2,1)}, u32[]{:S(2)}, u32[]{:S(2)}) collective-permute-start(bf16[4096,128]{1,0:T(8,128)(2,1)} %bitcast.28), channel_id=1, source_target_pairs={{0,2},{2,0},{1,3},{3,1},{4,6},{6,4},{5,7},{7,5},{8,10},{10,8},{9,1... | collective-permute-start | bytes 3145736 | tf_op jit(solution)/shard_map/ppermute | solution.py:165
  37.6 46.7 %all-gather.4 = f32[4,1,256]{2,1,0:T(1,128)S(1)} all-gather(f32[1,1,256]{2,1,0:T(1,128)S(1)} %bitcast.38), channel_id=2, replica_groups=mesh['z'=12,'x'=4,'q'=4,'p'=2,'c'=2] {'p','c'}, dimensions={0}, use_global_device_ids=true | all-gather | bytes 5120 | tf_op jit(solution)/shard_map/all_gather | solution.py:180
  84.3 1.0 copy-done.2
  85.3 1.0 copy-done.4
  86.3 1.0 copy-done.7
  87.4 21.0 %all-gather.1 = bf16[416,1024]{1,0:T(8,128)(2,1)S(1)} all-gather(bf16[104,1024]{1,0:T(8,128)(2,1)S(1)} %get-tuple-element.19), channel_id=3, replica_groups=mesh['z'=12,'x'=4,'q'=4,'p'=2,'c'=2] {'q'}, dimensions={0}, use_global_device_ids=true | all-gather | bytes 1064960 | tf_op jit(solution)/shard_map/all_gather | solution.py:194
  108.4 3.9 %collective-permute-start.5 = (bf16[4096,128]{1,0:T(8,128)(2,1)}, bf16[4096,128]{1,0:T(8,128)(2,1)}, u32[]{:S(2)}, u32[]{:S(2)}) collective-permute-start(bf16[4096,128]{1,0:T(8,128)(2,1)} %collective-permute-done.3.refs_2_), channel_id=1, source_target_pairs={{0,1},{1,0},{2,3},{3,2},{4,5},{5,4},{6,7},{7,6},{8,9},{9,8},{10,11... | collective-permute-start | bytes 3145736 | tf_op jit(solution)/shard_map/ppermute | solution.py:165
  112.2 1.9 collective-permute-start.6
  114.2 1.9 collective-permute-start.7
  116.2 37.7 %all-gather.2 = bf16[384,1024]{1,0:T(8,128)(2,1)S(1)} all-gather(bf16[96,1024]{1,0:T(8,128)(2,1)S(1)} %get-tuple-element.21), channel_id=4, replica_groups=mesh['z'=12,'x'=4,'q'=4,'p'=2,'c'=2] {'q'}, dimensions={0}, use_global_device_ids=true | all-gather | bytes 983040 | tf_op jit(solution)/shard_map/all_gather | solution.py:197
  153.9 1.2 copy-done.3
  155.2 1.2 copy-done.5
  156.4 4.3 %hidden.1 = bf16[192,512]{1,0:T(8,128)(2,1)S(1)} custom-call(s32[2]{0:T(128)S(1)} %pad_add_fusion.where_ref, bf16[4,104,1024]{2,1,0:T(8,128)(2,1)S(1)} %bitcast.18, bf16[4,96,1024]{2,1,0:T(8,128)(2,1)S(1)} %bitcast.19, bf16[4096,128]{1,0:T(8,128)(2,1)S(1)} %bitcast.26, bf16[4096,128]{1,0:T(8,128)(2,1)S(1)} %copy-done.3, ...), custom_call_target="tpu_custom_call" | custom-call | flops 2147483648 | bytes 1048576 | tf_op jit(solution)/shard_map/hidden/pallas_call | solution.py:200
  160.7 4.9 %collective-permute-start.8 = (bf16[2048,256]{1,0:T(8,128)(2,1)}, bf16[2048,256]{1,0:T(8,128)(2,1)S(1)}, u32[]{:S(2)}, u32[]{:S(2)}) collective-permute-start(bf16[2048,256]{1,0:T(8,128)(2,1)} %collective-permute-done.7.refs_2_), channel_id=1, source_target_pairs={{0,1},{1,0},{2,3},{3,2},{4,5},{5,4},{6,7},{7,6},{8,9},{9,8},{10,11... | collective-permute-start | bytes 3145736 | tf_op jit(solution)/shard_map/ppermute | solution.py:165
  165.6 15.4 %all-gather.3 = bf16[768,512]{1,0:T(8,128)(2,1)S(1)} all-gather(bf16[192,512]{1,0:T(8,128)(2,1)S(1)} %hidden.1), channel_id=5, replica_groups=mesh['z'=12,'x'=4,'q'=4,'p'=2,'c'=2] {'q'}, dimensions={0}, use_global_device_ids=true | all-gather | bytes 983040 | tf_op jit(solution)/shard_map/all_gather | solution.py:210
  181.1 2.2 down.1
  183.3 39.3 %all_to_all.10 = bf16[192,8,128]{2,1,0:T(8,128)(2,1)S(1)} all-to-all(bf16[192,8,128]{2,1,0:T(8,128)(2,1)S(1)} %bitcast.23), channel_id=1, replica_groups=mesh['z'=12,'x'=4,'q'=4,'p'=2,'c'=2] {'z','x','p','c'}, dimensions={0} | all-to-all | bytes 786432 | tf_op jit(solution)/shard_map/all_to_all | solution.py:220
  223.3 2.3 %combine.1 = bf16[256,256]{1,0:T(8,128)(2,1)} custom-call(s32[2,256]{1,0:T(2,128)S(1)} %bitcast.35, f32[2,256]{1,0:T(2,128)S(1)} %bitcast.36, bf16[1536,128]{1,0:T(8,128)(2,1)S(1)} %bitcast.22), custom_call_target="tpu_custom_call" | custom-call | bytes 1048576 | tf_op jit(solution)/shard_map/combine/pallas_call | solution.py:222
  (32 shorter events, 0.9 us)
Async XLA Ops:
  0.0 24.7 %copy-start = (bf16[1,4096,128]{2,1,0:T(8,128)(2,1)S(1)}, bf16[1,4096,128]{2,1,0:T(8,128)(2,1)}, u32[]{:S(2)}) copy-start(bf16[1,4096,128]{2,1,0:T(8,128)(2,1)} %param.11) | copy-start | bytes 3145732
  2.5 84.8 %all-to-all-start = ((bf16[192,8,128]{2,1,0:T(8,128)(2,1)}), bf16[192,8,128]{2,1,0:T(8,128)(2,1)S(1)}, u32[]{:S(2)}, u32[]{:S(2)}) async-start(bf16[192,8,128]{2,1,0:T(8,128)(2,1)} %bitcast.37), calls=%async_computation | async-start | bytes 786432 | tf_op jit(solution)/shard_map/all_to_all | solution.py:175
  24.7 59.7 %collective-permute-start = (bf16[4096,128]{1,0:T(8,128)(2,1)S(1)}, bf16[4096,128]{1,0:T(8,128)(2,1)S(1)}, u32[]{:S(2)}, u32[]{:S(2)}) collective-permute-start(bf16[4096,128]{1,0:T(8,128)(2,1)S(1)} %bitcast.24), channel_id=1, source_target_pairs={{0,1},{1,0},{2,3},{3,2},{4,5},{5,4},{6,7},{7,6},{8,9},{9,8},{10,11... | collective-permute-start | bytes 3145736 | tf_op jit(solution)/shard_map/ppermute | solution.py:165
  27.9 57.4 %collective-permute-start.1 = (bf16[4096,128]{1,0:T(8,128)(2,1)}, bf16[4096,128]{1,0:T(8,128)(2,1)S(1)}, u32[]{:S(2)}, u32[]{:S(2)}) collective-permute-start(bf16[4096,128]{1,0:T(8,128)(2,1)} %bitcast.27), channel_id=1, source_target_pairs={{0,1},{1,0},{2,3},{3,2},{4,5},{5,4},{6,7},{7,6},{8,9},{9,8},{10,11... | collective-permute-start | bytes 3145736 | tf_op jit(solution)/shard_map/ppermute | solution.py:165
  29.8 7.7 %copy-start.11 = (f32[256]{0:T(256)S(1)}, f32[256]{0:T(256)}, u32[]{:S(2)}) copy-start(f32[256]{0:T(256)} %param.8) | copy-start | bytes 3076
  29.9 56.4 %collective-permute-start.2 = (bf16[2048,256]{1,0:T(8,128)(2,1)}, bf16[2048,256]{1,0:T(8,128)(2,1)S(1)}, u32[]{:S(2)}, u32[]{:S(2)}) collective-permute-start(bf16[2048,256]{1,0:T(8,128)(2,1)} %bitcast.30), channel_id=1, source_target_pairs={{0,1},{1,0},{2,3},{3,2},{4,5},{5,4},{6,7},{7,6},{8,9},{9,8},{10,11... | collective-permute-start | bytes 3145736 | tf_op jit(solution)/shard_map/ppermute | solution.py:165
  32.3 76.1 %collective-permute-start.3 = (bf16[4096,128]{1,0:T(8,128)(2,1)S(1)}, bf16[4096,128]{1,0:T(8,128)(2,1)}, u32[]{:S(2)}, u32[]{:S(2)}) collective-permute-start(bf16[4096,128]{1,0:T(8,128)(2,1)S(1)} %bitcast.25), channel_id=1, source_target_pairs={{0,2},{2,0},{1,3},{3,1},{4,6},{6,4},{5,7},{7,5},{8,10},{10,8},{9,1... | collective-permute-start | bytes 3145736 | tf_op jit(solution)/shard_map/ppermute | solution.py:165
  34.6 73.8 %collective-permute-start.4 = (bf16[4096,128]{1,0:T(8,128)(2,1)}, bf16[4096,128]{1,0:T(8,128)(2,1)}, u32[]{:S(2)}, u32[]{:S(2)}) collective-permute-start(bf16[4096,128]{1,0:T(8,128)(2,1)} %bitcast.28), channel_id=1, source_target_pairs={{0,2},{2,0},{1,3},{3,1},{4,6},{6,4},{5,7},{7,5},{8,10},{10,8},{9,1... | collective-permute-start | bytes 3145736 | tf_op jit(solution)/shard_map/ppermute | solution.py:165
  84.3 1.0 copy-start.2
  85.3 1.0 copy-start.4
  86.3 1.0 copy-start.7
  87.4 66.5 %copy-start.1 = (bf16[1,4096,128]{2,1,0:T(8,128)(2,1)S(1)}, bf16[1,4096,128]{2,1,0:T(8,128)(2,1)}, u32[]{:S(2)}) copy-start(bf16[1,4096,128]{2,1,0:T(8,128)(2,1)} %param.12) | copy-start | bytes 3145732
  108.4 45.6 %collective-permute-start.5 = (bf16[4096,128]{1,0:T(8,128)(2,1)}, bf16[4096,128]{1,0:T(8,128)(2,1)}, u32[]{:S(2)}, u32[]{:S(2)}) collective-permute-start(bf16[4096,128]{1,0:T(8,128)(2,1)} %collective-permute-done.3.refs_2_), channel_id=1, source_target_pairs={{0,1},{1,0},{2,3},{3,2},{4,5},{5,4},{6,7},{7,6},{8,9},{9,8},{10,11... | collective-permute-start | bytes 3145736 | tf_op jit(solution)/shard_map/ppermute | solution.py:165
  112.2 41.7 %collective-permute-start.6 = (bf16[4096,128]{1,0:T(8,128)(2,1)}, bf16[4096,128]{1,0:T(8,128)(2,1)}, u32[]{:S(2)}, u32[]{:S(2)}) collective-permute-start(bf16[4096,128]{1,0:T(8,128)(2,1)} %collective-permute-done.4.refs_6_), channel_id=1, source_target_pairs={{0,1},{1,0},{2,3},{3,2},{4,5},{5,4},{6,7},{7,6},{8,9},{9,8},{10,11... | collective-permute-start | bytes 3145736 | tf_op jit(solution)/shard_map/ppermute | solution.py:165
  114.2 46.5 %collective-permute-start.7 = (bf16[2048,256]{1,0:T(8,128)(2,1)}, bf16[2048,256]{1,0:T(8,128)(2,1)}, u32[]{:S(2)}, u32[]{:S(2)}) collective-permute-start(bf16[2048,256]{1,0:T(8,128)(2,1)} %bitcast.31), channel_id=1, source_target_pairs={{0,2},{2,0},{1,3},{3,1},{4,6},{6,4},{5,7},{7,5},{8,10},{10,8},{9,1... | collective-permute-start | bytes 3145736 | tf_op jit(solution)/shard_map/ppermute | solution.py:165
  153.9 1.2 copy-start.3
  155.2 1.2 copy-start.5
  156.4 24.7 %copy-start.6 = (bf16[1,2048,256]{2,1,0:T(8,128)(2,1)S(1)}, bf16[1,2048,256]{2,1,0:T(8,128)(2,1)}, u32[]{:S(2)}) copy-start(bf16[1,2048,256]{2,1,0:T(8,128)(2,1)} %param.13) | copy-start | bytes 3145732
  156.4 24.7 %copy-start.8 = (bf16[2048,256]{1,0:T(8,128)(2,1)S(1)}, bf16[2048,256]{1,0:T(8,128)(2,1)}, u32[]{:S(2)}) copy-start(bf16[2048,256]{1,0:T(8,128)(2,1)} %copy-done.7) | copy-start | bytes 3145732
  160.7 20.4 %collective-permute-start.8 = (bf16[2048,256]{1,0:T(8,128)(2,1)}, bf16[2048,256]{1,0:T(8,128)(2,1)S(1)}, u32[]{:S(2)}, u32[]{:S(2)}) collective-permute-start(bf16[2048,256]{1,0:T(8,128)(2,1)} %collective-permute-done.7.refs_2_), channel_id=1, source_target_pairs={{0,1},{1,0},{2,3},{3,2},{4,5},{5,4},{6,7},{7,6},{8,9},{9,8},{10,11... | collective-permute-start | bytes 3145736 | tf_op jit(solution)/shard_map/ppermute | solution.py:165
  183.3 39.3 %copy-start.10 = (f32[256,2]{0,1:T(2,128)S(1)}, f32[256,2]{0,1:T(2,128)}, u32[]{:S(2)}) copy-start(f32[256,2]{0,1:T(2,128)} %param.10) | copy-start | bytes 6148
  222.7 0.7 copy-start.9

commit v5 on v1

--- a/solution.py
+++ b/solution.py
@@ -164,7 +164,7 @@
     half = experts * cap // 2
     where = jnp.stack([lax.axis_index("y"), lax.axis_index("c")]).astype(jnp.int32)
     ids = expert_ids.T
-    call = functools.partial(pl.pallas_call)
+    call = pl.pallas_call
 
     outgoing = call(
         functools.partial(dispatch_kernel, experts, cap),
@@ -177,16 +177,20 @@
     came = lax.all_to_all(outgoing.reshape(2 * experts, 8, width), ("z", "x", "c"), 0, 0, tiled=True)
 
     gain = norm_gain[None, :]
+    gate, up, down = gate_weight[0], up_weight[0], down_weight[0]
+    came, gain2, gate2, up2, down2 = lax.optimization_barrier(
+        (came, swap(gain), swap(gate), swap(up), swap(down))
+    )
     block = call(
         pack_kernel,
         out_shape=jax.ShapeDtypeStruct((half + PAD, 2 * width), BF),
         in_specs=[SM, VM, VM, VM],
         out_specs=VM,
+        compiler_params=pltpu.CompilerParams(vmem_limit_bytes=8 << 20),
         name="pack",
-    )(where, came, gain, swap(gain))
+    )(where, came, gain, gain2)
     found = ring(block, count)
 
-    gate, up, down = gate_weight[0], up_weight[0], down_weight[0]
     ff = gate.shape[1]
     hidden = call(
         functools.partial(hidden_kernel, count),
@@ -198,9 +202,9 @@
             pltpu.VMEM((half, 2 * ff), F32),
             pltpu.VMEM((half, 128), F32),
         ],
-        compiler_params=pltpu.CompilerParams(vmem_limit_bytes=40 << 20),
+        compiler_params=pltpu.CompilerParams(vmem_limit_bytes=12 << 20),
         name="hidden",
-    )(where, *found, gate, swap(gate), up, swap(up))
+    )(where, *found, gate, gate2, up, up2)
     found = ring(hidden, count)
 
     made = call(
@@ -209,9 +213,9 @@
         in_specs=[SM] + [VM] * 10,
         out_specs=VM,
         scratch_shapes=[pltpu.VMEM((half, width), F32), pltpu.VMEM((half, width), F32)],
-        compiler_params=pltpu.CompilerParams(vmem_limit_bytes=40 << 20),
+        compiler_params=pltpu.CompilerParams(vmem_limit_bytes=12 << 20),
         name="down",
-    )(where, *found, down, swap(down))
+    )(where, *found, down, down2)
     back = lax.all_to_all(made.reshape(2 * experts, 8, width), ("z", "x", "c"), 0, 0, tiled=True)
 
     return call(
@@ -219,6 +223,7 @@
         out_shape=jax.ShapeDtypeStruct((rows, width), BF),
         in_specs=[VM, VM, VM],
         out_specs=VM,
+        compiler_params=pltpu.CompilerParams(vmem_limit_bytes=8 << 20),
         name="combine",
     )(ids, expert_weights.T, back.reshape(experts * cap, width))
 

time: 172 us -> 173 us (level)
  blocking collectives: 31.4 us -> 42.4 us
  waiting for transfers between devices: 41.1 us -> 36.6 us
  starting transfers between devices: 84 us -> 80.8 us
    all_to_all x1, blocking collectives: 31.4 us -> 42.4 us  [body(): lax.all_to_all(made.reshape(2 * experts, 8, width), ('z', 'x', 'c'), 0, 0...]
    ppermute x6, starting transfers between devices: 20.7 us -> 11.7 us  [ring(): other = lax.ppermute(other, ('y', 'c'), perm(-1))]
    ppermute x2, waiting for transfers between devices: 10.6 us -> 3.35 us  [ring(): found.append(lax.ppermute(main, ('y', 'c'), perm(1)))]
    all_to_all x1, waiting for transfers between devices: 17.9 us -> 11.3 us  [body(): lax.all_to_all(outgoing.reshape(2 * experts, 8, width), ('z', 'x', 'c'),...]
    ppermute x6, waiting for transfers between devices: 6.39 us -> 12.9 us  [ring(): other = lax.ppermute(other, ('y', 'c'), perm(-1))]
    ppermute x6, starting transfers between devices: 25.8 us -> 30.9 us  [ring(): main = lax.ppermute(main, ('y', 'c'), perm(1))]
    ppermute x2, starting transfers between devices: 5.88 us -> 9.28 us  [ring(): found.append(lax.ppermute(main, ('y', 'c'), perm(1)))]
    ppermute x4, starting transfers between devices: 11.6 us -> 8.84 us  [swap(): return lax.ppermute(value, 'c', [(0, 1), (1, 0)])]
  transfers between devices with their start and end apart: 19 -> 19, of which waited for: 12 -> 14; matrix products, arithmetic and copies ran while one was open for 0% -> 0% of each run, Pallas kernels for 2% -> 0%
where the time goes in v5:
time: 173 us; the launch traced here: 171 us
  starting transfers between devices  80.8 us (47%)
  blocking collectives  42.4 us (25%)
  waiting for transfers between devices  36.6 us (21%)
  Pallas kernels  9.53 us (6%)
    all_to_all x1, blocking collectives, body(): lax.all_to_all(made.reshape(2 * experts, 8, width), ('z', 'x', 'c'), 0, 0...  42.4 us
    ppermute x6, starting transfers between devices, ring(): main = lax.ppermute(main, ('y', 'c'), perm(1))  30.9 us
    all_to_all x1, starting transfers between devices, body(): lax.all_to_all(outgoing.reshape(2 * experts, 8, width), ('z', 'x', 'c'),...  20 us
    ppermute x6, waiting for transfers between devices, ring(): other = lax.ppermute(other, ('y', 'c'), perm(-1))  12.9 us
    ppermute x6, starting transfers between devices, ring(): other = lax.ppermute(other, ('y', 'c'), perm(-1))  11.7 us
    all_to_all x1, waiting for transfers between devices, body(): lax.all_to_all(outgoing.reshape(2 * experts, 8, width), ('z', 'x', 'c'),...  11.3 us
    ppermute x2, starting transfers between devices, ring(): found.append(lax.ppermute(main, ('y', 'c'), perm(1)))  9.28 us
    ppermute x4, starting transfers between devices, swap(): return lax.ppermute(value, 'c', [(0, 1), (1, 0)])  8.84 us
  transfers between devices with their start and end apart: 19, of which 14 were waited for; matrix products, arithmetic and copies ran while one was open for 0% of the time, Pallas kernels for 0%

profile of v5, /device:TPU:1, one launch (start us, length us, event | category | flops | bytes accessed | tf_op | source)
XLA Modules:
  0.0 170.9 jit_solution(4130327079528927740)
XLA Ops:
  0.0 2.2 %dispatch.1 = bf16[768,256]{1,0:T(8,128)(2,1)} custom-call(s32[2,256]{1,0:T(2,128)} %bitcast.19, bf16[256,256]{1,0:T(8,128)(2,1)} %tok_ref.1), custom_call_target="tpu_custom_call" | custom-call | tf_op jit(solution)/shard_map/dispatch/pallas_call | solution.py:169
  2.2 20.0 %all-to-all-start = ((bf16[96,8,256]{2,1,0:T(8,128)(2,1)}), bf16[96,8,256]{2,1,0:T(8,128)(2,1)S(1)}, u32[]{:S(2)}, u32[]{:S(2)}) async-start(bf16[96,8,256]{2,1,0:T(8,128)(2,1)} %bitcast.24), calls=%async_computation | async-start | bytes 786432 | tf_op jit(solution)/shard_map/all_to_all | solution.py:177
  22.3 2.6 %collective-permute-start.1 = (bf16[4096,128]{1,0:T(8,128)(2,1)S(1)}, bf16[4096,128]{1,0:T(8,128)(2,1)}, u32[]{:S(2)}, u32[]{:S(2)}) collective-permute-start(bf16[4096,128]{1,0:T(8,128)(2,1)S(1)} %bitcast.13), channel_id=1, source_target_pairs={{0,1},{1,0},{2,3},{3,2},{4,5},{5,4},{6,7},{7,6},{8,9},{9,8},{10,11... | collective-permute-start | bytes 3145736 | tf_op jit(solution)/shard_map/ppermute | solution.py:156
  24.9 1.9 %collective-permute-start.2 = (bf16[4096,128]{1,0:T(8,128)(2,1)}, bf16[4096,128]{1,0:T(8,128)(2,1)}, u32[]{:S(2)}, u32[]{:S(2)}) collective-permute-start(bf16[4096,128]{1,0:T(8,128)(2,1)} %bitcast.15), channel_id=1, source_target_pairs={{0,1},{1,0},{2,3},{3,2},{4,5},{5,4},{6,7},{7,6},{8,9},{9,8},{10,11... | collective-permute-start | bytes 3145736 | tf_op jit(solution)/shard_map/ppermute | solution.py:156
  26.8 2.4 %collective-permute-start.3 = (bf16[2048,256]{1,0:T(8,128)(2,1)}, bf16[2048,256]{1,0:T(8,128)(2,1)S(1)}, u32[]{:S(2)}, u32[]{:S(2)}) collective-permute-start(bf16[2048,256]{1,0:T(8,128)(2,1)} %bitcast.17), channel_id=1, source_target_pairs={{0,1},{1,0},{2,3},{3,2},{4,5},{5,4},{6,7},{7,6},{8,9},{9,8},{10,11... | collective-permute-start | bytes 3145736 | tf_op jit(solution)/shard_map/ppermute | solution.py:156
  29.2 1.9 %collective-permute-start = (f32[1,256]{1,0:T(1,128)}, f32[1,256]{1,0:T(1,128)S(1)}, u32[]{:S(2)}, u32[]{:S(2)}) collective-permute-start(f32[1,256]{1,0:T(1,128)} %bitcast.22), channel_id=1, source_target_pairs={{0,1},{1,0},{2,3},{3,2},{4,5},{5,4},{6,7},{7,6},{8,9},{9,8},{10,11... | collective-permute-start | bytes 3080 | tf_op jit(solution)/shard_map/ppermute | solution.py:156
  32.5 11.3 %all-to-all-done.came_ref = bf16[96,8,256]{2,1,0:T(8,128)(2,1)S(1)} async-done(((bf16[96,8,256]{2,1,0:T(8,128)(2,1)}), bf16[96,8,256]{2,1,0:T(8,128)(2,1)S(1)}, u32[]{:S(2)}, u32[]{:S(2)}) %all-to-all-start) | async-done | bytes 393248 | tf_op jit(solution)/shard_map/all_to_all | solution.py:177
  45.0 5.2 %collective-permute-start.4 = (bf16[392,512]{1,0:T(8,128)(2,1)S(1)}, bf16[392,512]{1,0:T(8,128)(2,1)S(1)}, u32[]{:S(2)}, u32[]{:S(2)}) collective-permute-start(bf16[392,512]{1,0:T(8,128)(2,1)S(1)} %pack.1.refs_0_), channel_id=1, source_target_pairs={{0,2},{1,15},{2,4},{3,1},{4,6},{5,3},{6,8},{7,5},{8,10},{9,7},{10,... | collective-permute-start | bytes 1204232 | tf_op jit(solution)/shard_map/ppermute | solution.py:148
  50.3 1.9 %collective-permute-start.5 = (bf16[392,512]{1,0:T(8,128)(2,1)S(1)}, bf16[392,512]{1,0:T(8,128)(2,1)S(1)}, u32[]{:S(2)}, u32[]{:S(2)}) collective-permute-start(bf16[392,512]{1,0:T(8,128)(2,1)S(1)} %pack.1.refs_0_), channel_id=1, source_target_pairs={{0,14},{1,3},{2,0},{3,5},{4,2},{5,7},{6,4},{7,9},{8,6},{9,11},{10,... | collective-permute-start | bytes 1204232 | tf_op jit(solution)/shard_map/ppermute | solution.py:149
  52.2 3.3 %collective-permute-done.4.refs_1_ = bf16[392,512]{1,0:T(8,128)(2,1)S(1)} collective-permute-done((bf16[392,512]{1,0:T(8,128)(2,1)S(1)}, bf16[392,512]{1,0:T(8,128)(2,1)S(1)}, u32[]{:S(2)}, u32[]{:S(2)}) %collective-permute-start.4) | collective-permute-done | bytes 401440 | tf_op jit(solution)/shard_map/ppermute | solution.py:148
  55.5 5.3 %collective-permute-start.6 = (bf16[392,512]{1,0:T(8,128)(2,1)S(1)}, bf16[392,512]{1,0:T(8,128)(2,1)S(1)}, u32[]{:S(2)}, u32[]{:S(2)}) collective-permute-start(bf16[392,512]{1,0:T(8,128)(2,1)S(1)} %collective-permute-done.4.refs_1_), channel_id=1, source_target_pairs={{0,2},{1,15},{2,4},{3,1},{4,6},{5,3},{6,8},{7,5},{8,10},{9,7},{10,... | collective-permute-start | bytes 1204232 | tf_op jit(solution)/shard_map/ppermute | solution.py:148
  61.5 2.0 %collective-permute-start.7 = (bf16[392,512]{1,0:T(8,128)(2,1)S(1)}, bf16[392,512]{1,0:T(8,128)(2,1)S(1)}, u32[]{:S(2)}, u32[]{:S(2)}) collective-permute-start(bf16[392,512]{1,0:T(8,128)(2,1)S(1)} %collective-permute-done.5.refs_2_), channel_id=1, source_target_pairs={{0,14},{1,3},{2,0},{3,5},{4,2},{5,7},{6,4},{7,9},{8,6},{9,11},{10,... | collective-permute-start | bytes 1204232 | tf_op jit(solution)/shard_map/ppermute | solution.py:149
  63.5 2.1 %collective-permute-done.6.refs_3_ = bf16[392,512]{1,0:T(8,128)(2,1)S(1)} collective-permute-done((bf16[392,512]{1,0:T(8,128)(2,1)S(1)}, bf16[392,512]{1,0:T(8,128)(2,1)S(1)}, u32[]{:S(2)}, u32[]{:S(2)}) %collective-permute-start.6) | collective-permute-done | bytes 401440 | tf_op jit(solution)/shard_map/ppermute | solution.py:148
  65.6 5.0 %collective-permute-start.8 = (bf16[392,512]{1,0:T(8,128)(2,1)S(1)}, bf16[392,512]{1,0:T(8,128)(2,1)S(1)}, u32[]{:S(2)}, u32[]{:S(2)}) collective-permute-start(bf16[392,512]{1,0:T(8,128)(2,1)S(1)} %collective-permute-done.6.refs_3_), channel_id=1, source_target_pairs={{0,2},{1,15},{2,4},{3,1},{4,6},{5,3},{6,8},{7,5},{8,10},{9,7},{10,... | collective-permute-start | bytes 1204232 | tf_op jit(solution)/shard_map/ppermute | solution.py:148
  70.6 3.9 %collective-permute-done.7.refs_4_ = bf16[392,512]{1,0:T(8,128)(2,1)S(1)} collective-permute-done((bf16[392,512]{1,0:T(8,128)(2,1)S(1)}, bf16[392,512]{1,0:T(8,128)(2,1)S(1)}, u32[]{:S(2)}, u32[]{:S(2)}) %collective-permute-start.7) | collective-permute-done | bytes 401440 | tf_op jit(solution)/shard_map/ppermute | solution.py:149
  74.5 2.0 %collective-permute-start.9 = (bf16[392,512]{1,0:T(8,128)(2,1)S(1)}, bf16[392,512]{1,0:T(8,128)(2,1)S(1)}, u32[]{:S(2)}, u32[]{:S(2)}) collective-permute-start(bf16[392,512]{1,0:T(8,128)(2,1)S(1)} %collective-permute-done.7.refs_4_), channel_id=1, source_target_pairs={{0,14},{1,3},{2,0},{3,5},{4,2},{5,7},{6,4},{7,9},{8,6},{9,11},{10,... | collective-permute-start | bytes 1204232 | tf_op jit(solution)/shard_map/ppermute | solution.py:149
  77.0 4.3 %collective-permute-start.10 = (bf16[392,512]{1,0:T(8,128)(2,1)S(1)}, bf16[392,512]{1,0:T(8,128)(2,1)S(1)}, u32[]{:S(2)}, u32[]{:S(2)}) collective-permute-start(bf16[392,512]{1,0:T(8,128)(2,1)S(1)} %collective-permute-done.8.refs_5_), channel_id=1, source_target_pairs={{0,2},{1,15},{2,4},{3,1},{4,6},{5,3},{6,8},{7,5},{8,10},{9,7},{10,... | collective-permute-start | bytes 1204232 | tf_op jit(solution)/shard_map/ppermute | solution.py:151
  81.3 7.6 %collective-permute-done.9.refs_6_ = bf16[392,512]{1,0:T(8,128)(2,1)S(1)} collective-permute-done((bf16[392,512]{1,0:T(8,128)(2,1)S(1)}, bf16[392,512]{1,0:T(8,128)(2,1)S(1)}, u32[]{:S(2)}, u32[]{:S(2)}) %collective-permute-start.9) | collective-permute-done | bytes 401440 | tf_op jit(solution)/shard_map/ppermute | solution.py:149
  90.3 3.5 %hidden.1.refs_0_ = bf16[384,256]{1,0:T(8,128)(2,1)S(1)} custom-call(s32[2]{0:T(128)S(1)} %pad_add_fusion.where_ref, bf16[392,512]{1,0:T(8,128)(2,1)S(1)} %pack.1.refs_0_, bf16[392,512]{1,0:T(8,128)(2,1)S(1)} %collective-permute-done.4.refs_1_, bf16[392,512]{1,0:T(8,128)(2,1)S(1)} %collective-permute-done.5.refs_2_, ...), custom_call_target="tpu_custom_call" | custom-call | tf_op jit(solution)/shard_map/hidden/pallas_call | solution.py:195
  93.9 5.3 %collective-permute-start.11 = (bf16[384,256]{1,0:T(8,128)(2,1)S(1)}, bf16[384,256]{1,0:T(8,128)(2,1)S(1)}, u32[]{:S(2)}, u32[]{:S(2)}) collective-permute-start(bf16[384,256]{1,0:T(8,128)(2,1)S(1)} %hidden.1.refs_0_), channel_id=1, source_target_pairs={{0,2},{1,15},{2,4},{3,1},{4,6},{5,3},{6,8},{7,5},{8,10},{9,7},{10,... | collective-permute-start | bytes 589832 | tf_op jit(solution)/shard_map/ppermute | solution.py:148
  101.8 5.0 %collective-permute-start.13 = (bf16[384,256]{1,0:T(8,128)(2,1)S(1)}, bf16[384,256]{1,0:T(8,128)(2,1)S(1)}, u32[]{:S(2)}, u32[]{:S(2)}) collective-permute-start(bf16[384,256]{1,0:T(8,128)(2,1)S(1)} %collective-permute-done.11.refs_1_), channel_id=1, source_target_pairs={{0,2},{1,15},{2,4},{3,1},{4,6},{5,3},{6,8},{7,5},{8,10},{9,7},{10,... | collective-permute-start | bytes 589832 | tf_op jit(solution)/shard_map/ppermute | solution.py:148
  109.4 5.0 %collective-permute-start.15 = (bf16[384,256]{1,0:T(8,128)(2,1)S(1)}, bf16[384,256]{1,0:T(8,128)(2,1)S(1)}, u32[]{:S(2)}, u32[]{:S(2)}) collective-permute-start(bf16[384,256]{1,0:T(8,128)(2,1)S(1)} %collective-permute-done.13.refs_3_), channel_id=1, source_target_pairs={{0,2},{1,15},{2,4},{3,1},{4,6},{5,3},{6,8},{7,5},{8,10},{9,7},{10,... | collective-permute-start | bytes 589832 | tf_op jit(solution)/shard_map/ppermute | solution.py:148
  117.0 5.0 %collective-permute-start.17 = (bf16[384,256]{1,0:T(8,128)(2,1)S(1)}, bf16[384,256]{1,0:T(8,128)(2,1)S(1)}, u32[]{:S(2)}, u32[]{:S(2)}) collective-permute-start(bf16[384,256]{1,0:T(8,128)(2,1)S(1)} %collective-permute-done.15.refs_5_), channel_id=1, source_target_pairs={{0,2},{1,15},{2,4},{3,1},{4,6},{5,3},{6,8},{7,5},{8,10},{9,7},{10,... | collective-permute-start | bytes 589832 | tf_op jit(solution)/shard_map/ppermute | solution.py:151
  126.2 42.4 %all_to_all.10 = bf16[96,8,256]{2,1,0:T(8,128)(2,1)S(1)} all-to-all(bf16[96,8,256]{2,1,0:T(8,128)(2,1)S(1)} %bitcast.11), channel_id=1, replica_groups=mesh['z'=12,'x'=4,'y'=8,'c'=2] {'z','x','c'}, dimensions={0} | all-to-all | bytes 786432 | tf_op jit(solution)/shard_map/all_to_all | solution.py:219
  (33 shorter events, 19.5 us)
Async XLA Ops:
  0.0 22.3 %copy-start = (bf16[1,4096,128]{2,1,0:T(8,128)(2,1)S(1)}, bf16[1,4096,128]{2,1,0:T(8,128)(2,1)}, u32[]{:S(2)}) copy-start(bf16[1,4096,128]{2,1,0:T(8,128)(2,1)} %param.11) | copy-start | bytes 3145732
  0.0 90.3 %copy-start.1 = (bf16[1,4096,128]{2,1,0:T(8,128)(2,1)S(1)}, bf16[1,4096,128]{2,1,0:T(8,128)(2,1)}, u32[]{:S(2)}) copy-start(bf16[1,4096,128]{2,1,0:T(8,128)(2,1)} %param.12) | copy-start | bytes 3145732
  2.2 41.5 %all-to-all-start = ((bf16[96,8,256]{2,1,0:T(8,128)(2,1)}), bf16[96,8,256]{2,1,0:T(8,128)(2,1)S(1)}, u32[]{:S(2)}, u32[]{:S(2)}) async-start(bf16[96,8,256]{2,1,0:T(8,128)(2,1)} %bitcast.24), calls=%async_computation | async-start | bytes 786432 | tf_op jit(solution)/shard_map/all_to_all | solution.py:177
  22.3 10.2 %collective-permute-start.1 = (bf16[4096,128]{1,0:T(8,128)(2,1)S(1)}, bf16[4096,128]{1,0:T(8,128)(2,1)}, u32[]{:S(2)}, u32[]{:S(2)}) collective-permute-start(bf16[4096,128]{1,0:T(8,128)(2,1)S(1)} %bitcast.13), channel_id=1, source_target_pairs={{0,1},{1,0},{2,3},{3,2},{4,5},{5,4},{6,7},{7,6},{8,9},{9,8},{10,11... | collective-permute-start | bytes 3145736 | tf_op jit(solution)/shard_map/ppermute | solution.py:156
  24.9 7.6 %collective-permute-start.2 = (bf16[4096,128]{1,0:T(8,128)(2,1)}, bf16[4096,128]{1,0:T(8,128)(2,1)}, u32[]{:S(2)}, u32[]{:S(2)}) collective-permute-start(bf16[4096,128]{1,0:T(8,128)(2,1)} %bitcast.15), channel_id=1, source_target_pairs={{0,1},{1,0},{2,3},{3,2},{4,5},{5,4},{6,7},{7,6},{8,9},{9,8},{10,11... | collective-permute-start | bytes 3145736 | tf_op jit(solution)/shard_map/ppermute | solution.py:156
  26.8 5.7 %collective-permute-start.3 = (bf16[2048,256]{1,0:T(8,128)(2,1)}, bf16[2048,256]{1,0:T(8,128)(2,1)S(1)}, u32[]{:S(2)}, u32[]{:S(2)}) collective-permute-start(bf16[2048,256]{1,0:T(8,128)(2,1)} %bitcast.17), channel_id=1, source_target_pairs={{0,1},{1,0},{2,3},{3,2},{4,5},{5,4},{6,7},{7,6},{8,9},{9,8},{10,11... | collective-permute-start | bytes 3145736 | tf_op jit(solution)/shard_map/ppermute | solution.py:156
  29.2 3.3 %collective-permute-start = (f32[1,256]{1,0:T(1,128)}, f32[1,256]{1,0:T(1,128)S(1)}, u32[]{:S(2)}, u32[]{:S(2)}) collective-permute-start(f32[1,256]{1,0:T(1,128)} %bitcast.22), channel_id=1, source_target_pairs={{0,1},{1,0},{2,3},{3,2},{4,5},{5,4},{6,7},{7,6},{8,9},{9,8},{10,11... | collective-permute-start | bytes 3080 | tf_op jit(solution)/shard_map/ppermute | solution.py:156
  45.0 79.6 %copy-start.2 = (bf16[1,2048,256]{2,1,0:T(8,128)(2,1)S(1)}, bf16[1,2048,256]{2,1,0:T(8,128)(2,1)}, u32[]{:S(2)}) copy-start(bf16[1,2048,256]{2,1,0:T(8,128)(2,1)} %param.13) | copy-start | bytes 3145732
  45.0 10.4 %collective-permute-start.4 = (bf16[392,512]{1,0:T(8,128)(2,1)S(1)}, bf16[392,512]{1,0:T(8,128)(2,1)S(1)}, u32[]{:S(2)}, u32[]{:S(2)}) collective-permute-start(bf16[392,512]{1,0:T(8,128)(2,1)S(1)} %pack.1.refs_0_), channel_id=1, source_target_pairs={{0,2},{1,15},{2,4},{3,1},{4,6},{5,3},{6,8},{7,5},{8,10},{9,7},{10,... | collective-permute-start | bytes 1204232 | tf_op jit(solution)/shard_map/ppermute | solution.py:148
  50.3 11.2 %collective-permute-start.5 = (bf16[392,512]{1,0:T(8,128)(2,1)S(1)}, bf16[392,512]{1,0:T(8,128)(2,1)S(1)}, u32[]{:S(2)}, u32[]{:S(2)}) collective-permute-start(bf16[392,512]{1,0:T(8,128)(2,1)S(1)} %pack.1.refs_0_), channel_id=1, source_target_pairs={{0,14},{1,3},{2,0},{3,5},{4,2},{5,7},{6,4},{7,9},{8,6},{9,11},{10,... | collective-permute-start | bytes 1204232 | tf_op jit(solution)/shard_map/ppermute | solution.py:149
  55.5 10.1 %collective-permute-start.6 = (bf16[392,512]{1,0:T(8,128)(2,1)S(1)}, bf16[392,512]{1,0:T(8,128)(2,1)S(1)}, u32[]{:S(2)}, u32[]{:S(2)}) collective-permute-start(bf16[392,512]{1,0:T(8,128)(2,1)S(1)} %collective-permute-done.4.refs_1_), channel_id=1, source_target_pairs={{0,2},{1,15},{2,4},{3,1},{4,6},{5,3},{6,8},{7,5},{8,10},{9,7},{10,... | collective-permute-start | bytes 1204232 | tf_op jit(solution)/shard_map/ppermute | solution.py:148
  61.5 13.0 %collective-permute-start.7 = (bf16[392,512]{1,0:T(8,128)(2,1)S(1)}, bf16[392,512]{1,0:T(8,128)(2,1)S(1)}, u32[]{:S(2)}, u32[]{:S(2)}) collective-permute-start(bf16[392,512]{1,0:T(8,128)(2,1)S(1)} %collective-permute-done.5.refs_2_), channel_id=1, source_target_pairs={{0,14},{1,3},{2,0},{3,5},{4,2},{5,7},{6,4},{7,9},{8,6},{9,11},{10,... | collective-permute-start | bytes 1204232 | tf_op jit(solution)/shard_map/ppermute | solution.py:149
  65.6 11.4 %collective-permute-start.8 = (bf16[392,512]{1,0:T(8,128)(2,1)S(1)}, bf16[392,512]{1,0:T(8,128)(2,1)S(1)}, u32[]{:S(2)}, u32[]{:S(2)}) collective-permute-start(bf16[392,512]{1,0:T(8,128)(2,1)S(1)} %collective-permute-done.6.refs_3_), channel_id=1, source_target_pairs={{0,2},{1,15},{2,4},{3,1},{4,6},{5,3},{6,8},{7,5},{8,10},{9,7},{10,... | collective-permute-start | bytes 1204232 | tf_op jit(solution)/shard_map/ppermute | solution.py:148
  74.5 14.4 %collective-permute-start.9 = (bf16[392,512]{1,0:T(8,128)(2,1)S(1)}, bf16[392,512]{1,0:T(8,128)(2,1)S(1)}, u32[]{:S(2)}, u32[]{:S(2)}) collective-permute-start(bf16[392,512]{1,0:T(8,128)(2,1)S(1)} %collective-permute-done.7.refs_4_), channel_id=1, source_target_pairs={{0,14},{1,3},{2,0},{3,5},{4,2},{5,7},{6,4},{7,9},{8,6},{9,11},{10,... | collective-permute-start | bytes 1204232 | tf_op jit(solution)/shard_map/ppermute | solution.py:149
  77.0 13.3 %collective-permute-start.10 = (bf16[392,512]{1,0:T(8,128)(2,1)S(1)}, bf16[392,512]{1,0:T(8,128)(2,1)S(1)}, u32[]{:S(2)}, u32[]{:S(2)}) collective-permute-start(bf16[392,512]{1,0:T(8,128)(2,1)S(1)} %collective-permute-done.8.refs_5_), channel_id=1, source_target_pairs={{0,2},{1,15},{2,4},{3,1},{4,6},{5,3},{6,8},{7,5},{8,10},{9,7},{10,... | collective-permute-start | bytes 1204232 | tf_op jit(solution)/shard_map/ppermute | solution.py:151
  93.9 7.9 %collective-permute-start.11 = (bf16[384,256]{1,0:T(8,128)(2,1)S(1)}, bf16[384,256]{1,0:T(8,128)(2,1)S(1)}, u32[]{:S(2)}, u32[]{:S(2)}) collective-permute-start(bf16[384,256]{1,0:T(8,128)(2,1)S(1)} %hidden.1.refs_0_), channel_id=1, source_target_pairs={{0,2},{1,15},{2,4},{3,1},{4,6},{5,3},{6,8},{7,5},{8,10},{9,7},{10,... | collective-permute-start | bytes 589832 | tf_op jit(solution)/shard_map/ppermute | solution.py:148
  99.2 7.6 %collective-permute-start.12 = (bf16[384,256]{1,0:T(8,128)(2,1)S(1)}, bf16[384,256]{1,0:T(8,128)(2,1)S(1)}, u32[]{:S(2)}, u32[]{:S(2)}) collective-permute-start(bf16[384,256]{1,0:T(8,128)(2,1)S(1)} %hidden.1.refs_0_), channel_id=1, source_target_pairs={{0,14},{1,3},{2,0},{3,5},{4,2},{5,7},{6,4},{7,9},{8,6},{9,11},{10,... | collective-permute-start | bytes 589832 | tf_op jit(solution)/shard_map/ppermute | solution.py:149
  101.8 7.6 %collective-permute-start.13 = (bf16[384,256]{1,0:T(8,128)(2,1)S(1)}, bf16[384,256]{1,0:T(8,128)(2,1)S(1)}, u32[]{:S(2)}, u32[]{:S(2)}) collective-permute-start(bf16[384,256]{1,0:T(8,128)(2,1)S(1)} %collective-permute-done.11.refs_1_), channel_id=1, source_target_pairs={{0,2},{1,15},{2,4},{3,1},{4,6},{5,3},{6,8},{7,5},{8,10},{9,7},{10,... | collective-permute-start | bytes 589832 | tf_op jit(solution)/shard_map/ppermute | solution.py:148
  106.8 7.6 %collective-permute-start.14 = (bf16[384,256]{1,0:T(8,128)(2,1)S(1)}, bf16[384,256]{1,0:T(8,128)(2,1)S(1)}, u32[]{:S(2)}, u32[]{:S(2)}) collective-permute-start(bf16[384,256]{1,0:T(8,128)(2,1)S(1)} %collective-permute-done.12.refs_2_), channel_id=1, source_target_pairs={{0,14},{1,3},{2,0},{3,5},{4,2},{5,7},{6,4},{7,9},{8,6},{9,11},{10,... | collective-permute-start | bytes 589832 | tf_op jit(solution)/shard_map/ppermute | solution.py:149
  109.4 7.6 %collective-permute-start.15 = (bf16[384,256]{1,0:T(8,128)(2,1)S(1)}, bf16[384,256]{1,0:T(8,128)(2,1)S(1)}, u32[]{:S(2)}, u32[]{:S(2)}) collective-permute-start(bf16[384,256]{1,0:T(8,128)(2,1)S(1)} %collective-permute-done.13.refs_3_), channel_id=1, source_target_pairs={{0,2},{1,15},{2,4},{3,1},{4,6},{5,3},{6,8},{7,5},{8,10},{9,7},{10,... | collective-permute-start | bytes 589832 | tf_op jit(solution)/shard_map/ppermute | solution.py:148
  114.4 8.3 %collective-permute-start.16 = (bf16[384,256]{1,0:T(8,128)(2,1)S(1)}, bf16[384,256]{1,0:T(8,128)(2,1)S(1)}, u32[]{:S(2)}, u32[]{:S(2)}) collective-permute-start(bf16[384,256]{1,0:T(8,128)(2,1)S(1)} %collective-permute-done.14.refs_4_), channel_id=1, source_target_pairs={{0,14},{1,3},{2,0},{3,5},{4,2},{5,7},{6,4},{7,9},{8,6},{9,11},{10,... | collective-permute-start | bytes 589832 | tf_op jit(solution)/shard_map/ppermute | solution.py:149
  117.0 7.6 %collective-permute-start.17 = (bf16[384,256]{1,0:T(8,128)(2,1)S(1)}, bf16[384,256]{1,0:T(8,128)(2,1)S(1)}, u32[]{:S(2)}, u32[]{:S(2)}) collective-permute-start(bf16[384,256]{1,0:T(8,128)(2,1)S(1)} %collective-permute-done.15.refs_5_), channel_id=1, source_target_pairs={{0,2},{1,15},{2,4},{3,1},{4,6},{5,3},{6,8},{7,5},{8,10},{9,7},{10,... | collective-permute-start | bytes 589832 | tf_op jit(solution)/shard_map/ppermute | solution.py:151
  126.2 42.4 %copy-start.4 = (f32[256,2]{0,1:T(2,128)S(1)}, f32[256,2]{0,1:T(2,128)}, u32[]{:S(2)}) copy-start(f32[256,2]{0,1:T(2,128)} %param.10) | copy-start | bytes 6148
  168.6 0.7 copy-start.3
  (1 other events, 0.7 us)

commit v6 on v3

v6 whole, which is shorter than its diff:
```python
import functools

import jax
import jax.numpy as jnp
from jax import lax
from jax.experimental import pallas as pl
from jax.experimental.pallas import tpu as pltpu
from jax.sharding import Mesh, PartitionSpec as P

BF = jnp.bfloat16
F32 = jnp.float32
VM = pl.BlockSpec(memory_space=pltpu.VMEM)
STEPS = (0, 1, -1, 2, -2, 3, -3, 4)
PAD = 8


def dot(a, b):
    return jnp.dot(a, b, preferred_element_type=F32)


def dispatch_kernel(experts, cap, ids_ref, tok_ref, out_ref, pick_ref):
    rows = tok_ref.shape[0]
    expert = lax.broadcasted_iota(jnp.int32, (experts, rows), 0)
    named = (expert == ids_ref[0:1, :]) | (expert == ids_ref[1:2, :])
    before = lax.broadcasted_iota(jnp.int32, (rows, rows), 0) < lax.broadcasted_iota(
        jnp.int32, (rows, rows), 1
    )
    rank = dot(named.astype(F32).astype(BF), before.astype(F32).astype(BF))
    rank = jnp.where(named, rank, -1.0)
    slot = lax.broadcasted_iota(jnp.int32, (cap, rows), 0).astype(F32)
    for e in range(experts):
        pick_ref[e * cap : (e + 1) * cap, :] = (
            (rank[e : e + 1, :] == slot).astype(F32).astype(BF)
        )
    out_ref[...] = dot(pick_ref[...], tok_ref[...]).astype(BF)


def plan_kernel(experts, cap, ids_ref, weight_ref, pick_ref, share_ref):
    rows = pick_ref.shape[1]
    line = lax.broadcasted_iota(jnp.int32, (8, rows), 0)
    table = jnp.where(line == 0, ids_ref[0:1, :].astype(F32), 0.0)
    table = jnp.where(line == 1, ids_ref[1:2, :].astype(F32), table)
    table = jnp.where(line == 2, weight_ref[0:1, :], table)
    table = jnp.where(line == 3, weight_ref[1:2, :], table)
    column = table.T
    first, second = column[:, 0:1], column[:, 1:2]
    lanes = lax.broadcasted_iota(jnp.int32, (rows, 128), 1).astype(F32)
    named = (lanes == first) | (lanes == second)
    after = lax.broadcasted_iota(jnp.int32, (rows, rows), 1) < lax.broadcasted_iota(
        jnp.int32, (rows, rows), 0
    )
    rank = dot(after.astype(F32).astype(BF), named.astype(F32).astype(BF))
    place = lax.broadcasted_iota(jnp.int32, (rows, experts * cap), 1).astype(F32)
    for k, name in enumerate((first, second)):
        mine = jnp.sum(jnp.where(lanes == name, rank, 0.0), axis=1, keepdims=True)
        pick_ref[k] = (place == name * cap + mine).astype(F32).astype(BF)
        share_ref[k] = jnp.broadcast_to(column[:, 2 + k : 3 + k], (rows, 128))


def combine_kernel(pick_ref, share_ref, back_ref, out_ref):
    total = None
    for k in range(2):
        term = dot(pick_ref[k], back_ref[...]) * share_ref[k][:, :1]
        total = term if k == 0 else total + term
    out_ref[...] = total.astype(BF)


def pack_kernel(came_ref, gain_ref, out_ref):
    sources = came_ref.shape[0] // 2
    width = came_ref.shape[2]
    for s in range(sources):
        for c in range(2):
            out_ref[s * 8 : s * 8 + 8, c * width : (c + 1) * width] = came_ref[2 * s + c]
    gain = jnp.concatenate([gain_ref[0], gain_ref[1]], axis=1)
    top = gain.astype(BF).astype(F32)
    mid = (gain - top).astype(BF).astype(F32)
    low = gain - top - mid
    line = lax.broadcasted_iota(jnp.int32, (PAD, 2 * width), 0)
    split = jnp.where(line == 0, top, jnp.where(line == 1, mid, jnp.where(line == 2, low, 0.0)))
    out_ref[sources * 8 : sources * 8 + PAD, :] = split.astype(BF)


def source_of(step, count):
    turn = 1 - 2 * lax.axis_index("c")
    return lax.rem(lax.axis_index("y") - step * turn + 2 * count, count)


def take(refs, sizes):
    parts, at = [], 0
    for size in sizes:
        parts.append(refs[at : at + size])
        at += size
    return parts


def hidden_kernel(count, skip, inputs, last, *refs):
    kept = 3 if skip else 0
    blocks, weights, before, outs = take(refs, (inputs, 4, kept, len(refs) - inputs - 4 - kept))
    gate_ref, gate2_ref, up_ref, up2_ref = weights
    depth = blocks[0].shape[1]
    rows, half = blocks[0].shape[0] - PAD, gate_ref.shape[1]
    total = [ref[...] for ref in before] if skip else None
    for step, block in zip(STEPS[skip : skip + inputs], blocks):
        start = pl.multiple_of(source_of(step, count) * depth, depth)
        gain = jnp.sum(block[rows : rows + PAD, :].astype(F32), axis=0, keepdims=True)
        raw = block[0:rows, :].astype(F32)
        squares = raw * raw
        part = squares[:, 0:128]
        for lane in range(128, depth, 128):
            part = part + squares[:, lane : lane + 128]
        scaled = (raw * gain).astype(BF)
        gate = jnp.concatenate([gate_ref[pl.ds(start, depth), :], gate2_ref[pl.ds(start, depth), :]], axis=1)
        up = jnp.concatenate([up_ref[pl.ds(start, depth), :], up2_ref[pl.ds(start, depth), :]], axis=1)
        new = [dot(scaled, gate), dot(scaled, up), part]
        total = new if total is None else [t + n for t, n in zip(total, new)]
    if not last:
        for ref, value in zip(outs, total):
            ref[...] = value
        return
    mean = jnp.sum(total[2], axis=1, keepdims=True) / (depth * count)
    scale = lax.rsqrt(mean + 1e-06)
    gate, up = total[0] * scale, total[1] * scale
    hidden = (gate / (1.0 + jnp.exp(-gate)) * up).astype(BF)
    core = lax.axis_index("c")
    outs[0][:, pl.ds(pl.multiple_of(core * half, half), half)] = hidden[:, :half]
    outs[0][:, pl.ds(pl.multiple_of((1 - core) * half, half), half)] = hidden[:, half:]


def down_kernel(count, skip, inputs, last, *refs):
    kept = 2 if skip else 0
    blocks, weights, before, outs = take(refs, (inputs, 2, kept, len(refs) - inputs - 2 - kept))
    rows, depth = blocks[0].shape
    total = [ref[...] for ref in before] if skip else None
    for step, block in zip(STEPS[skip : skip + inputs], blocks):
        start = pl.multiple_of(source_of(step, count) * depth, depth)
        new = [dot(block[...], ref[pl.ds(start, depth), :]) for ref in weights]
        total = new if total is None else [t + n for t, n in zip(total, new)]
    if not last:
        for ref, value in zip(outs, total):
            ref[...] = value
        return
    core = lax.axis_index("c")
    for s in range(rows // 8):
        outs[0][s, core] = total[0][s * 8 : s * 8 + 8, :].astype(BF)
        outs[0][s, 1 - core] = total[1][s * 8 : s * 8 + 8, :].astype(BF)


def ring(block, count):
    def perm(sign):
        return [
            (y * 2 + c, (y + sign * (1 - 2 * c)) % count * 2 + c) for y in range(count) for c in range(2)
        ]

    main = other = block
    found = [block]
    for k in range(3):
        main = lax.ppermute(main, ("y", "c"), perm(1))
        other = lax.ppermute(other, ("y", "c"), perm(-1))
        found += [main, other]
    found.append(lax.ppermute(main, ("y", "c"), perm(1)))
    return found


def swap(value):
    return lax.ppermute(value, "c", [(0, 1), (1, 0)])


def body(tokens, norm_gain, expert_ids, expert_weights, gate_weight, up_weight, down_weight):
    count = lax.axis_size("y")
    experts = lax.axis_size("z") * lax.axis_size("x")
    rows, width = tokens.shape
    cap = 3 * rows * expert_ids.shape[1] // (2 * experts)
    half = experts * cap // 2
    ids = expert_ids.T
    call = pl.pallas_call

    outgoing = call(
        functools.partial(dispatch_kernel, experts, cap),
        out_shape=jax.ShapeDtypeStruct((experts * cap, width), BF),
        in_specs=[VM, VM],
        out_specs=VM,
        scratch_shapes=[pltpu.VMEM((experts * cap, rows), BF)],
        name="dispatch",
    )(ids, tokens)
    came = lax.all_to_all(outgoing.reshape(2 * experts, 8, width), ("z", "x", "c"), 0, 0, tiled=True)

    picks, shares = call(
        functools.partial(plan_kernel, experts, cap),
        out_shape=[
            jax.ShapeDtypeStruct((2, rows, experts * cap), BF),
            jax.ShapeDtypeStruct((2, rows, 128), F32),
        ],
        in_specs=[VM, VM],
        out_specs=[VM, VM],
        compiler_params=pltpu.CompilerParams(vmem_limit_bytes=8 << 20),
        cost_estimate=pl.CostEstimate(flops=1 << 30, bytes_accessed=1 << 20, transcendentals=0),
        name="plan",
    )(ids, expert_weights.T)
    gate, up, down = gate_weight[0], up_weight[0], down_weight[0]
    came, gains, gate2, up2, down2, picks, shares = lax.optimization_barrier(
        (came, lax.all_gather(norm_gain[None], "c", axis=0), swap(gate), swap(up), swap(down), picks, shares)
    )
    block = call(
        pack_kernel,
        out_shape=jax.ShapeDtypeStruct((half + PAD, 2 * width), BF),
        in_specs=[VM, VM],
        out_specs=VM,
        compiler_params=pltpu.CompilerParams(vmem_limit_bytes=8 << 20),
        name="pack",
    )(came, gains)

    def product(kernel, name, found, weights, sums, outs, each):
        total, skip = [], 0
        for group in (found,):
            last = skip + len(group) == count
            shapes = outs if last else sums
            total = call(
                functools.partial(kernel, count, skip, len(group), last),
                out_shape=shapes,
                in_specs=[VM] * (len(group) + len(weights) + len(total)),
                out_specs=[VM] * len(shapes),
                compiler_params=pltpu.CompilerParams(vmem_limit_bytes=16 << 20),
                cost_estimate=pl.CostEstimate(
                    flops=len(group) * each, bytes_accessed=1 << 20, transcendentals=0
                ),
                name=name,
            )(*group, *weights, *total)
            skip += len(group)
        return total

    ff = gate.shape[1]
    (hidden,) = product(
        hidden_kernel,
        "hidden",
        ring(block, count),
        (gate, gate2, up, up2),
        [jax.ShapeDtypeStruct((half, 2 * ff), F32)] * 2 + [jax.ShapeDtypeStruct((half, 128), F32)],
        [jax.ShapeDtypeStruct((half, 2 * ff), BF)],
        2 * half * 2 * width * 4 * ff,
    )
    (made,) = product(
        down_kernel,
        "down",
        ring(hidden, count),
        (down, down2),
        [jax.ShapeDtypeStruct((half, width), F32)] * 2,
        [jax.ShapeDtypeStruct((experts, 2, 8, width), BF)],
        2 * half * 2 * ff * 2 * width,
    )
    back = lax.all_to_all(made.reshape(2 * experts, 8, width), ("z", "x", "c"), 0, 0, tiled=True)

    return call(
        combine_kernel,
        out_shape=jax.ShapeDtypeStruct((rows, width), BF),
        in_specs=[VM, VM, VM],
        out_specs=VM,
        compiler_params=pltpu.CompilerParams(vmem_limit_bytes=8 << 20),
        name="combine",
    )(picks, shares, back.reshape(experts * cap, width))


def solution(mesh):
    split = Mesh(mesh.devices.reshape(12, 4, 8, 2), ("z", "x", "y", "c"))
    ep, tp = ("z", "x"), ("y", "c")
    in_specs = (
        P(ep, tp),
        P(tp),
        P(ep, None),
        P(ep, None),
        P(ep, None, tp),
        P(ep, None, tp),
        P(ep, None, tp),
    )
    return jax.shard_map(body, mesh=split, in_specs=in_specs, out_specs=P(ep, tp), check_vma=False)
```

time: 180 us -> 172 us (0.956)
  waiting for transfers between devices: 67 us -> 32 us
  starting transfers between devices: 55.7 us -> 78.7 us
  Pallas kernels: 14.5 us -> 6.92 us
  local copies, waits for them, and re-layouts: 1.96 us -> 7.23 us
  blocking collectives: 40 us -> 44.8 us
    ppermute x8 -> x14, waiting for transfers between devices: 54.5 us -> 24 us  [the longest x6 12.9 us: ring(): other = lax.ppermute(other, ('y', 'c'), perm(-1))]
    ppermute x8 -> x14, starting transfers between devices: 26.7 us -> 51.8 us  [the longest x6 30.8 us: ring(): main = lax.ppermute(main, ('y', 'c'), perm(1))]
    pallas_call x6 -> x2, Pallas kernels: 10.1 us -> 2.96 us  [product(): call(functools.partial(kernel, count, skip, len(group), last), out_shape=...]
    unnamed x14 -> x28, local copies, waits for them, and re-layouts: 1.92 us -> 7.23 us
    all_to_all x1, waiting for transfers between devices: 11.5 us -> 8 us  [body(): lax.all_to_all(outgoing.reshape(2 * experts, 8, width), ('z', 'x', 'c'),...]
    all_to_all x1, blocking collectives: 40 us -> 42.5 us  [body(): lax.all_to_all(made.reshape(2 * experts, 8, width), ('z', 'x', 'c'), 0, 0...]
    all_gather x0 -> x1, blocking collectives: none -> 2.23 us  [body(): lax.all_gather(norm_gain[None], 'c', axis=0)]
    ppermute x4 -> x3, starting transfers between devices: 8.84 us -> 6.91 us  [swap(): return lax.ppermute(value, 'c', [(0, 1), (1, 0)])]
  transfers between devices with their start and end apart: 13 -> 18, of which waited for: 10 -> 13; matrix products, arithmetic and copies ran while one was open for 0% -> 0% of each run, Pallas kernels for 4% -> 0%
where the time goes in v6:
time: 172 us; the launch traced here: 170 us
  starting transfers between devices  78.7 us (46%)
  blocking collectives  44.8 us (26%)
  waiting for transfers between devices  32 us (19%)
  local copies, waits for them, and re-layouts  7.23 us (4%)
  Pallas kernels  6.92 us (4%)
    all_to_all x1, blocking collectives, body(): lax.all_to_all(made.reshape(2 * experts, 8, width), ('z', 'x', 'c'), 0, 0...  42.5 us
    ppermute x6, starting transfers between devices, ring(): main = lax.ppermute(main, ('y', 'c'), perm(1))  30.8 us
    all_to_all x1, starting transfers between devices, body(): lax.all_to_all(outgoing.reshape(2 * experts, 8, width), ('z', 'x', 'c'),...  20 us
    ppermute x6, waiting for transfers between devices, ring(): other = lax.ppermute(other, ('y', 'c'), perm(-1))  12.9 us
    ppermute x6, starting transfers between devices, ring(): other = lax.ppermute(other, ('y', 'c'), perm(-1))  11.7 us
    ppermute x2, starting transfers between devices, ring(): found.append(lax.ppermute(main, ('y', 'c'), perm(1)))  9.28 us
    all_to_all x1, waiting for transfers between devices, body(): lax.all_to_all(outgoing.reshape(2 * experts, 8, width), ('z', 'x', 'c'),...  8 us
    ppermute x6, waiting for transfers between devices, ring(): main = lax.ppermute(main, ('y', 'c'), perm(1))  7.78 us
  transfers between devices with their start and end apart: 18, of which 13 were waited for; matrix products, arithmetic and copies ran while one was open for 0% of the time, Pallas kernels for 0%

profile of v6, /device:TPU:1, one launch (start us, length us, event | category | flops | bytes accessed | tf_op | source)
XLA Modules:
  0.0 169.9 jit_solution(12054527448290990698)
XLA Ops:
  0.0 2.2 %dispatch.1 = bf16[768,256]{1,0:T(8,128)(2,1)} custom-call(s32[2,256]{1,0:T(2,128)} %bitcast.17, bf16[256,256]{1,0:T(8,128)(2,1)} %tok_ref.1), custom_call_target="tpu_custom_call" | custom-call | tf_op jit(solution)/shard_map/dispatch/pallas_call | solution.py:177
  2.2 20.0 %all-to-all-start = ((bf16[96,8,256]{2,1,0:T(8,128)(2,1)}), bf16[96,8,256]{2,1,0:T(8,128)(2,1)S(1)}, u32[]{:S(2)}, u32[]{:S(2)}) async-start(bf16[96,8,256]{2,1,0:T(8,128)(2,1)} %bitcast.20), calls=%async_computation | async-start | bytes 786432 | tf_op jit(solution)/shard_map/all_to_all | solution.py:185
  22.2 2.6 %collective-permute-start = (bf16[4096,128]{1,0:T(8,128)(2,1)}, bf16[4096,128]{1,0:T(8,128)(2,1)S(1)}, u32[]{:S(2)}, u32[]{:S(2)}) collective-permute-start(bf16[4096,128]{1,0:T(8,128)(2,1)} %bitcast.13), channel_id=1, source_target_pairs={{0,1},{1,0},{2,3},{3,2},{4,5},{5,4},{6,7},{7,6},{8,9},{9,8},{10,11... | collective-permute-start | bytes 3145736 | tf_op jit(solution)/shard_map/ppermute | solution.py:165
  24.8 1.9 %collective-permute-start.1 = (bf16[4096,128]{1,0:T(8,128)(2,1)}, bf16[4096,128]{1,0:T(8,128)(2,1)S(1)}, u32[]{:S(2)}, u32[]{:S(2)}) collective-permute-start(bf16[4096,128]{1,0:T(8,128)(2,1)} %bitcast.15), channel_id=1, source_target_pairs={{0,1},{1,0},{2,3},{3,2},{4,5},{5,4},{6,7},{7,6},{8,9},{9,8},{10,11... | collective-permute-start | bytes 3145736 | tf_op jit(solution)/shard_map/ppermute | solution.py:165
  26.7 2.4 %collective-permute-start.2 = (bf16[2048,256]{1,0:T(8,128)(2,1)S(1)}, bf16[2048,256]{1,0:T(8,128)(2,1)S(1)}, u32[]{:S(2)}, u32[]{:S(2)}) collective-permute-start(bf16[2048,256]{1,0:T(8,128)(2,1)S(1)} %bitcast.11), channel_id=1, source_target_pairs={{0,1},{1,0},{2,3},{3,2},{4,5},{5,4},{6,7},{7,6},{8,9},{9,8},{10,11... | collective-permute-start | bytes 3145736 | tf_op jit(solution)/shard_map/ppermute | solution.py:165
  29.2 2.2 %all-gather.1.gain_ref = f32[2,1,256]{2,1,0:T(1,128)S(1)} all-gather(f32[1,1,256]{2,1,0:T(1,128)S(1)} %bitcast.21), channel_id=2, replica_groups=mesh['z'=12,'x'=4,'y'=8,'c'=2] {'c'}, dimensions={0}, use_global_device_ids=true | all-gather | bytes 3072 | tf_op jit(solution)/shard_map/all_gather | solution.py:201
  35.7 8.0 %all-to-all-done.came_ref = bf16[96,8,256]{2,1,0:T(8,128)(2,1)S(1)} async-done(((bf16[96,8,256]{2,1,0:T(8,128)(2,1)}), bf16[96,8,256]{2,1,0:T(8,128)(2,1)S(1)}, u32[]{:S(2)}, u32[]{:S(2)}) %all-to-all-start) | async-done | bytes 393248 | tf_op jit(solution)/shard_map/all_to_all | solution.py:185
  43.7 5.1 %collective-permute-start.3 = (bf16[392,512]{1,0:T(8,128)(2,1)S(1)}, bf16[392,512]{1,0:T(8,128)(2,1)S(1)}, u32[]{:S(2)}, u32[]{:S(2)}) collective-permute-start(bf16[392,512]{1,0:T(8,128)(2,1)S(1)} %pack.1.refs_0_), channel_id=1, source_target_pairs={{0,2},{1,15},{2,4},{3,1},{4,6},{5,3},{6,8},{7,5},{8,10},{9,7},{10,... | collective-permute-start | bytes 1204232 | tf_op jit(solution)/shard_map/ppermute | solution.py:157
  50.8 3.3 %collective-permute-done.3.refs_1_ = bf16[392,512]{1,0:T(8,128)(2,1)S(1)} collective-permute-done((bf16[392,512]{1,0:T(8,128)(2,1)S(1)}, bf16[392,512]{1,0:T(8,128)(2,1)S(1)}, u32[]{:S(2)}, u32[]{:S(2)}) %collective-permute-start.3) | collective-permute-done | bytes 401440 | tf_op jit(solution)/shard_map/ppermute | solution.py:157
  54.0 5.3 %collective-permute-start.5 = (bf16[392,512]{1,0:T(8,128)(2,1)S(1)}, bf16[392,512]{1,0:T(8,128)(2,1)S(1)}, u32[]{:S(2)}, u32[]{:S(2)}) collective-permute-start(bf16[392,512]{1,0:T(8,128)(2,1)S(1)} %collective-permute-done.3.refs_1_), channel_id=1, source_target_pairs={{0,2},{1,15},{2,4},{3,1},{4,6},{5,3},{6,8},{7,5},{8,10},{9,7},{10,... | collective-permute-start | bytes 1204232 | tf_op jit(solution)/shard_map/ppermute | solution.py:157
  60.1 2.0 %collective-permute-start.6 = (bf16[392,512]{1,0:T(8,128)(2,1)S(1)}, bf16[392,512]{1,0:T(8,128)(2,1)S(1)}, u32[]{:S(2)}, u32[]{:S(2)}) collective-permute-start(bf16[392,512]{1,0:T(8,128)(2,1)S(1)} %collective-permute-done.4.refs_2_), channel_id=1, source_target_pairs={{0,14},{1,3},{2,0},{3,5},{4,2},{5,7},{6,4},{7,9},{8,6},{9,11},{10,... | collective-permute-start | bytes 1204232 | tf_op jit(solution)/shard_map/ppermute | solution.py:158
  62.1 2.1 %collective-permute-done.5.refs_3_ = bf16[392,512]{1,0:T(8,128)(2,1)S(1)} collective-permute-done((bf16[392,512]{1,0:T(8,128)(2,1)S(1)}, bf16[392,512]{1,0:T(8,128)(2,1)S(1)}, u32[]{:S(2)}, u32[]{:S(2)}) %collective-permute-start.5) | collective-permute-done | bytes 401440 | tf_op jit(solution)/shard_map/ppermute | solution.py:157
  64.1 5.0 %collective-permute-start.7 = (bf16[392,512]{1,0:T(8,128)(2,1)S(1)}, bf16[392,512]{1,0:T(8,128)(2,1)S(1)}, u32[]{:S(2)}, u32[]{:S(2)}) collective-permute-start(bf16[392,512]{1,0:T(8,128)(2,1)S(1)} %collective-permute-done.5.refs_3_), channel_id=1, source_target_pairs={{0,2},{1,15},{2,4},{3,1},{4,6},{5,3},{6,8},{7,5},{8,10},{9,7},{10,... | collective-permute-start | bytes 1204232 | tf_op jit(solution)/shard_map/ppermute | solution.py:157
  69.2 3.9 %collective-permute-done.6.refs_4_ = bf16[392,512]{1,0:T(8,128)(2,1)S(1)} collective-permute-done((bf16[392,512]{1,0:T(8,128)(2,1)S(1)}, bf16[392,512]{1,0:T(8,128)(2,1)S(1)}, u32[]{:S(2)}, u32[]{:S(2)}) %collective-permute-start.6) | collective-permute-done | bytes 401440 | tf_op jit(solution)/shard_map/ppermute | solution.py:158
  73.1 2.0 %collective-permute-start.8 = (bf16[392,512]{1,0:T(8,128)(2,1)S(1)}, bf16[392,512]{1,0:T(8,128)(2,1)S(1)}, u32[]{:S(2)}, u32[]{:S(2)}) collective-permute-start(bf16[392,512]{1,0:T(8,128)(2,1)S(1)} %collective-permute-done.6.refs_4_), channel_id=1, source_target_pairs={{0,14},{1,3},{2,0},{3,5},{4,2},{5,7},{6,4},{7,9},{8,6},{9,11},{10,... | collective-permute-start | bytes 1204232 | tf_op jit(solution)/shard_map/ppermute | solution.py:158
  75.6 4.3 %collective-permute-start.9 = (bf16[392,512]{1,0:T(8,128)(2,1)S(1)}, bf16[392,512]{1,0:T(8,128)(2,1)S(1)}, u32[]{:S(2)}, u32[]{:S(2)}) collective-permute-start(bf16[392,512]{1,0:T(8,128)(2,1)S(1)} %collective-permute-done.7.refs_5_), channel_id=1, source_target_pairs={{0,2},{1,15},{2,4},{3,1},{4,6},{5,3},{6,8},{7,5},{8,10},{9,7},{10,... | collective-permute-start | bytes 1204232 | tf_op jit(solution)/shard_map/ppermute | solution.py:160
  79.9 7.6 %collective-permute-done.8.refs_6_ = bf16[392,512]{1,0:T(8,128)(2,1)S(1)} collective-permute-done((bf16[392,512]{1,0:T(8,128)(2,1)S(1)}, bf16[392,512]{1,0:T(8,128)(2,1)S(1)}, u32[]{:S(2)}, u32[]{:S(2)}) %collective-permute-start.8) | collective-permute-done | bytes 401440 | tf_op jit(solution)/shard_map/ppermute | solution.py:158
  92.6 2.0 %hidden.1.refs_0_ = bf16[384,256]{1,0:T(8,128)(2,1)S(1)} custom-call(bf16[392,512]{1,0:T(8,128)(2,1)S(1)} %pack.1.refs_0_, bf16[392,512]{1,0:T(8,128)(2,1)S(1)} %collective-permute-done.3.refs_1_, bf16[392,512]{1,0:T(8,128)(2,1)S(1)} %collective-permute-done.4.refs_2_, bf16[392,512]{1,0:T(8,128)(2,1)S(1)} %collective-permute-done.5.refs_3_, ...), custom_call_target="tpu_custom_call" | custom-call | flops 1610612736 | bytes 1048576 | tf_op jit(solution)/shard_map/hidden/pallas_call | solution.py:217
  94.6 5.3 %collective-permute-start.10 = (bf16[384,256]{1,0:T(8,128)(2,1)S(1)}, bf16[384,256]{1,0:T(8,128)(2,1)S(1)}, u32[]{:S(2)}, u32[]{:S(2)}) collective-permute-start(bf16[384,256]{1,0:T(8,128)(2,1)S(1)} %hidden.1.refs_0_), channel_id=1, source_target_pairs={{0,2},{1,15},{2,4},{3,1},{4,6},{5,3},{6,8},{7,5},{8,10},{9,7},{10,... | collective-permute-start | bytes 589832 | tf_op jit(solution)/shard_map/ppermute | solution.py:157
  99.9 1.9 %collective-permute-start.11 = (bf16[384,256]{1,0:T(8,128)(2,1)S(1)}, bf16[384,256]{1,0:T(8,128)(2,1)S(1)}, u32[]{:S(2)}, u32[]{:S(2)}) collective-permute-start(bf16[384,256]{1,0:T(8,128)(2,1)S(1)} %hidden.1.refs_0_), channel_id=1, source_target_pairs={{0,14},{1,3},{2,0},{3,5},{4,2},{5,7},{6,4},{7,9},{8,6},{9,11},{10,... | collective-permute-start | bytes 589832 | tf_op jit(solution)/shard_map/ppermute | solution.py:158
  102.5 5.0 %collective-permute-start.12 = (bf16[384,256]{1,0:T(8,128)(2,1)S(1)}, bf16[384,256]{1,0:T(8,128)(2,1)S(1)}, u32[]{:S(2)}, u32[]{:S(2)}) collective-permute-start(bf16[384,256]{1,0:T(8,128)(2,1)S(1)} %collective-permute-done.10.refs_1_), channel_id=1, source_target_pairs={{0,2},{1,15},{2,4},{3,1},{4,6},{5,3},{6,8},{7,5},{8,10},{9,7},{10,... | collective-permute-start | bytes 589832 | tf_op jit(solution)/shard_map/ppermute | solution.py:157
  110.1 5.0 %collective-permute-start.14 = (bf16[384,256]{1,0:T(8,128)(2,1)S(1)}, bf16[384,256]{1,0:T(8,128)(2,1)S(1)}, u32[]{:S(2)}, u32[]{:S(2)}) collective-permute-start(bf16[384,256]{1,0:T(8,128)(2,1)S(1)} %collective-permute-done.12.refs_3_), channel_id=1, source_target_pairs={{0,2},{1,15},{2,4},{3,1},{4,6},{5,3},{6,8},{7,5},{8,10},{9,7},{10,... | collective-permute-start | bytes 589832 | tf_op jit(solution)/shard_map/ppermute | solution.py:157
  117.7 5.0 %collective-permute-start.16 = (bf16[384,256]{1,0:T(8,128)(2,1)S(1)}, bf16[384,256]{1,0:T(8,128)(2,1)S(1)}, u32[]{:S(2)}, u32[]{:S(2)}) collective-permute-start(bf16[384,256]{1,0:T(8,128)(2,1)S(1)} %collective-permute-done.14.refs_5_), channel_id=1, source_target_pairs={{0,2},{1,15},{2,4},{3,1},{4,6},{5,3},{6,8},{7,5},{8,10},{9,7},{10,... | collective-permute-start | bytes 589832 | tf_op jit(solution)/shard_map/ppermute | solution.py:160
  126.3 42.5 %all_to_all.10 = bf16[96,8,256]{2,1,0:T(8,128)(2,1)S(1)} all-to-all(bf16[96,8,256]{2,1,0:T(8,128)(2,1)S(1)} %bitcast.10), channel_id=1, replica_groups=mesh['z'=12,'x'=4,'y'=8,'c'=2] {'z','x','c'}, dimensions={0} | all-to-all | bytes 786432 | tf_op jit(solution)/shard_map/all_to_all | solution.py:250
  (48 shorter events, 23.0 us)
Async XLA Ops:
  0.0 26.7 %copy-start = (bf16[1,2048,256]{2,1,0:T(8,128)(2,1)S(1)}, bf16[1,2048,256]{2,1,0:T(8,128)(2,1)}, u32[]{:S(2)}) copy-start(bf16[1,2048,256]{2,1,0:T(8,128)(2,1)} %param.13) | copy-start | bytes 3145732
  2.2 41.5 %all-to-all-start = ((bf16[96,8,256]{2,1,0:T(8,128)(2,1)}), bf16[96,8,256]{2,1,0:T(8,128)(2,1)S(1)}, u32[]{:S(2)}, u32[]{:S(2)}) async-start(bf16[96,8,256]{2,1,0:T(8,128)(2,1)} %bitcast.20), calls=%async_computation | async-start | bytes 786432 | tf_op jit(solution)/shard_map/all_to_all | solution.py:185
  22.2 11.5 %collective-permute-start = (bf16[4096,128]{1,0:T(8,128)(2,1)}, bf16[4096,128]{1,0:T(8,128)(2,1)S(1)}, u32[]{:S(2)}, u32[]{:S(2)}) collective-permute-start(bf16[4096,128]{1,0:T(8,128)(2,1)} %bitcast.13), channel_id=1, source_target_pairs={{0,1},{1,0},{2,3},{3,2},{4,5},{5,4},{6,7},{7,6},{8,9},{9,8},{10,11... | collective-permute-start | bytes 3145736 | tf_op jit(solution)/shard_map/ppermute | solution.py:165
  24.8 9.9 %collective-permute-start.1 = (bf16[4096,128]{1,0:T(8,128)(2,1)}, bf16[4096,128]{1,0:T(8,128)(2,1)S(1)}, u32[]{:S(2)}, u32[]{:S(2)}) collective-permute-start(bf16[4096,128]{1,0:T(8,128)(2,1)} %bitcast.15), channel_id=1, source_target_pairs={{0,1},{1,0},{2,3},{3,2},{4,5},{5,4},{6,7},{7,6},{8,9},{9,8},{10,11... | collective-permute-start | bytes 3145736 | tf_op jit(solution)/shard_map/ppermute | solution.py:165
  26.7 2.4 %copy-start.13 = (f32[256]{0:T(256)S(1)}, f32[256]{0:T(256)}, u32[]{:S(2)}) copy-start(f32[256]{0:T(256)} %param.8) | copy-start | bytes 3076
  26.7 8.9 %collective-permute-start.2 = (bf16[2048,256]{1,0:T(8,128)(2,1)S(1)}, bf16[2048,256]{1,0:T(8,128)(2,1)S(1)}, u32[]{:S(2)}, u32[]{:S(2)}) collective-permute-start(bf16[2048,256]{1,0:T(8,128)(2,1)S(1)} %bitcast.11), channel_id=1, source_target_pairs={{0,1},{1,0},{2,3},{3,2},{4,5},{5,4},{6,7},{7,6},{8,9},{9,8},{10,11... | collective-permute-start | bytes 3145736 | tf_op jit(solution)/shard_map/ppermute | solution.py:165
  29.2 2.3 %copy-start.11 = (s32[256,2]{0,1:T(2,128)S(1)}, s32[256,2]{0,1:T(2,128)}, u32[]{:S(2)}) copy-start(s32[256,2]{0,1:T(2,128)} %param.9) | copy-start | bytes 6148
  31.4 57.5 %copy-start.1 = (bf16[1,4096,128]{2,1,0:T(8,128)(2,1)S(1)}, bf16[1,4096,128]{2,1,0:T(8,128)(2,1)}, u32[]{:S(2)}) copy-start(bf16[1,4096,128]{2,1,0:T(8,128)(2,1)} %param.11) | copy-start | bytes 3145732
  43.7 10.3 %collective-permute-start.3 = (bf16[392,512]{1,0:T(8,128)(2,1)S(1)}, bf16[392,512]{1,0:T(8,128)(2,1)S(1)}, u32[]{:S(2)}, u32[]{:S(2)}) collective-permute-start(bf16[392,512]{1,0:T(8,128)(2,1)S(1)} %pack.1.refs_0_), channel_id=1, source_target_pairs={{0,2},{1,15},{2,4},{3,1},{4,6},{5,3},{6,8},{7,5},{8,10},{9,7},{10,... | collective-permute-start | bytes 1204232 | tf_op jit(solution)/shard_map/ppermute | solution.py:157
  48.8 11.2 %collective-permute-start.4 = (bf16[392,512]{1,0:T(8,128)(2,1)S(1)}, bf16[392,512]{1,0:T(8,128)(2,1)S(1)}, u32[]{:S(2)}, u32[]{:S(2)}) collective-permute-start(bf16[392,512]{1,0:T(8,128)(2,1)S(1)} %pack.1.refs_0_), channel_id=1, source_target_pairs={{0,14},{1,3},{2,0},{3,5},{4,2},{5,7},{6,4},{7,9},{8,6},{9,11},{10,... | collective-permute-start | bytes 1204232 | tf_op jit(solution)/shard_map/ppermute | solution.py:158
  54.0 10.1 %collective-permute-start.5 = (bf16[392,512]{1,0:T(8,128)(2,1)S(1)}, bf16[392,512]{1,0:T(8,128)(2,1)S(1)}, u32[]{:S(2)}, u32[]{:S(2)}) collective-permute-start(bf16[392,512]{1,0:T(8,128)(2,1)S(1)} %collective-permute-done.3.refs_1_), channel_id=1, source_target_pairs={{0,2},{1,15},{2,4},{3,1},{4,6},{5,3},{6,8},{7,5},{8,10},{9,7},{10,... | collective-permute-start | bytes 1204232 | tf_op jit(solution)/shard_map/ppermute | solution.py:157
  60.1 13.0 %collective-permute-start.6 = (bf16[392,512]{1,0:T(8,128)(2,1)S(1)}, bf16[392,512]{1,0:T(8,128)(2,1)S(1)}, u32[]{:S(2)}, u32[]{:S(2)}) collective-permute-start(bf16[392,512]{1,0:T(8,128)(2,1)S(1)} %collective-permute-done.4.refs_2_), channel_id=1, source_target_pairs={{0,14},{1,3},{2,0},{3,5},{4,2},{5,7},{6,4},{7,9},{8,6},{9,11},{10,... | collective-permute-start | bytes 1204232 | tf_op jit(solution)/shard_map/ppermute | solution.py:158
  64.1 11.4 %collective-permute-start.7 = (bf16[392,512]{1,0:T(8,128)(2,1)S(1)}, bf16[392,512]{1,0:T(8,128)(2,1)S(1)}, u32[]{:S(2)}, u32[]{:S(2)}) collective-permute-start(bf16[392,512]{1,0:T(8,128)(2,1)S(1)} %collective-permute-done.5.refs_3_), channel_id=1, source_target_pairs={{0,2},{1,15},{2,4},{3,1},{4,6},{5,3},{6,8},{7,5},{8,10},{9,7},{10,... | collective-permute-start | bytes 1204232 | tf_op jit(solution)/shard_map/ppermute | solution.py:157
  73.1 14.4 %collective-permute-start.8 = (bf16[392,512]{1,0:T(8,128)(2,1)S(1)}, bf16[392,512]{1,0:T(8,128)(2,1)S(1)}, u32[]{:S(2)}, u32[]{:S(2)}) collective-permute-start(bf16[392,512]{1,0:T(8,128)(2,1)S(1)} %collective-permute-done.6.refs_4_), channel_id=1, source_target_pairs={{0,14},{1,3},{2,0},{3,5},{4,2},{5,7},{6,4},{7,9},{8,6},{9,11},{10,... | collective-permute-start | bytes 1204232 | tf_op jit(solution)/shard_map/ppermute | solution.py:158
  75.6 13.3 %collective-permute-start.9 = (bf16[392,512]{1,0:T(8,128)(2,1)S(1)}, bf16[392,512]{1,0:T(8,128)(2,1)S(1)}, u32[]{:S(2)}, u32[]{:S(2)}) collective-permute-start(bf16[392,512]{1,0:T(8,128)(2,1)S(1)} %collective-permute-done.7.refs_5_), channel_id=1, source_target_pairs={{0,2},{1,15},{2,4},{3,1},{4,6},{5,3},{6,8},{7,5},{8,10},{9,7},{10,... | collective-permute-start | bytes 1204232 | tf_op jit(solution)/shard_map/ppermute | solution.py:160
  94.6 7.9 %collective-permute-start.10 = (bf16[384,256]{1,0:T(8,128)(2,1)S(1)}, bf16[384,256]{1,0:T(8,128)(2,1)S(1)}, u32[]{:S(2)}, u32[]{:S(2)}) collective-permute-start(bf16[384,256]{1,0:T(8,128)(2,1)S(1)} %hidden.1.refs_0_), channel_id=1, source_target_pairs={{0,2},{1,15},{2,4},{3,1},{4,6},{5,3},{6,8},{7,5},{8,10},{9,7},{10,... | collective-permute-start | bytes 589832 | tf_op jit(solution)/shard_map/ppermute | solution.py:157
  99.9 7.6 %collective-permute-start.11 = (bf16[384,256]{1,0:T(8,128)(2,1)S(1)}, bf16[384,256]{1,0:T(8,128)(2,1)S(1)}, u32[]{:S(2)}, u32[]{:S(2)}) collective-permute-start(bf16[384,256]{1,0:T(8,128)(2,1)S(1)} %hidden.1.refs_0_), channel_id=1, source_target_pairs={{0,14},{1,3},{2,0},{3,5},{4,2},{5,7},{6,4},{7,9},{8,6},{9,11},{10,... | collective-permute-start | bytes 589832 | tf_op jit(solution)/shard_map/ppermute | solution.py:158
  102.5 7.6 %collective-permute-start.12 = (bf16[384,256]{1,0:T(8,128)(2,1)S(1)}, bf16[384,256]{1,0:T(8,128)(2,1)S(1)}, u32[]{:S(2)}, u32[]{:S(2)}) collective-permute-start(bf16[384,256]{1,0:T(8,128)(2,1)S(1)} %collective-permute-done.10.refs_1_), channel_id=1, source_target_pairs={{0,2},{1,15},{2,4},{3,1},{4,6},{5,3},{6,8},{7,5},{8,10},{9,7},{10,... | collective-permute-start | bytes 589832 | tf_op jit(solution)/shard_map/ppermute | solution.py:157
  107.5 7.6 %collective-permute-start.13 = (bf16[384,256]{1,0:T(8,128)(2,1)S(1)}, bf16[384,256]{1,0:T(8,128)(2,1)S(1)}, u32[]{:S(2)}, u32[]{:S(2)}) collective-permute-start(bf16[384,256]{1,0:T(8,128)(2,1)S(1)} %collective-permute-done.11.refs_2_), channel_id=1, source_target_pairs={{0,14},{1,3},{2,0},{3,5},{4,2},{5,7},{6,4},{7,9},{8,6},{9,11},{10,... | collective-permute-start | bytes 589832 | tf_op jit(solution)/shard_map/ppermute | solution.py:158
  110.1 7.6 %collective-permute-start.14 = (bf16[384,256]{1,0:T(8,128)(2,1)S(1)}, bf16[384,256]{1,0:T(8,128)(2,1)S(1)}, u32[]{:S(2)}, u32[]{:S(2)}) collective-permute-start(bf16[384,256]{1,0:T(8,128)(2,1)S(1)} %collective-permute-done.12.refs_3_), channel_id=1, source_target_pairs={{0,2},{1,15},{2,4},{3,1},{4,6},{5,3},{6,8},{7,5},{8,10},{9,7},{10,... | collective-permute-start | bytes 589832 | tf_op jit(solution)/shard_map/ppermute | solution.py:157
  115.1 8.3 %collective-permute-start.15 = (bf16[384,256]{1,0:T(8,128)(2,1)S(1)}, bf16[384,256]{1,0:T(8,128)(2,1)S(1)}, u32[]{:S(2)}, u32[]{:S(2)}) collective-permute-start(bf16[384,256]{1,0:T(8,128)(2,1)S(1)} %collective-permute-done.13.refs_4_), channel_id=1, source_target_pairs={{0,14},{1,3},{2,0},{3,5},{4,2},{5,7},{6,4},{7,9},{8,6},{9,11},{10,... | collective-permute-start | bytes 589832 | tf_op jit(solution)/shard_map/ppermute | solution.py:158
  117.7 7.6 %collective-permute-start.16 = (bf16[384,256]{1,0:T(8,128)(2,1)S(1)}, bf16[384,256]{1,0:T(8,128)(2,1)S(1)}, u32[]{:S(2)}, u32[]{:S(2)}) collective-permute-start(bf16[384,256]{1,0:T(8,128)(2,1)S(1)} %collective-permute-done.14.refs_5_), channel_id=1, source_target_pairs={{0,2},{1,15},{2,4},{3,1},{4,6},{5,3},{6,8},{7,5},{8,10},{9,7},{10,... | collective-permute-start | bytes 589832 | tf_op jit(solution)/shard_map/ppermute | solution.py:160
  125.3 43.5 %copy-start.10 = (f32[2,256,128]{2,1,0:T(8,128)S(1)}, f32[2,256,128]{2,1,0:T(8,128)}, u32[]{:S(2)}) copy-start(f32[2,256,128]{2,1,0:T(8,128)} %copy-done.9) | copy-start | bytes 786436
  126.3 42.5 %copy-start.8 = (bf16[2,256,768]{2,1,0:T(8,128)(2,1)S(1)}, bf16[2,256,768]{2,1,0:T(8,128)(2,1)}, u32[]{:S(2)}) copy-start(bf16[2,256,768]{2,1,0:T(8,128)(2,1)} %copy-done.7) | copy-start | bytes 2359300
  (8 other events, 9.5 us)

commit v7 on v6

--- a/solution.py
+++ b/solution.py
@@ -197,9 +197,10 @@
         name="plan",
     )(ids, expert_weights.T)
     gate, up, down = gate_weight[0], up_weight[0], down_weight[0]
-    came, gains, gate2, up2, down2, picks, shares = lax.optimization_barrier(
-        (came, lax.all_gather(norm_gain[None], "c", axis=0), swap(gate), swap(up), swap(down), picks, shares)
-    )
+    came, gains, picks, shares = lax.optimization_barrier(
+        (came, lax.all_gather(norm_gain[None], "c", axis=0), picks, shares)
+    )
+    gate2, up2, down2 = swap(gate), swap(up), swap(down)
     block = call(
         pack_kernel,
         out_shape=jax.ShapeDtypeStruct((half + PAD, 2 * width), BF),

time: 172 us -> 165 us (0.959)
  blocking collectives: 44.8 us -> 33.1 us
  waiting for transfers between devices: 32 us -> 38.7 us
  local copies, waits for them, and re-layouts: 7.23 us -> 2.28 us
  starting transfers between devices: 78.7 us -> 81.5 us
    all_to_all x1, blocking collectives: 42.5 us -> 30.8 us  [body(): lax.all_to_all(made.reshape(2 * experts, 8, width), ('z', 'x', 'c'), 0, 0...]
    ppermute x6, starting transfers between devices: 11.7 us -> 20.7 us  [ring(): other = lax.ppermute(other, ('y', 'c'), perm(-1))]
    all_to_all x1, waiting for transfers between devices: 8 us -> 16.2 us  [body(): lax.all_to_all(outgoing.reshape(2 * experts, 8, width), ('z', 'x', 'c'),...]
    ppermute x2, waiting for transfers between devices: 3.35 us -> 10.6 us  [ring(): found.append(lax.ppermute(main, ('y', 'c'), perm(1)))]
    ppermute x6, waiting for transfers between devices: 12.9 us -> 6.38 us  [ring(): other = lax.ppermute(other, ('y', 'c'), perm(-1))]
    unnamed x28 -> x20, local copies, waits for them, and re-layouts: 7.23 us -> 2.28 us
    ppermute x6, starting transfers between devices: 30.8 us -> 25.9 us  [ring(): main = lax.ppermute(main, ('y', 'c'), perm(1))]
    ppermute x2, starting transfers between devices: 9.28 us -> 5.88 us  [ring(): found.append(lax.ppermute(main, ('y', 'c'), perm(1)))]
  transfers between devices with their start and end apart: 18 -> 18, of which waited for: 13 -> 11; matrix products, arithmetic and copies ran while one was open for 0% -> 0% of each run, Pallas kernels for 0% -> 2%
where the time goes in v7:
time: 165 us; the launch traced here: 163 us
  starting transfers between devices  81.5 us (49%)
  waiting for transfers between devices  38.7 us (23%)
  blocking collectives  33.1 us (20%)
  Pallas kernels  6.84 us (4%)
  local copies, waits for them, and re-layouts  2.28 us (1%)
    all_to_all x1, blocking collectives, body(): lax.all_to_all(made.reshape(2 * experts, 8, width), ('z', 'x', 'c'), 0, 0...  30.8 us
    ppermute x6, starting transfers between devices, ring(): main = lax.ppermute(main, ('y', 'c'), perm(1))  25.9 us
    ppermute x6, starting transfers between devices, ring(): other = lax.ppermute(other, ('y', 'c'), perm(-1))  20.7 us
    all_to_all x1, starting transfers between devices, body(): lax.all_to_all(outgoing.reshape(2 * experts, 8, width), ('z', 'x', 'c'),...  20 us
    all_to_all x1, waiting for transfers between devices, body(): lax.all_to_all(outgoing.reshape(2 * experts, 8, width), ('z', 'x', 'c'),...  16.2 us
    ppermute x2, waiting for transfers between devices, ring(): found.append(lax.ppermute(main, ('y', 'c'), perm(1)))  10.6 us
    ppermute x3, starting transfers between devices, swap(): return lax.ppermute(value, 'c', [(0, 1), (1, 0)])  8.99 us
    ppermute x6, waiting for transfers between devices, ring(): other = lax.ppermute(other, ('y', 'c'), perm(-1))  6.38 us
  transfers between devices with their start and end apart: 18, of which 11 were waited for; matrix products, arithmetic and copies ran while one was open for 0% of the time, Pallas kernels for 2%

profile of v7, /device:TPU:1, one launch (start us, length us, event | category | flops | bytes accessed | tf_op | source)
XLA Modules:
  0.0 162.7 jit_solution(13475718439975352698)
XLA Ops:
  0.0 2.1 %dispatch.1 = bf16[768,256]{1,0:T(8,128)(2,1)} custom-call(s32[2,256]{1,0:T(2,128)} %bitcast.17, bf16[256,256]{1,0:T(8,128)(2,1)} %tok_ref.1), custom_call_target="tpu_custom_call" | custom-call | tf_op jit(solution)/shard_map/dispatch/pallas_call | solution.py:177
  2.1 20.0 %all-to-all-start = ((bf16[96,8,256]{2,1,0:T(8,128)(2,1)}), bf16[96,8,256]{2,1,0:T(8,128)(2,1)S(1)}, u32[]{:S(2)}, u32[]{:S(2)}) async-start(bf16[96,8,256]{2,1,0:T(8,128)(2,1)} %bitcast.20), calls=%async_computation | async-start | bytes 786432 | tf_op jit(solution)/shard_map/all_to_all | solution.py:185
  22.8 2.3 %all-gather.1.gain_ref = f32[2,1,256]{2,1,0:T(1,128)S(1)} all-gather(f32[1,1,256]{2,1,0:T(1,128)S(1)} %bitcast.21), channel_id=2, replica_groups=mesh['z'=12,'x'=4,'y'=8,'c'=2] {'c'}, dimensions={0}, use_global_device_ids=true | all-gather | bytes 3072 | tf_op jit(solution)/shard_map/all_gather | solution.py:201
  27.4 16.2 %all-to-all-done.came_ref = bf16[96,8,256]{2,1,0:T(8,128)(2,1)S(1)} async-done(((bf16[96,8,256]{2,1,0:T(8,128)(2,1)}), bf16[96,8,256]{2,1,0:T(8,128)(2,1)S(1)}, u32[]{:S(2)}, u32[]{:S(2)}) %all-to-all-start) | async-done | bytes 393248 | tf_op jit(solution)/shard_map/all_to_all | solution.py:185
  43.7 5.1 %collective-permute-start = (bf16[392,512]{1,0:T(8,128)(2,1)S(1)}, bf16[392,512]{1,0:T(8,128)(2,1)S(1)}, u32[]{:S(2)}, u32[]{:S(2)}) collective-permute-start(bf16[392,512]{1,0:T(8,128)(2,1)S(1)} %pack.1.refs_0_), channel_id=1, source_target_pairs={{0,2},{1,15},{2,4},{3,1},{4,6},{5,3},{6,8},{7,5},{8,10},{9,7},{10,... | collective-permute-start | bytes 1204232 | tf_op jit(solution)/shard_map/ppermute | solution.py:157
  50.7 3.3 %collective-permute-done.refs_1_ = bf16[392,512]{1,0:T(8,128)(2,1)S(1)} collective-permute-done((bf16[392,512]{1,0:T(8,128)(2,1)S(1)}, bf16[392,512]{1,0:T(8,128)(2,1)S(1)}, u32[]{:S(2)}, u32[]{:S(2)}) %collective-permute-start) | collective-permute-done | bytes 401440 | tf_op jit(solution)/shard_map/ppermute | solution.py:157
  54.0 5.3 %collective-permute-start.2 = (bf16[392,512]{1,0:T(8,128)(2,1)S(1)}, bf16[392,512]{1,0:T(8,128)(2,1)S(1)}, u32[]{:S(2)}, u32[]{:S(2)}) collective-permute-start(bf16[392,512]{1,0:T(8,128)(2,1)S(1)} %collective-permute-done.refs_1_), channel_id=1, source_target_pairs={{0,2},{1,15},{2,4},{3,1},{4,6},{5,3},{6,8},{7,5},{8,10},{9,7},{10,... | collective-permute-start | bytes 1204232 | tf_op jit(solution)/shard_map/ppermute | solution.py:157
  59.3 4.3 %collective-permute-start.7 = (bf16[4096,128]{1,0:T(8,128)(2,1)S(1)}, bf16[4096,128]{1,0:T(8,128)(2,1)S(1)}, u32[]{:S(2)}, u32[]{:S(2)}) collective-permute-start(bf16[4096,128]{1,0:T(8,128)(2,1)S(1)} %bitcast.13), channel_id=1, source_target_pairs={{0,1},{1,0},{2,3},{3,2},{4,5},{5,4},{6,7},{7,6},{8,9},{9,8},{10,11... | collective-permute-start | bytes 3145736 | tf_op jit(solution)/shard_map/ppermute | solution.py:165
  65.5 4.1 %collective-permute-start.3 = (bf16[392,512]{1,0:T(8,128)(2,1)S(1)}, bf16[392,512]{1,0:T(8,128)(2,1)S(1)}, u32[]{:S(2)}, u32[]{:S(2)}) collective-permute-start(bf16[392,512]{1,0:T(8,128)(2,1)S(1)} %collective-permute-done.1.refs_2_), channel_id=1, source_target_pairs={{0,14},{1,3},{2,0},{3,5},{4,2},{5,7},{6,4},{7,9},{8,6},{9,11},{10,... | collective-permute-start | bytes 1204232 | tf_op jit(solution)/shard_map/ppermute | solution.py:158
  69.6 2.4 %collective-permute-start.4 = (bf16[392,512]{1,0:T(8,128)(2,1)S(1)}, bf16[392,512]{1,0:T(8,128)(2,1)S(1)}, u32[]{:S(2)}, u32[]{:S(2)}) collective-permute-start(bf16[392,512]{1,0:T(8,128)(2,1)S(1)} %collective-permute-done.2.refs_3_), channel_id=1, source_target_pairs={{0,2},{1,15},{2,4},{3,1},{4,6},{5,3},{6,8},{7,5},{8,10},{9,7},{10,... | collective-permute-start | bytes 1204232 | tf_op jit(solution)/shard_map/ppermute | solution.py:157
  72.0 3.8 %collective-permute-done.3.refs_4_ = bf16[392,512]{1,0:T(8,128)(2,1)S(1)} collective-permute-done((bf16[392,512]{1,0:T(8,128)(2,1)S(1)}, bf16[392,512]{1,0:T(8,128)(2,1)S(1)}, u32[]{:S(2)}, u32[]{:S(2)}) %collective-permute-start.3) | collective-permute-done | bytes 401440 | tf_op jit(solution)/shard_map/ppermute | solution.py:158
  75.8 4.1 %collective-permute-start.5 = (bf16[392,512]{1,0:T(8,128)(2,1)S(1)}, bf16[392,512]{1,0:T(8,128)(2,1)S(1)}, u32[]{:S(2)}, u32[]{:S(2)}) collective-permute-start(bf16[392,512]{1,0:T(8,128)(2,1)S(1)} %collective-permute-done.3.refs_4_), channel_id=1, source_target_pairs={{0,14},{1,3},{2,0},{3,5},{4,2},{5,7},{6,4},{7,9},{8,6},{9,11},{10,... | collective-permute-start | bytes 1204232 | tf_op jit(solution)/shard_map/ppermute | solution.py:158
  80.1 4.0 %collective-permute-start.6 = (bf16[392,512]{1,0:T(8,128)(2,1)S(1)}, bf16[392,512]{1,0:T(8,128)(2,1)S(1)}, u32[]{:S(2)}, u32[]{:S(2)}) collective-permute-start(bf16[392,512]{1,0:T(8,128)(2,1)S(1)} %collective-permute-done.4.refs_5_), channel_id=1, source_target_pairs={{0,2},{1,15},{2,4},{3,1},{4,6},{5,3},{6,8},{7,5},{8,10},{9,7},{10,... | collective-permute-start | bytes 1204232 | tf_op jit(solution)/shard_map/ppermute | solution.py:160
  84.1 2.8 %collective-permute-start.16 = (bf16[2048,256]{1,0:T(8,128)(2,1)S(1)}, bf16[2048,256]{1,0:T(8,128)(2,1)S(1)}, u32[]{:S(2)}, u32[]{:S(2)}) collective-permute-start(bf16[2048,256]{1,0:T(8,128)(2,1)S(1)} %bitcast.11), channel_id=1, source_target_pairs={{0,1},{1,0},{2,3},{3,2},{4,5},{5,4},{6,7},{7,6},{8,9},{9,8},{10,11... | collective-permute-start | bytes 3145736 | tf_op jit(solution)/shard_map/ppermute | solution.py:165
  87.0 5.4 %collective-permute-done.6.refs_7_ = bf16[392,512]{1,0:T(8,128)(2,1)S(1)} collective-permute-done((bf16[392,512]{1,0:T(8,128)(2,1)S(1)}, bf16[392,512]{1,0:T(8,128)(2,1)S(1)}, u32[]{:S(2)}, u32[]{:S(2)}) %collective-permute-start.6) | collective-permute-done | bytes 401440 | tf_op jit(solution)/shard_map/ppermute | solution.py:160
  92.3 2.0 %hidden.1.refs_0_ = bf16[384,256]{1,0:T(8,128)(2,1)S(1)} custom-call(bf16[392,512]{1,0:T(8,128)(2,1)S(1)} %pack.1.refs_0_, bf16[392,512]{1,0:T(8,128)(2,1)S(1)} %collective-permute-done.refs_1_, bf16[392,512]{1,0:T(8,128)(2,1)S(1)} %collective-permute-done.1.refs_2_, bf16[392,512]{1,0:T(8,128)(2,1)S(1)} %collective-permute-done.2.refs_3_, ...), custom_call_target="tpu_custom_call" | custom-call | flops 1610612736 | bytes 1048576 | tf_op jit(solution)/shard_map/hidden/pallas_call | solution.py:218
  94.3 5.0 %collective-permute-start.9 = (bf16[384,256]{1,0:T(8,128)(2,1)S(1)}, bf16[384,256]{1,0:T(8,128)(2,1)S(1)}, u32[]{:S(2)}, u32[]{:S(2)}) collective-permute-start(bf16[384,256]{1,0:T(8,128)(2,1)S(1)} %hidden.1.refs_0_), channel_id=1, source_target_pairs={{0,2},{1,15},{2,4},{3,1},{4,6},{5,3},{6,8},{7,5},{8,10},{9,7},{10,... | collective-permute-start | bytes 589832 | tf_op jit(solution)/shard_map/ppermute | solution.py:157
  102.0 5.0 %collective-permute-start.11 = (bf16[384,256]{1,0:T(8,128)(2,1)S(1)}, bf16[384,256]{1,0:T(8,128)(2,1)S(1)}, u32[]{:S(2)}, u32[]{:S(2)}) collective-permute-start(bf16[384,256]{1,0:T(8,128)(2,1)S(1)} %collective-permute-done.9.refs_1_), channel_id=1, source_target_pairs={{0,2},{1,15},{2,4},{3,1},{4,6},{5,3},{6,8},{7,5},{8,10},{9,7},{10,... | collective-permute-start | bytes 589832 | tf_op jit(solution)/shard_map/ppermute | solution.py:157
  107.0 3.7 %collective-permute-start.12 = (bf16[384,256]{1,0:T(8,128)(2,1)S(1)}, bf16[384,256]{1,0:T(8,128)(2,1)S(1)}, u32[]{:S(2)}, u32[]{:S(2)}) collective-permute-start(bf16[384,256]{1,0:T(8,128)(2,1)S(1)} %collective-permute-done.10.refs_2_), channel_id=1, source_target_pairs={{0,14},{1,3},{2,0},{3,5},{4,2},{5,7},{6,4},{7,9},{8,6},{9,11},{10,... | collective-permute-start | bytes 589832 | tf_op jit(solution)/shard_map/ppermute | solution.py:158
  111.5 3.1 %collective-permute-start.13 = (bf16[384,256]{1,0:T(8,128)(2,1)S(1)}, bf16[384,256]{1,0:T(8,128)(2,1)S(1)}, u32[]{:S(2)}, u32[]{:S(2)}) collective-permute-start(bf16[384,256]{1,0:T(8,128)(2,1)S(1)} %collective-permute-done.11.refs_3_), channel_id=1, source_target_pairs={{0,2},{1,15},{2,4},{3,1},{4,6},{5,3},{6,8},{7,5},{8,10},{9,7},{10,... | collective-permute-start | bytes 589832 | tf_op jit(solution)/shard_map/ppermute | solution.py:157
  115.2 5.0 %collective-permute-start.14 = (bf16[384,256]{1,0:T(8,128)(2,1)S(1)}, bf16[384,256]{1,0:T(8,128)(2,1)S(1)}, u32[]{:S(2)}, u32[]{:S(2)}) collective-permute-start(bf16[384,256]{1,0:T(8,128)(2,1)S(1)} %collective-permute-done.12.refs_4_), channel_id=1, source_target_pairs={{0,14},{1,3},{2,0},{3,5},{4,2},{5,7},{6,4},{7,9},{8,6},{9,11},{10,... | collective-permute-start | bytes 589832 | tf_op jit(solution)/shard_map/ppermute | solution.py:158
  122.5 2.0 %collective-permute-done.14.refs_6_ = bf16[384,256]{1,0:T(8,128)(2,1)S(1)} collective-permute-done((bf16[384,256]{1,0:T(8,128)(2,1)S(1)}, bf16[384,256]{1,0:T(8,128)(2,1)S(1)}, u32[]{:S(2)}, u32[]{:S(2)}) %collective-permute-start.14) | collective-permute-done | bytes 196640 | tf_op jit(solution)/shard_map/ppermute | solution.py:158
  124.6 5.3 %collective-permute-done.15.refs_7_ = bf16[384,256]{1,0:T(8,128)(2,1)S(1)} collective-permute-done((bf16[384,256]{1,0:T(8,128)(2,1)S(1)}, bf16[384,256]{1,0:T(8,128)(2,1)S(1)}, u32[]{:S(2)}, u32[]{:S(2)}) %collective-permute-start.15) | collective-permute-done | bytes 196640 | tf_op jit(solution)/shard_map/ppermute | solution.py:160
  130.8 30.8 %all_to_all.10 = bf16[96,8,256]{2,1,0:T(8,128)(2,1)S(1)} all-to-all(bf16[96,8,256]{2,1,0:T(8,128)(2,1)S(1)} %bitcast.10), channel_id=1, replica_groups=mesh['z'=12,'x'=4,'y'=8,'c'=2] {'z','x','c'}, dimensions={0} | all-to-all | bytes 786432 | tf_op jit(solution)/shard_map/all_to_all | solution.py:251
  (40 shorter events, 15.5 us)
Async XLA Ops:
  2.1 41.5 %all-to-all-start = ((bf16[96,8,256]{2,1,0:T(8,128)(2,1)}), bf16[96,8,256]{2,1,0:T(8,128)(2,1)S(1)}, u32[]{:S(2)}, u32[]{:S(2)}) async-start(bf16[96,8,256]{2,1,0:T(8,128)(2,1)} %bitcast.20), calls=%async_computation | async-start | bytes 786432 | tf_op jit(solution)/shard_map/all_to_all | solution.py:185
  22.8 2.3 %copy-start.8 = (f32[256,2]{0,1:T(2,128)S(1)}, f32[256,2]{0,1:T(2,128)}, u32[]{:S(2)}) copy-start(f32[256,2]{0,1:T(2,128)} %param.10) | copy-start | bytes 6148
  25.1 34.2 %copy-start.1 = (bf16[1,4096,128]{2,1,0:T(8,128)(2,1)S(1)}, bf16[1,4096,128]{2,1,0:T(8,128)(2,1)}, u32[]{:S(2)}) copy-start(bf16[1,4096,128]{2,1,0:T(8,128)(2,1)} %param.11) | copy-start | bytes 3145732
  25.1 38.5 %copy-start.2 = (bf16[1,4096,128]{2,1,0:T(8,128)(2,1)S(1)}, bf16[1,4096,128]{2,1,0:T(8,128)(2,1)}, u32[]{:S(2)}) copy-start(bf16[1,4096,128]{2,1,0:T(8,128)(2,1)} %param.12) | copy-start | bytes 3145732
  25.1 59.1 %copy-start = (bf16[1,2048,256]{2,1,0:T(8,128)(2,1)S(1)}, bf16[1,2048,256]{2,1,0:T(8,128)(2,1)}, u32[]{:S(2)}) copy-start(bf16[1,2048,256]{2,1,0:T(8,128)(2,1)} %param.13) | copy-start | bytes 3145732
  43.7 10.3 %collective-permute-start = (bf16[392,512]{1,0:T(8,128)(2,1)S(1)}, bf16[392,512]{1,0:T(8,128)(2,1)S(1)}, u32[]{:S(2)}, u32[]{:S(2)}) collective-permute-start(bf16[392,512]{1,0:T(8,128)(2,1)S(1)} %pack.1.refs_0_), channel_id=1, source_target_pairs={{0,2},{1,15},{2,4},{3,1},{4,6},{5,3},{6,8},{7,5},{8,10},{9,7},{10,... | collective-permute-start | bytes 1204232 | tf_op jit(solution)/shard_map/ppermute | solution.py:157
  48.8 16.8 %collective-permute-start.1 = (bf16[392,512]{1,0:T(8,128)(2,1)S(1)}, bf16[392,512]{1,0:T(8,128)(2,1)S(1)}, u32[]{:S(2)}, u32[]{:S(2)}) collective-permute-start(bf16[392,512]{1,0:T(8,128)(2,1)S(1)} %pack.1.refs_0_), channel_id=1, source_target_pairs={{0,14},{1,3},{2,0},{3,5},{4,2},{5,7},{6,4},{7,9},{8,6},{9,11},{10,... | collective-permute-start | bytes 1204232 | tf_op jit(solution)/shard_map/ppermute | solution.py:158
  54.0 15.7 %collective-permute-start.2 = (bf16[392,512]{1,0:T(8,128)(2,1)S(1)}, bf16[392,512]{1,0:T(8,128)(2,1)S(1)}, u32[]{:S(2)}, u32[]{:S(2)}) collective-permute-start(bf16[392,512]{1,0:T(8,128)(2,1)S(1)} %collective-permute-done.refs_1_), channel_id=1, source_target_pairs={{0,2},{1,15},{2,4},{3,1},{4,6},{5,3},{6,8},{7,5},{8,10},{9,7},{10,... | collective-permute-start | bytes 1204232 | tf_op jit(solution)/shard_map/ppermute | solution.py:157
  59.3 27.7 %collective-permute-start.7 = (bf16[4096,128]{1,0:T(8,128)(2,1)S(1)}, bf16[4096,128]{1,0:T(8,128)(2,1)S(1)}, u32[]{:S(2)}, u32[]{:S(2)}) collective-permute-start(bf16[4096,128]{1,0:T(8,128)(2,1)S(1)} %bitcast.13), channel_id=1, source_target_pairs={{0,1},{1,0},{2,3},{3,2},{4,5},{5,4},{6,7},{7,6},{8,9},{9,8},{10,11... | collective-permute-start | bytes 3145736 | tf_op jit(solution)/shard_map/ppermute | solution.py:165
  63.6 23.4 %collective-permute-start.8 = (bf16[4096,128]{1,0:T(8,128)(2,1)S(1)}, bf16[4096,128]{1,0:T(8,128)(2,1)S(1)}, u32[]{:S(2)}, u32[]{:S(2)}) collective-permute-start(bf16[4096,128]{1,0:T(8,128)(2,1)S(1)} %bitcast.15), channel_id=1, source_target_pairs={{0,1},{1,0},{2,3},{3,2},{4,5},{5,4},{6,7},{7,6},{8,9},{9,8},{10,11... | collective-permute-start | bytes 3145736 | tf_op jit(solution)/shard_map/ppermute | solution.py:165
  65.5 10.3 %collective-permute-start.3 = (bf16[392,512]{1,0:T(8,128)(2,1)S(1)}, bf16[392,512]{1,0:T(8,128)(2,1)S(1)}, u32[]{:S(2)}, u32[]{:S(2)}) collective-permute-start(bf16[392,512]{1,0:T(8,128)(2,1)S(1)} %collective-permute-done.1.refs_2_), channel_id=1, source_target_pairs={{0,14},{1,3},{2,0},{3,5},{4,2},{5,7},{6,4},{7,9},{8,6},{9,11},{10,... | collective-permute-start | bytes 1204232 | tf_op jit(solution)/shard_map/ppermute | solution.py:158
  69.6 10.5 %collective-permute-start.4 = (bf16[392,512]{1,0:T(8,128)(2,1)S(1)}, bf16[392,512]{1,0:T(8,128)(2,1)S(1)}, u32[]{:S(2)}, u32[]{:S(2)}) collective-permute-start(bf16[392,512]{1,0:T(8,128)(2,1)S(1)} %collective-permute-done.2.refs_3_), channel_id=1, source_target_pairs={{0,2},{1,15},{2,4},{3,1},{4,6},{5,3},{6,8},{7,5},{8,10},{9,7},{10,... | collective-permute-start | bytes 1204232 | tf_op jit(solution)/shard_map/ppermute | solution.py:157
  75.8 11.1 %collective-permute-start.5 = (bf16[392,512]{1,0:T(8,128)(2,1)S(1)}, bf16[392,512]{1,0:T(8,128)(2,1)S(1)}, u32[]{:S(2)}, u32[]{:S(2)}) collective-permute-start(bf16[392,512]{1,0:T(8,128)(2,1)S(1)} %collective-permute-done.3.refs_4_), channel_id=1, source_target_pairs={{0,14},{1,3},{2,0},{3,5},{4,2},{5,7},{6,4},{7,9},{8,6},{9,11},{10,... | collective-permute-start | bytes 1204232 | tf_op jit(solution)/shard_map/ppermute | solution.py:158
  80.1 12.2 %collective-permute-start.6 = (bf16[392,512]{1,0:T(8,128)(2,1)S(1)}, bf16[392,512]{1,0:T(8,128)(2,1)S(1)}, u32[]{:S(2)}, u32[]{:S(2)}) collective-permute-start(bf16[392,512]{1,0:T(8,128)(2,1)S(1)} %collective-permute-done.4.refs_5_), channel_id=1, source_target_pairs={{0,2},{1,15},{2,4},{3,1},{4,6},{5,3},{6,8},{7,5},{8,10},{9,7},{10,... | collective-permute-start | bytes 1204232 | tf_op jit(solution)/shard_map/ppermute | solution.py:160
  84.1 38.4 %collective-permute-start.16 = (bf16[2048,256]{1,0:T(8,128)(2,1)S(1)}, bf16[2048,256]{1,0:T(8,128)(2,1)S(1)}, u32[]{:S(2)}, u32[]{:S(2)}) collective-permute-start(bf16[2048,256]{1,0:T(8,128)(2,1)S(1)} %bitcast.11), channel_id=1, source_target_pairs={{0,1},{1,0},{2,3},{3,2},{4,5},{5,4},{6,7},{7,6},{8,9},{9,8},{10,11... | collective-permute-start | bytes 3145736 | tf_op jit(solution)/shard_map/ppermute | solution.py:165
  94.3 7.6 %collective-permute-start.9 = (bf16[384,256]{1,0:T(8,128)(2,1)S(1)}, bf16[384,256]{1,0:T(8,128)(2,1)S(1)}, u32[]{:S(2)}, u32[]{:S(2)}) collective-permute-start(bf16[384,256]{1,0:T(8,128)(2,1)S(1)} %hidden.1.refs_0_), channel_id=1, source_target_pairs={{0,2},{1,15},{2,4},{3,1},{4,6},{5,3},{6,8},{7,5},{8,10},{9,7},{10,... | collective-permute-start | bytes 589832 | tf_op jit(solution)/shard_map/ppermute | solution.py:157
  99.4 7.6 %collective-permute-start.10 = (bf16[384,256]{1,0:T(8,128)(2,1)S(1)}, bf16[384,256]{1,0:T(8,128)(2,1)S(1)}, u32[]{:S(2)}, u32[]{:S(2)}) collective-permute-start(bf16[384,256]{1,0:T(8,128)(2,1)S(1)} %hidden.1.refs_0_), channel_id=1, source_target_pairs={{0,14},{1,3},{2,0},{3,5},{4,2},{5,7},{6,4},{7,9},{8,6},{9,11},{10,... | collective-permute-start | bytes 589832 | tf_op jit(solution)/shard_map/ppermute | solution.py:158
  102.0 9.5 %collective-permute-start.11 = (bf16[384,256]{1,0:T(8,128)(2,1)S(1)}, bf16[384,256]{1,0:T(8,128)(2,1)S(1)}, u32[]{:S(2)}, u32[]{:S(2)}) collective-permute-start(bf16[384,256]{1,0:T(8,128)(2,1)S(1)} %collective-permute-done.9.refs_1_), channel_id=1, source_target_pairs={{0,2},{1,15},{2,4},{3,1},{4,6},{5,3},{6,8},{7,5},{8,10},{9,7},{10,... | collective-permute-start | bytes 589832 | tf_op jit(solution)/shard_map/ppermute | solution.py:157
  107.0 8.2 %collective-permute-start.12 = (bf16[384,256]{1,0:T(8,128)(2,1)S(1)}, bf16[384,256]{1,0:T(8,128)(2,1)S(1)}, u32[]{:S(2)}, u32[]{:S(2)}) collective-permute-start(bf16[384,256]{1,0:T(8,128)(2,1)S(1)} %collective-permute-done.10.refs_2_), channel_id=1, source_target_pairs={{0,14},{1,3},{2,0},{3,5},{4,2},{5,7},{6,4},{7,9},{8,6},{9,11},{10,... | collective-permute-start | bytes 589832 | tf_op jit(solution)/shard_map/ppermute | solution.py:158
  111.5 9.1 %collective-permute-start.13 = (bf16[384,256]{1,0:T(8,128)(2,1)S(1)}, bf16[384,256]{1,0:T(8,128)(2,1)S(1)}, u32[]{:S(2)}, u32[]{:S(2)}) collective-permute-start(bf16[384,256]{1,0:T(8,128)(2,1)S(1)} %collective-permute-done.11.refs_3_), channel_id=1, source_target_pairs={{0,2},{1,15},{2,4},{3,1},{4,6},{5,3},{6,8},{7,5},{8,10},{9,7},{10,... | collective-permute-start | bytes 589832 | tf_op jit(solution)/shard_map/ppermute | solution.py:157
  115.2 9.4 %collective-permute-start.14 = (bf16[384,256]{1,0:T(8,128)(2,1)S(1)}, bf16[384,256]{1,0:T(8,128)(2,1)S(1)}, u32[]{:S(2)}, u32[]{:S(2)}) collective-permute-start(bf16[384,256]{1,0:T(8,128)(2,1)S(1)} %collective-permute-done.12.refs_4_), channel_id=1, source_target_pairs={{0,14},{1,3},{2,0},{3,5},{4,2},{5,7},{6,4},{7,9},{8,6},{9,11},{10,... | collective-permute-start | bytes 589832 | tf_op jit(solution)/shard_map/ppermute | solution.py:158
  120.6 9.2 %collective-permute-start.15 = (bf16[384,256]{1,0:T(8,128)(2,1)S(1)}, bf16[384,256]{1,0:T(8,128)(2,1)S(1)}, u32[]{:S(2)}, u32[]{:S(2)}) collective-permute-start(bf16[384,256]{1,0:T(8,128)(2,1)S(1)} %collective-permute-done.13.refs_5_), channel_id=1, source_target_pairs={{0,2},{1,15},{2,4},{3,1},{4,6},{5,3},{6,8},{7,5},{8,10},{9,7},{10,... | collective-permute-start | bytes 589832 | tf_op jit(solution)/shard_map/ppermute | solution.py:160
  129.8 31.8 %copy-start.6 = (f32[2,256,128]{2,1,0:T(8,128)S(1)}, f32[2,256,128]{2,1,0:T(8,128)}, u32[]{:S(2)}) copy-start(f32[2,256,128]{2,1,0:T(8,128)} %copy-done.5) | copy-start | bytes 786436
  130.8 30.8 %copy-start.4 = (bf16[2,256,768]{2,1,0:T(8,128)(2,1)S(1)}, bf16[2,256,768]{2,1,0:T(8,128)(2,1)}, u32[]{:S(2)}) copy-start(bf16[2,256,768]{2,1,0:T(8,128)(2,1)} %copy-done.3) | copy-start | bytes 2359300
  (4 other events, 4.5 us)

commit v8 on v7

--- a/solution.py
+++ b/solution.py
@@ -83,6 +83,24 @@
 def source_of(step, count):
     turn = 1 - 2 * lax.axis_index("c")
     return lax.rem(lax.axis_index("y") - step * turn + 2 * count, count)
+
+
+def partner(y, odd, count):
+    return (((y + odd) ^ 1) - odd + count) % count
+
+
+def exchange_origins(count):
+    here, core = lax.axis_index("y"), lax.axis_index("c")
+
+    def path(turns):
+        y = here
+        for turn in turns:
+            odd = core if turn == 0 else 1 - core
+            y = lax.rem(((y + odd) ^ 1) - odd + count, count)
+        return y
+
+    turns = ((), (0,), (1,), (1, 0), (0, 1), (0, 1, 0), (1, 0, 1), (1, 0, 1, 0))
+    return [path(t) for t in turns]
 
 
 def take(refs, sizes):
@@ -131,8 +149,8 @@
     blocks, weights, before, outs = take(refs, (inputs, 2, kept, len(refs) - inputs - 2 - kept))
     rows, depth = blocks[0].shape
     total = [ref[...] for ref in before] if skip else None
-    for step, block in zip(STEPS[skip : skip + inputs], blocks):
-        start = pl.multiple_of(source_of(step, count) * depth, depth)
+    for place, block in zip(exchange_origins(count)[skip : skip + inputs], blocks):
+        start = pl.multiple_of(place * depth, depth)
         new = [dot(block[...], ref[pl.ds(start, depth), :]) for ref in weights]
         total = new if total is None else [t + n for t, n in zip(total, new)]
     if not last:
@@ -156,6 +174,22 @@
     for k in range(3):
         main = lax.ppermute(main, ("y", "c"), perm(1))
         other = lax.ppermute(other, ("y", "c"), perm(-1))
+        found += [main, other]
+    found.append(lax.ppermute(main, ("y", "c"), perm(1)))
+    return found
+
+
+def exchange(block, count):
+    def perm(turn):
+        return [
+            (y * 2 + c, partner(y, (turn + c) % 2, count) * 2 + c) for y in range(count) for c in range(2)
+        ]
+
+    main = other = block
+    found = [block]
+    for k in range(3):
+        main = lax.ppermute(main, ("y", "c"), perm(k))
+        other = lax.ppermute(other, ("y", "c"), perm(k + 1))
         found += [main, other]
     found.append(lax.ppermute(main, ("y", "c"), perm(1)))
     return found
@@ -242,7 +276,7 @@
     (made,) = product(
         down_kernel,
         "down",
-        ring(hidden, count),
+        exchange(hidden, count),
         (down, down2),
         [jax.ShapeDtypeStruct((half, width), F32)] * 2,
         [jax.ShapeDtypeStruct((experts, 2, 8, width), BF)],

time: 165 us -> 168 us (1.018)
  the two profiles are of different devices: /device:TPU:1 before, /device:TPU:24 now
where the time goes in v8:
time: 168 us; the launch traced here: 167 us
  starting transfers between devices  66.9 us (40%)
  waiting for transfers between devices  61 us (36%)
  blocking collectives  29.6 us (18%)
  Pallas kernels  6.84 us (4%)
  local copies, waits for them, and re-layouts  2.28 us (1%)
    all_to_all x1, blocking collectives, body(): lax.all_to_all(made.reshape(2 * experts, 8, width), ('z', 'x', 'c'), 0, 0...  27.7 us
    all_to_all x1, starting transfers between devices, body(): lax.all_to_all(outgoing.reshape(2 * experts, 8, width), ('z', 'x', 'c'),...  19.2 us
    all_to_all x1, waiting for transfers between devices, body(): lax.all_to_all(outgoing.reshape(2 * experts, 8, width), ('z', 'x', 'c'),...  17.4 us
    ppermute x3, waiting for transfers between devices, exchange(): main = lax.ppermute(main, ('y', 'c'), perm(k))  15.9 us
    ppermute x3, starting transfers between devices, ring(): main = lax.ppermute(main, ('y', 'c'), perm(1))  15.4 us
    ppermute x3, waiting for transfers between devices, ring(): other = lax.ppermute(other, ('y', 'c'), perm(-1))  13.3 us
    ppermute x3, waiting for transfers between devices, ring(): main = lax.ppermute(main, ('y', 'c'), perm(1))  7.6 us
    ppermute x3, starting transfers between devices, exchange(): other = lax.ppermute(other, ('y', 'c'), perm(k + 1))  7.55 us
  transfers between devices with their start and end apart: 18, of which 8 were waited for; matrix products, arithmetic and copies ran while one was open for 0% of the time, Pallas kernels for 2%

profile of v8, /device:TPU:24, one launch (start us, length us, event | category | flops | bytes accessed | tf_op | source)
XLA Modules:
  0.0 166.9 jit_solution(17947910776498901315)
XLA Ops:
  0.0 2.1 %dispatch.1 = bf16[768,256]{1,0:T(8,128)(2,1)} custom-call(s32[2,256]{1,0:T(2,128)} %bitcast.17, bf16[256,256]{1,0:T(8,128)(2,1)} %tok_ref.1), custom_call_target="tpu_custom_call" | custom-call | tf_op jit(solution)/shard_map/dispatch/pallas_call | solution.py:211
  2.1 19.2 %all-to-all-start = ((bf16[96,8,256]{2,1,0:T(8,128)(2,1)}), bf16[96,8,256]{2,1,0:T(8,128)(2,1)S(1)}, u32[]{:S(2)}, u32[]{:S(2)}) async-start(bf16[96,8,256]{2,1,0:T(8,128)(2,1)} %bitcast.20), calls=%async_computation | async-start | bytes 786432 | tf_op jit(solution)/shard_map/all_to_all | solution.py:219
  22.0 1.9 %all-gather.1.gain_ref = f32[2,1,256]{2,1,0:T(1,128)S(1)} all-gather(f32[1,1,256]{2,1,0:T(1,128)S(1)} %bitcast.21), channel_id=2, replica_groups=mesh['z'=12,'x'=4,'y'=8,'c'=2] {'c'}, dimensions={0}, use_global_device_ids=true | all-gather | bytes 3072 | tf_op jit(solution)/shard_map/all_gather | solution.py:235
  26.2 17.4 %all-to-all-done.came_ref = bf16[96,8,256]{2,1,0:T(8,128)(2,1)S(1)} async-done(((bf16[96,8,256]{2,1,0:T(8,128)(2,1)}), bf16[96,8,256]{2,1,0:T(8,128)(2,1)S(1)}, u32[]{:S(2)}, u32[]{:S(2)}) %all-to-all-start) | async-done | bytes 393248 | tf_op jit(solution)/shard_map/all_to_all | solution.py:219
  43.6 4.7 %collective-permute-start = (bf16[392,512]{1,0:T(8,128)(2,1)S(1)}, bf16[392,512]{1,0:T(8,128)(2,1)S(1)}, u32[]{:S(2)}, u32[]{:S(2)}) collective-permute-start(bf16[392,512]{1,0:T(8,128)(2,1)S(1)} %pack.1.refs_0_), channel_id=1, source_target_pairs={{0,2},{1,15},{2,4},{3,1},{4,6},{5,3},{6,8},{7,5},{8,10},{9,7},{10,... | collective-permute-start | bytes 1204232 | tf_op jit(solution)/shard_map/ppermute | solution.py:175
  48.4 1.9 %collective-permute-start.1 = (bf16[392,512]{1,0:T(8,128)(2,1)S(1)}, bf16[392,512]{1,0:T(8,128)(2,1)S(1)}, u32[]{:S(2)}, u32[]{:S(2)}) collective-permute-start(bf16[392,512]{1,0:T(8,128)(2,1)S(1)} %pack.1.refs_0_), channel_id=1, source_target_pairs={{0,14},{1,3},{2,0},{3,5},{4,2},{5,7},{6,4},{7,9},{8,6},{9,11},{10,... | collective-permute-start | bytes 1204232 | tf_op jit(solution)/shard_map/ppermute | solution.py:176
  50.3 7.6 %collective-permute-done.refs_1_ = bf16[392,512]{1,0:T(8,128)(2,1)S(1)} collective-permute-done((bf16[392,512]{1,0:T(8,128)(2,1)S(1)}, bf16[392,512]{1,0:T(8,128)(2,1)S(1)}, u32[]{:S(2)}, u32[]{:S(2)}) %collective-permute-start) | collective-permute-done | bytes 401440 | tf_op jit(solution)/shard_map/ppermute | solution.py:175
  57.9 5.6 %collective-permute-start.2 = (bf16[392,512]{1,0:T(8,128)(2,1)S(1)}, bf16[392,512]{1,0:T(8,128)(2,1)S(1)}, u32[]{:S(2)}, u32[]{:S(2)}) collective-permute-start(bf16[392,512]{1,0:T(8,128)(2,1)S(1)} %collective-permute-done.refs_1_), channel_id=1, source_target_pairs={{0,2},{1,15},{2,4},{3,1},{4,6},{5,3},{6,8},{7,5},{8,10},{9,7},{10,... | collective-permute-start | bytes 1204232 | tf_op jit(solution)/shard_map/ppermute | solution.py:175
  63.5 1.9 %collective-permute-start.7 = (bf16[4096,128]{1,0:T(8,128)(2,1)S(1)}, bf16[4096,128]{1,0:T(8,128)(2,1)S(1)}, u32[]{:S(2)}, u32[]{:S(2)}) collective-permute-start(bf16[4096,128]{1,0:T(8,128)(2,1)S(1)} %bitcast.13), channel_id=1, source_target_pairs={{0,1},{1,0},{2,3},{3,2},{4,5},{5,4},{6,7},{7,6},{8,9},{9,8},{10,11... | collective-permute-start | bytes 3145736 | tf_op jit(solution)/shard_map/ppermute | solution.py:199
  65.4 2.4 %collective-permute-start.8 = (bf16[4096,128]{1,0:T(8,128)(2,1)S(1)}, bf16[4096,128]{1,0:T(8,128)(2,1)S(1)}, u32[]{:S(2)}, u32[]{:S(2)}) collective-permute-start(bf16[4096,128]{1,0:T(8,128)(2,1)S(1)} %bitcast.15), channel_id=1, source_target_pairs={{0,1},{1,0},{2,3},{3,2},{4,5},{5,4},{6,7},{7,6},{8,9},{9,8},{10,11... | collective-permute-start | bytes 3145736 | tf_op jit(solution)/shard_map/ppermute | solution.py:199
  67.8 1.9 %collective-permute-start.3 = (bf16[392,512]{1,0:T(8,128)(2,1)S(1)}, bf16[392,512]{1,0:T(8,128)(2,1)S(1)}, u32[]{:S(2)}, u32[]{:S(2)}) collective-permute-start(bf16[392,512]{1,0:T(8,128)(2,1)S(1)} %collective-permute-done.1.refs_2_), channel_id=1, source_target_pairs={{0,14},{1,3},{2,0},{3,5},{4,2},{5,7},{6,4},{7,9},{8,6},{9,11},{10,... | collective-permute-start | bytes 1204232 | tf_op jit(solution)/shard_map/ppermute | solution.py:176
  69.8 5.1 %collective-permute-start.4 = (bf16[392,512]{1,0:T(8,128)(2,1)S(1)}, bf16[392,512]{1,0:T(8,128)(2,1)S(1)}, u32[]{:S(2)}, u32[]{:S(2)}) collective-permute-start(bf16[392,512]{1,0:T(8,128)(2,1)S(1)} %collective-permute-done.2.refs_3_), channel_id=1, source_target_pairs={{0,2},{1,15},{2,4},{3,1},{4,6},{5,3},{6,8},{7,5},{8,10},{9,7},{10,... | collective-permute-start | bytes 1204232 | tf_op jit(solution)/shard_map/ppermute | solution.py:175
  74.9 7.2 %collective-permute-done.3.refs_4_ = bf16[392,512]{1,0:T(8,128)(2,1)S(1)} collective-permute-done((bf16[392,512]{1,0:T(8,128)(2,1)S(1)}, bf16[392,512]{1,0:T(8,128)(2,1)S(1)}, u32[]{:S(2)}, u32[]{:S(2)}) %collective-permute-start.3) | collective-permute-done | bytes 401440 | tf_op jit(solution)/shard_map/ppermute | solution.py:176
  84.1 5.1 %collective-permute-start.6 = (bf16[392,512]{1,0:T(8,128)(2,1)S(1)}, bf16[392,512]{1,0:T(8,128)(2,1)S(1)}, u32[]{:S(2)}, u32[]{:S(2)}) collective-permute-start(bf16[392,512]{1,0:T(8,128)(2,1)S(1)} %collective-permute-done.4.refs_5_), channel_id=1, source_target_pairs={{0,2},{1,15},{2,4},{3,1},{4,6},{5,3},{6,8},{7,5},{8,10},{9,7},{10,... | collective-permute-start | bytes 1204232 | tf_op jit(solution)/shard_map/ppermute | solution.py:178
  91.2 6.1 %collective-permute-done.5.refs_6_ = bf16[392,512]{1,0:T(8,128)(2,1)S(1)} collective-permute-done((bf16[392,512]{1,0:T(8,128)(2,1)S(1)}, bf16[392,512]{1,0:T(8,128)(2,1)S(1)}, u32[]{:S(2)}, u32[]{:S(2)}) %collective-permute-start.5) | collective-permute-done | bytes 401440 | tf_op jit(solution)/shard_map/ppermute | solution.py:176
  97.2 2.0 %hidden.1.refs_0_ = bf16[384,256]{1,0:T(8,128)(2,1)S(1)} custom-call(bf16[392,512]{1,0:T(8,128)(2,1)S(1)} %pack.1.refs_0_, bf16[392,512]{1,0:T(8,128)(2,1)S(1)} %collective-permute-done.refs_1_, bf16[392,512]{1,0:T(8,128)(2,1)S(1)} %collective-permute-done.1.refs_2_, bf16[392,512]{1,0:T(8,128)(2,1)S(1)} %collective-permute-done.2.refs_3_, ...), custom_call_target="tpu_custom_call" | custom-call | flops 1610612736 | bytes 1048576 | tf_op jit(solution)/shard_map/hidden/pallas_call | solution.py:252
  99.2 1.9 %collective-permute-start.9 = (bf16[384,256]{1,0:T(8,128)(2,1)S(1)}, bf16[384,256]{1,0:T(8,128)(2,1)S(1)}, u32[]{:S(2)}, u32[]{:S(2)}) collective-permute-start(bf16[384,256]{1,0:T(8,128)(2,1)S(1)} %hidden.1.refs_0_), channel_id=1, source_target_pairs={{0,2},{1,15},{2,0},{3,5},{4,6},{5,3},{6,4},{7,9},{8,10},{9,7},{10,... | collective-permute-start | bytes 589832 | tf_op jit(solution)/shard_map/ppermute | solution.py:191
  101.1 2.9 %collective-permute-start.10 = (bf16[384,256]{1,0:T(8,128)(2,1)S(1)}, bf16[384,256]{1,0:T(8,128)(2,1)S(1)}, u32[]{:S(2)}, u32[]{:S(2)}) collective-permute-start(bf16[384,256]{1,0:T(8,128)(2,1)S(1)} %hidden.1.refs_0_), channel_id=1, source_target_pairs={{0,14},{1,3},{2,4},{3,1},{4,2},{5,7},{6,8},{7,5},{8,6},{9,11},{10,... | collective-permute-start | bytes 589832 | tf_op jit(solution)/shard_map/ppermute | solution.py:192
  104.1 3.9 %collective-permute-done.9.refs_1_ = bf16[384,256]{1,0:T(8,128)(2,1)S(1)} collective-permute-done((bf16[384,256]{1,0:T(8,128)(2,1)S(1)}, bf16[384,256]{1,0:T(8,128)(2,1)S(1)}, u32[]{:S(2)}, u32[]{:S(2)}) %collective-permute-start.9) | collective-permute-done | bytes 196640 | tf_op jit(solution)/shard_map/ppermute | solution.py:191
  109.9 2.7 %collective-permute-start.12 = (bf16[384,256]{1,0:T(8,128)(2,1)S(1)}, bf16[384,256]{1,0:T(8,128)(2,1)S(1)}, u32[]{:S(2)}, u32[]{:S(2)}) collective-permute-start(bf16[384,256]{1,0:T(8,128)(2,1)S(1)} %collective-permute-done.10.refs_2_), channel_id=1, source_target_pairs={{0,2},{1,15},{2,0},{3,5},{4,6},{5,3},{6,4},{7,9},{8,10},{9,7},{10,... | collective-permute-start | bytes 589832 | tf_op jit(solution)/shard_map/ppermute | solution.py:192
  112.6 6.2 %collective-permute-done.11.refs_3_ = bf16[384,256]{1,0:T(8,128)(2,1)S(1)} collective-permute-done((bf16[384,256]{1,0:T(8,128)(2,1)S(1)}, bf16[384,256]{1,0:T(8,128)(2,1)S(1)}, u32[]{:S(2)}, u32[]{:S(2)}) %collective-permute-start.11) | collective-permute-done | bytes 196640 | tf_op jit(solution)/shard_map/ppermute | solution.py:191
  122.7 5.8 %collective-permute-done.13.refs_5_ = bf16[384,256]{1,0:T(8,128)(2,1)S(1)} collective-permute-done((bf16[384,256]{1,0:T(8,128)(2,1)S(1)}, bf16[384,256]{1,0:T(8,128)(2,1)S(1)}, u32[]{:S(2)}, u32[]{:S(2)}) %collective-permute-start.13) | collective-permute-done | bytes 196640 | tf_op jit(solution)/shard_map/ppermute | solution.py:191
  130.4 6.8 %collective-permute-done.15.refs_7_ = bf16[384,256]{1,0:T(8,128)(2,1)S(1)} collective-permute-done((bf16[384,256]{1,0:T(8,128)(2,1)S(1)}, bf16[384,256]{1,0:T(8,128)(2,1)S(1)}, u32[]{:S(2)}, u32[]{:S(2)}) %collective-permute-start.15) | collective-permute-done | bytes 196640 | tf_op jit(solution)/shard_map/ppermute | solution.py:194
  138.2 27.7 %all_to_all.10 = bf16[96,8,256]{2,1,0:T(8,128)(2,1)S(1)} all-to-all(bf16[96,8,256]{2,1,0:T(8,128)(2,1)S(1)} %bitcast.10), channel_id=1, replica_groups=mesh['z'=12,'x'=4,'y'=8,'c'=2] {'z','x','c'}, dimensions={0} | all-to-all | bytes 786432 | tf_op jit(solution)/shard_map/all_to_all | solution.py:285
  (40 shorter events, 16.6 us)
Async XLA Ops:
  2.1 41.5 %all-to-all-start = ((bf16[96,8,256]{2,1,0:T(8,128)(2,1)}), bf16[96,8,256]{2,1,0:T(8,128)(2,1)S(1)}, u32[]{:S(2)}, u32[]{:S(2)}) async-start(bf16[96,8,256]{2,1,0:T(8,128)(2,1)} %bitcast.20), calls=%async_computation | async-start | bytes 786432 | tf_op jit(solution)/shard_map/all_to_all | solution.py:219
  22.0 1.9 %copy-start.8 = (f32[256,2]{0,1:T(2,128)S(1)}, f32[256,2]{0,1:T(2,128)}, u32[]{:S(2)}) copy-start(f32[256,2]{0,1:T(2,128)} %param.10) | copy-start | bytes 6148
  23.9 39.6 %copy-start.1 = (bf16[1,4096,128]{2,1,0:T(8,128)(2,1)S(1)}, bf16[1,4096,128]{2,1,0:T(8,128)(2,1)}, u32[]{:S(2)}) copy-start(bf16[1,4096,128]{2,1,0:T(8,128)(2,1)} %param.11) | copy-start | bytes 3145732
  23.9 41.5 %copy-start.2 = (bf16[1,4096,128]{2,1,0:T(8,128)(2,1)S(1)}, bf16[1,4096,128]{2,1,0:T(8,128)(2,1)}, u32[]{:S(2)}) copy-start(bf16[1,4096,128]{2,1,0:T(8,128)(2,1)} %param.12) | copy-start | bytes 3145732
  23.9 65.3 %copy-start = (bf16[1,2048,256]{2,1,0:T(8,128)(2,1)S(1)}, bf16[1,2048,256]{2,1,0:T(8,128)(2,1)}, u32[]{:S(2)}) copy-start(bf16[1,2048,256]{2,1,0:T(8,128)(2,1)} %param.13) | copy-start | bytes 3145732
  43.6 14.2 %collective-permute-start = (bf16[392,512]{1,0:T(8,128)(2,1)S(1)}, bf16[392,512]{1,0:T(8,128)(2,1)S(1)}, u32[]{:S(2)}, u32[]{:S(2)}) collective-permute-start(bf16[392,512]{1,0:T(8,128)(2,1)S(1)} %pack.1.refs_0_), channel_id=1, source_target_pairs={{0,2},{1,15},{2,4},{3,1},{4,6},{5,3},{6,8},{7,5},{8,10},{9,7},{10,... | collective-permute-start | bytes 1204232 | tf_op jit(solution)/shard_map/ppermute | solution.py:175
  48.4 19.5 %collective-permute-start.1 = (bf16[392,512]{1,0:T(8,128)(2,1)S(1)}, bf16[392,512]{1,0:T(8,128)(2,1)S(1)}, u32[]{:S(2)}, u32[]{:S(2)}) collective-permute-start(bf16[392,512]{1,0:T(8,128)(2,1)S(1)} %pack.1.refs_0_), channel_id=1, source_target_pairs={{0,14},{1,3},{2,0},{3,5},{4,2},{5,7},{6,4},{7,9},{8,6},{9,11},{10,... | collective-permute-start | bytes 1204232 | tf_op jit(solution)/shard_map/ppermute | solution.py:176
  57.9 11.9 %collective-permute-start.2 = (bf16[392,512]{1,0:T(8,128)(2,1)S(1)}, bf16[392,512]{1,0:T(8,128)(2,1)S(1)}, u32[]{:S(2)}, u32[]{:S(2)}) collective-permute-start(bf16[392,512]{1,0:T(8,128)(2,1)S(1)} %collective-permute-done.refs_1_), channel_id=1, source_target_pairs={{0,2},{1,15},{2,4},{3,1},{4,6},{5,3},{6,8},{7,5},{8,10},{9,7},{10,... | collective-permute-start | bytes 1204232 | tf_op jit(solution)/shard_map/ppermute | solution.py:175
  63.5 27.7 %collective-permute-start.7 = (bf16[4096,128]{1,0:T(8,128)(2,1)S(1)}, bf16[4096,128]{1,0:T(8,128)(2,1)S(1)}, u32[]{:S(2)}, u32[]{:S(2)}) collective-permute-start(bf16[4096,128]{1,0:T(8,128)(2,1)S(1)} %bitcast.13), channel_id=1, source_target_pairs={{0,1},{1,0},{2,3},{3,2},{4,5},{5,4},{6,7},{7,6},{8,9},{9,8},{10,11... | collective-permute-start | bytes 3145736 | tf_op jit(solution)/shard_map/ppermute | solution.py:199
  65.4 25.7 %collective-permute-start.8 = (bf16[4096,128]{1,0:T(8,128)(2,1)S(1)}, bf16[4096,128]{1,0:T(8,128)(2,1)S(1)}, u32[]{:S(2)}, u32[]{:S(2)}) collective-permute-start(bf16[4096,128]{1,0:T(8,128)(2,1)S(1)} %bitcast.15), channel_id=1, source_target_pairs={{0,1},{1,0},{2,3},{3,2},{4,5},{5,4},{6,7},{7,6},{8,9},{9,8},{10,11... | collective-permute-start | bytes 3145736 | tf_op jit(solution)/shard_map/ppermute | solution.py:199
  67.8 14.3 %collective-permute-start.3 = (bf16[392,512]{1,0:T(8,128)(2,1)S(1)}, bf16[392,512]{1,0:T(8,128)(2,1)S(1)}, u32[]{:S(2)}, u32[]{:S(2)}) collective-permute-start(bf16[392,512]{1,0:T(8,128)(2,1)S(1)} %collective-permute-done.1.refs_2_), channel_id=1, source_target_pairs={{0,14},{1,3},{2,0},{3,5},{4,2},{5,7},{6,4},{7,9},{8,6},{9,11},{10,... | collective-permute-start | bytes 1204232 | tf_op jit(solution)/shard_map/ppermute | solution.py:176
  69.8 14.3 %collective-permute-start.4 = (bf16[392,512]{1,0:T(8,128)(2,1)S(1)}, bf16[392,512]{1,0:T(8,128)(2,1)S(1)}, u32[]{:S(2)}, u32[]{:S(2)}) collective-permute-start(bf16[392,512]{1,0:T(8,128)(2,1)S(1)} %collective-permute-done.2.refs_3_), channel_id=1, source_target_pairs={{0,2},{1,15},{2,4},{3,1},{4,6},{5,3},{6,8},{7,5},{8,10},{9,7},{10,... | collective-permute-start | bytes 1204232 | tf_op jit(solution)/shard_map/ppermute | solution.py:175
  82.1 15.1 %collective-permute-start.5 = (bf16[392,512]{1,0:T(8,128)(2,1)S(1)}, bf16[392,512]{1,0:T(8,128)(2,1)S(1)}, u32[]{:S(2)}, u32[]{:S(2)}) collective-permute-start(bf16[392,512]{1,0:T(8,128)(2,1)S(1)} %collective-permute-done.3.refs_4_), channel_id=1, source_target_pairs={{0,14},{1,3},{2,0},{3,5},{4,2},{5,7},{6,4},{7,9},{8,6},{9,11},{10,... | collective-permute-start | bytes 1204232 | tf_op jit(solution)/shard_map/ppermute | solution.py:176
  84.1 13.2 %collective-permute-start.6 = (bf16[392,512]{1,0:T(8,128)(2,1)S(1)}, bf16[392,512]{1,0:T(8,128)(2,1)S(1)}, u32[]{:S(2)}, u32[]{:S(2)}) collective-permute-start(bf16[392,512]{1,0:T(8,128)(2,1)S(1)} %collective-permute-done.4.refs_5_), channel_id=1, source_target_pairs={{0,2},{1,15},{2,4},{3,1},{4,6},{5,3},{6,8},{7,5},{8,10},{9,7},{10,... | collective-permute-start | bytes 1204232 | tf_op jit(solution)/shard_map/ppermute | solution.py:178
  89.2 41.2 %collective-permute-start.16 = (bf16[2048,256]{1,0:T(8,128)(2,1)S(1)}, bf16[2048,256]{1,0:T(8,128)(2,1)S(1)}, u32[]{:S(2)}, u32[]{:S(2)}) collective-permute-start(bf16[2048,256]{1,0:T(8,128)(2,1)S(1)} %bitcast.11), channel_id=1, source_target_pairs={{0,1},{1,0},{2,3},{3,2},{4,5},{5,4},{6,7},{7,6},{8,9},{9,8},{10,11... | collective-permute-start | bytes 3145736 | tf_op jit(solution)/shard_map/ppermute | solution.py:199
  99.2 8.8 %collective-permute-start.9 = (bf16[384,256]{1,0:T(8,128)(2,1)S(1)}, bf16[384,256]{1,0:T(8,128)(2,1)S(1)}, u32[]{:S(2)}, u32[]{:S(2)}) collective-permute-start(bf16[384,256]{1,0:T(8,128)(2,1)S(1)} %hidden.1.refs_0_), channel_id=1, source_target_pairs={{0,2},{1,15},{2,0},{3,5},{4,6},{5,3},{6,4},{7,9},{8,10},{9,7},{10,... | collective-permute-start | bytes 589832 | tf_op jit(solution)/shard_map/ppermute | solution.py:191
  101.1 8.8 %collective-permute-start.10 = (bf16[384,256]{1,0:T(8,128)(2,1)S(1)}, bf16[384,256]{1,0:T(8,128)(2,1)S(1)}, u32[]{:S(2)}, u32[]{:S(2)}) collective-permute-start(bf16[384,256]{1,0:T(8,128)(2,1)S(1)} %hidden.1.refs_0_), channel_id=1, source_target_pairs={{0,14},{1,3},{2,4},{3,1},{4,2},{5,7},{6,8},{7,5},{8,6},{9,11},{10,... | collective-permute-start | bytes 589832 | tf_op jit(solution)/shard_map/ppermute | solution.py:192
  108.0 10.8 %collective-permute-start.11 = (bf16[384,256]{1,0:T(8,128)(2,1)S(1)}, bf16[384,256]{1,0:T(8,128)(2,1)S(1)}, u32[]{:S(2)}, u32[]{:S(2)}) collective-permute-start(bf16[384,256]{1,0:T(8,128)(2,1)S(1)} %collective-permute-done.9.refs_1_), channel_id=1, source_target_pairs={{0,14},{1,3},{2,4},{3,1},{4,2},{5,7},{6,8},{7,5},{8,6},{9,11},{10,... | collective-permute-start | bytes 589832 | tf_op jit(solution)/shard_map/ppermute | solution.py:191
  109.9 10.8 %collective-permute-start.12 = (bf16[384,256]{1,0:T(8,128)(2,1)S(1)}, bf16[384,256]{1,0:T(8,128)(2,1)S(1)}, u32[]{:S(2)}, u32[]{:S(2)}) collective-permute-start(bf16[384,256]{1,0:T(8,128)(2,1)S(1)} %collective-permute-done.10.refs_2_), channel_id=1, source_target_pairs={{0,2},{1,15},{2,0},{3,5},{4,6},{5,3},{6,4},{7,9},{8,10},{9,7},{10,... | collective-permute-start | bytes 589832 | tf_op jit(solution)/shard_map/ppermute | solution.py:192
  118.8 9.7 %collective-permute-start.13 = (bf16[384,256]{1,0:T(8,128)(2,1)S(1)}, bf16[384,256]{1,0:T(8,128)(2,1)S(1)}, u32[]{:S(2)}, u32[]{:S(2)}) collective-permute-start(bf16[384,256]{1,0:T(8,128)(2,1)S(1)} %collective-permute-done.11.refs_3_), channel_id=1, source_target_pairs={{0,2},{1,15},{2,0},{3,5},{4,6},{5,3},{6,4},{7,9},{8,10},{9,7},{10,... | collective-permute-start | bytes 589832 | tf_op jit(solution)/shard_map/ppermute | solution.py:191
  120.7 9.7 %collective-permute-start.14 = (bf16[384,256]{1,0:T(8,128)(2,1)S(1)}, bf16[384,256]{1,0:T(8,128)(2,1)S(1)}, u32[]{:S(2)}, u32[]{:S(2)}) collective-permute-start(bf16[384,256]{1,0:T(8,128)(2,1)S(1)} %collective-permute-done.12.refs_4_), channel_id=1, source_target_pairs={{0,14},{1,3},{2,4},{3,1},{4,2},{5,7},{6,8},{7,5},{8,6},{9,11},{10,... | collective-permute-start | bytes 589832 | tf_op jit(solution)/shard_map/ppermute | solution.py:192
  128.5 8.8 %collective-permute-start.15 = (bf16[384,256]{1,0:T(8,128)(2,1)S(1)}, bf16[384,256]{1,0:T(8,128)(2,1)S(1)}, u32[]{:S(2)}, u32[]{:S(2)}) collective-permute-start(bf16[384,256]{1,0:T(8,128)(2,1)S(1)} %collective-permute-done.13.refs_5_), channel_id=1, source_target_pairs={{0,14},{1,3},{2,4},{3,1},{4,2},{5,7},{6,8},{7,5},{8,6},{9,11},{10,... | collective-permute-start | bytes 589832 | tf_op jit(solution)/shard_map/ppermute | solution.py:194
  137.2 28.7 %copy-start.6 = (f32[2,256,128]{2,1,0:T(8,128)S(1)}, f32[2,256,128]{2,1,0:T(8,128)}, u32[]{:S(2)}) copy-start(f32[2,256,128]{2,1,0:T(8,128)} %copy-done.5) | copy-start | bytes 786436
  138.2 27.7 %copy-start.4 = (bf16[2,256,768]{2,1,0:T(8,128)(2,1)S(1)}, bf16[2,256,768]{2,1,0:T(8,128)(2,1)}, u32[]{:S(2)}) copy-start(bf16[2,256,768]{2,1,0:T(8,128)(2,1)} %copy-done.3) | copy-start | bytes 2359300
  (4 other events, 4.2 us)

commit v9 on v7

--- a/solution.py
+++ b/solution.py
@@ -6,6 +6,7 @@
 from jax.experimental import pallas as pl
 from jax.experimental.pallas import tpu as pltpu
 from jax.sharding import Mesh, PartitionSpec as P
+
 
 BF = jnp.bfloat16
 F32 = jnp.float32
@@ -153,7 +154,7 @@
 
     main = other = block
     found = [block]
-    for k in range(3):
+    for _ in range(3):
         main = lax.ppermute(main, ("y", "c"), perm(1))
         other = lax.ppermute(other, ("y", "c"), perm(-1))
         found += [main, other]
@@ -165,7 +166,7 @@
     return lax.ppermute(value, "c", [(0, 1), (1, 0)])
 
 
-def body(tokens, norm_gain, expert_ids, expert_weights, gate_weight, up_weight, down_weight):
+def layer(tokens, norm_gain, expert_ids, expert_weights, gate_weight, up_weight, down_weight):
     count = lax.axis_size("y")
     experts = lax.axis_size("z") * lax.axis_size("x")
     rows, width = tokens.shape
@@ -200,7 +201,9 @@
     came, gains, picks, shares = lax.optimization_barrier(
         (came, lax.all_gather(norm_gain[None], "c", axis=0), picks, shares)
     )
-    gate2, up2, down2 = swap(gate), swap(up), swap(down)
+    gate2 = swap(gate)
+    up2 = swap(up)
+    down2 = swap(down)
     block = call(
         pack_kernel,
         out_shape=jax.ShapeDtypeStruct((half + PAD, 2 * width), BF),
@@ -210,7 +213,7 @@
         name="pack",
     )(came, gains)
 
-    def product(kernel, name, found, weights, sums, outs, each):
+    def product(kernel, found, weights, sums, outs, each):
         total, skip = [], 0
         for group in (found,):
             last = skip + len(group) == count
@@ -224,7 +227,6 @@
                 cost_estimate=pl.CostEstimate(
                     flops=len(group) * each, bytes_accessed=1 << 20, transcendentals=0
                 ),
-                name=name,
             )(*group, *weights, *total)
             skip += len(group)
         return total
@@ -232,7 +234,6 @@
     ff = gate.shape[1]
     (hidden,) = product(
         hidden_kernel,
-        "hidden",
         ring(block, count),
         (gate, gate2, up, up2),
         [jax.ShapeDtypeStruct((half, 2 * ff), F32)] * 2 + [jax.ShapeDtypeStruct((half, 128), F32)],
@@ -241,7 +242,6 @@
     )
     (made,) = product(
         down_kernel,
-        "down",
         ring(hidden, count),
         (down, down2),
         [jax.ShapeDtypeStruct((half, width), F32)] * 2,
@@ -272,4 +272,4 @@
         P(ep, None, tp),
         P(ep, None, tp),
     )
-    return jax.shard_map(body, mesh=split, in_specs=in_specs, out_specs=P(ep, tp), check_vma=False)
+    return jax.shard_map(layer, mesh=split, in_specs=in_specs, out_specs=P(ep, tp), check_vma=False)

time: 165 us -> 165 us (level)
  no operation moved by 1% of the time
where the time goes in v9:
time: 165 us; the launch traced here: 163 us
  starting transfers between devices  81.5 us (49%)
  waiting for transfers between devices  38.7 us (23%)
  blocking collectives  33.1 us (20%)
  Pallas kernels  6.84 us (4%)
  local copies, waits for them, and re-layouts  2.28 us (1%)
    all_to_all x1, blocking collectives, layer(): lax.all_to_all(made.reshape(2 * experts, 8, width), ('z', 'x', 'c'), 0, 0...  30.8 us
    ppermute x6, starting transfers between devices, ring(): main = lax.ppermute(main, ('y', 'c'), perm(1))  25.9 us
    ppermute x6, starting transfers between devices, ring(): other = lax.ppermute(other, ('y', 'c'), perm(-1))  20.7 us
    all_to_all x1, starting transfers between devices, layer(): lax.all_to_all(outgoing.reshape(2 * experts, 8, width), ('z', 'x', 'c'),...  20 us
    all_to_all x1, waiting for transfers between devices, layer(): lax.all_to_all(outgoing.reshape(2 * experts, 8, width), ('z', 'x', 'c'),...  16.2 us
    ppermute x2, waiting for transfers between devices, ring(): found.append(lax.ppermute(main, ('y', 'c'), perm(1)))  10.6 us
    ppermute x3, starting transfers between devices, swap(): return lax.ppermute(value, 'c', [(0, 1), (1, 0)])  8.99 us
    ppermute x6, waiting for transfers between devices, ring(): other = lax.ppermute(other, ('y', 'c'), perm(-1))  6.38 us
  transfers between devices with their start and end apart: 18, of which 11 were waited for; matrix products, arithmetic and copies ran while one was open for 0% of the time, Pallas kernels for 2%

profile of v9, /device:TPU:1, one launch (start us, length us, event | category | flops | bytes accessed | tf_op | source)
XLA Modules:
  0.0 162.7 jit_solution(13475718439975352698)
XLA Ops:
  0.0 2.1 %dispatch.1 = bf16[768,256]{1,0:T(8,128)(2,1)} custom-call(s32[2,256]{1,0:T(2,128)} %bitcast.17, bf16[256,256]{1,0:T(8,128)(2,1)} %tok_ref.1), custom_call_target="tpu_custom_call" | custom-call | tf_op jit(solution)/shard_map/dispatch/pallas_call | solution.py:178
  2.1 20.0 %all-to-all-start = ((bf16[96,8,256]{2,1,0:T(8,128)(2,1)}), bf16[96,8,256]{2,1,0:T(8,128)(2,1)S(1)}, u32[]{:S(2)}, u32[]{:S(2)}) async-start(bf16[96,8,256]{2,1,0:T(8,128)(2,1)} %bitcast.20), calls=%async_computation | async-start | bytes 786432 | tf_op jit(solution)/shard_map/all_to_all | solution.py:186
  22.8 2.3 %all-gather.1.gain_ref = f32[2,1,256]{2,1,0:T(1,128)S(1)} all-gather(f32[1,1,256]{2,1,0:T(1,128)S(1)} %bitcast.21), channel_id=2, replica_groups=mesh['z'=12,'x'=4,'y'=8,'c'=2] {'c'}, dimensions={0}, use_global_device_ids=true | all-gather | bytes 3072 | tf_op jit(solution)/shard_map/all_gather | solution.py:202
  27.4 16.2 %all-to-all-done.came_ref = bf16[96,8,256]{2,1,0:T(8,128)(2,1)S(1)} async-done(((bf16[96,8,256]{2,1,0:T(8,128)(2,1)}), bf16[96,8,256]{2,1,0:T(8,128)(2,1)S(1)}, u32[]{:S(2)}, u32[]{:S(2)}) %all-to-all-start) | async-done | bytes 393248 | tf_op jit(solution)/shard_map/all_to_all | solution.py:186
  43.7 5.1 %collective-permute-start = (bf16[392,512]{1,0:T(8,128)(2,1)S(1)}, bf16[392,512]{1,0:T(8,128)(2,1)S(1)}, u32[]{:S(2)}, u32[]{:S(2)}) collective-permute-start(bf16[392,512]{1,0:T(8,128)(2,1)S(1)} %pack.1.refs_0_), channel_id=1, source_target_pairs={{0,2},{1,15},{2,4},{3,1},{4,6},{5,3},{6,8},{7,5},{8,10},{9,7},{10,... | collective-permute-start | bytes 1204232 | tf_op jit(solution)/shard_map/ppermute | solution.py:158
  50.7 3.3 %collective-permute-done.refs_1_ = bf16[392,512]{1,0:T(8,128)(2,1)S(1)} collective-permute-done((bf16[392,512]{1,0:T(8,128)(2,1)S(1)}, bf16[392,512]{1,0:T(8,128)(2,1)S(1)}, u32[]{:S(2)}, u32[]{:S(2)}) %collective-permute-start) | collective-permute-done | bytes 401440 | tf_op jit(solution)/shard_map/ppermute | solution.py:158
  54.0 5.3 %collective-permute-start.2 = (bf16[392,512]{1,0:T(8,128)(2,1)S(1)}, bf16[392,512]{1,0:T(8,128)(2,1)S(1)}, u32[]{:S(2)}, u32[]{:S(2)}) collective-permute-start(bf16[392,512]{1,0:T(8,128)(2,1)S(1)} %collective-permute-done.refs_1_), channel_id=1, source_target_pairs={{0,2},{1,15},{2,4},{3,1},{4,6},{5,3},{6,8},{7,5},{8,10},{9,7},{10,... | collective-permute-start | bytes 1204232 | tf_op jit(solution)/shard_map/ppermute | solution.py:158
  59.3 4.3 %collective-permute-start.7 = (bf16[4096,128]{1,0:T(8,128)(2,1)S(1)}, bf16[4096,128]{1,0:T(8,128)(2,1)S(1)}, u32[]{:S(2)}, u32[]{:S(2)}) collective-permute-start(bf16[4096,128]{1,0:T(8,128)(2,1)S(1)} %bitcast.13), channel_id=1, source_target_pairs={{0,1},{1,0},{2,3},{3,2},{4,5},{5,4},{6,7},{7,6},{8,9},{9,8},{10,11... | collective-permute-start | bytes 3145736 | tf_op jit(solution)/shard_map/ppermute | solution.py:166
  65.5 4.1 %collective-permute-start.3 = (bf16[392,512]{1,0:T(8,128)(2,1)S(1)}, bf16[392,512]{1,0:T(8,128)(2,1)S(1)}, u32[]{:S(2)}, u32[]{:S(2)}) collective-permute-start(bf16[392,512]{1,0:T(8,128)(2,1)S(1)} %collective-permute-done.1.refs_2_), channel_id=1, source_target_pairs={{0,14},{1,3},{2,0},{3,5},{4,2},{5,7},{6,4},{7,9},{8,6},{9,11},{10,... | collective-permute-start | bytes 1204232 | tf_op jit(solution)/shard_map/ppermute | solution.py:159
  69.6 2.4 %collective-permute-start.4 = (bf16[392,512]{1,0:T(8,128)(2,1)S(1)}, bf16[392,512]{1,0:T(8,128)(2,1)S(1)}, u32[]{:S(2)}, u32[]{:S(2)}) collective-permute-start(bf16[392,512]{1,0:T(8,128)(2,1)S(1)} %collective-permute-done.2.refs_3_), channel_id=1, source_target_pairs={{0,2},{1,15},{2,4},{3,1},{4,6},{5,3},{6,8},{7,5},{8,10},{9,7},{10,... | collective-permute-start | bytes 1204232 | tf_op jit(solution)/shard_map/ppermute | solution.py:158
  72.0 3.8 %collective-permute-done.3.refs_4_ = bf16[392,512]{1,0:T(8,128)(2,1)S(1)} collective-permute-done((bf16[392,512]{1,0:T(8,128)(2,1)S(1)}, bf16[392,512]{1,0:T(8,128)(2,1)S(1)}, u32[]{:S(2)}, u32[]{:S(2)}) %collective-permute-start.3) | collective-permute-done | bytes 401440 | tf_op jit(solution)/shard_map/ppermute | solution.py:159
  75.8 4.1 %collective-permute-start.5 = (bf16[392,512]{1,0:T(8,128)(2,1)S(1)}, bf16[392,512]{1,0:T(8,128)(2,1)S(1)}, u32[]{:S(2)}, u32[]{:S(2)}) collective-permute-start(bf16[392,512]{1,0:T(8,128)(2,1)S(1)} %collective-permute-done.3.refs_4_), channel_id=1, source_target_pairs={{0,14},{1,3},{2,0},{3,5},{4,2},{5,7},{6,4},{7,9},{8,6},{9,11},{10,... | collective-permute-start | bytes 1204232 | tf_op jit(solution)/shard_map/ppermute | solution.py:159
  80.1 4.0 %collective-permute-start.6 = (bf16[392,512]{1,0:T(8,128)(2,1)S(1)}, bf16[392,512]{1,0:T(8,128)(2,1)S(1)}, u32[]{:S(2)}, u32[]{:S(2)}) collective-permute-start(bf16[392,512]{1,0:T(8,128)(2,1)S(1)} %collective-permute-done.4.refs_5_), channel_id=1, source_target_pairs={{0,2},{1,15},{2,4},{3,1},{4,6},{5,3},{6,8},{7,5},{8,10},{9,7},{10,... | collective-permute-start | bytes 1204232 | tf_op jit(solution)/shard_map/ppermute | solution.py:161
  84.1 2.8 %collective-permute-start.16 = (bf16[2048,256]{1,0:T(8,128)(2,1)S(1)}, bf16[2048,256]{1,0:T(8,128)(2,1)S(1)}, u32[]{:S(2)}, u32[]{:S(2)}) collective-permute-start(bf16[2048,256]{1,0:T(8,128)(2,1)S(1)} %bitcast.11), channel_id=1, source_target_pairs={{0,1},{1,0},{2,3},{3,2},{4,5},{5,4},{6,7},{7,6},{8,9},{9,8},{10,11... | collective-permute-start | bytes 3145736 | tf_op jit(solution)/shard_map/ppermute | solution.py:166
  87.0 5.4 %collective-permute-done.6.refs_7_ = bf16[392,512]{1,0:T(8,128)(2,1)S(1)} collective-permute-done((bf16[392,512]{1,0:T(8,128)(2,1)S(1)}, bf16[392,512]{1,0:T(8,128)(2,1)S(1)}, u32[]{:S(2)}, u32[]{:S(2)}) %collective-permute-start.6) | collective-permute-done | bytes 401440 | tf_op jit(solution)/shard_map/ppermute | solution.py:161
  92.3 2.0 %shard_map.73.refs_0_ = bf16[384,256]{1,0:T(8,128)(2,1)S(1)} custom-call(bf16[392,512]{1,0:T(8,128)(2,1)S(1)} %pack.1.refs_0_, bf16[392,512]{1,0:T(8,128)(2,1)S(1)} %collective-permute-done.refs_1_, bf16[392,512]{1,0:T(8,128)(2,1)S(1)} %collective-permute-done.1.refs_2_, bf16[392,512]{1,0:T(8,128)(2,1)S(1)} %collective-permute-done.2.refs_3_, ...), custom_call_target="tpu_custom_call" | custom-call | flops 1610612736 | bytes 1048576 | tf_op jit(solution)/shard_map/pallas_call | solution.py:221
  94.3 5.0 %collective-permute-start.9 = (bf16[384,256]{1,0:T(8,128)(2,1)S(1)}, bf16[384,256]{1,0:T(8,128)(2,1)S(1)}, u32[]{:S(2)}, u32[]{:S(2)}) collective-permute-start(bf16[384,256]{1,0:T(8,128)(2,1)S(1)} %shard_map.73.refs_0_), channel_id=1, source_target_pairs={{0,2},{1,15},{2,4},{3,1},{4,6},{5,3},{6,8},{7,5},{8,10},{9,7},{10,... | collective-permute-start | bytes 589832 | tf_op jit(solution)/shard_map/ppermute | solution.py:158
  102.0 5.0 %collective-permute-start.11 = (bf16[384,256]{1,0:T(8,128)(2,1)S(1)}, bf16[384,256]{1,0:T(8,128)(2,1)S(1)}, u32[]{:S(2)}, u32[]{:S(2)}) collective-permute-start(bf16[384,256]{1,0:T(8,128)(2,1)S(1)} %collective-permute-done.9.refs_1_), channel_id=1, source_target_pairs={{0,2},{1,15},{2,4},{3,1},{4,6},{5,3},{6,8},{7,5},{8,10},{9,7},{10,... | collective-permute-start | bytes 589832 | tf_op jit(solution)/shard_map/ppermute | solution.py:158
  107.0 3.7 %collective-permute-start.12 = (bf16[384,256]{1,0:T(8,128)(2,1)S(1)}, bf16[384,256]{1,0:T(8,128)(2,1)S(1)}, u32[]{:S(2)}, u32[]{:S(2)}) collective-permute-start(bf16[384,256]{1,0:T(8,128)(2,1)S(1)} %collective-permute-done.10.refs_2_), channel_id=1, source_target_pairs={{0,14},{1,3},{2,0},{3,5},{4,2},{5,7},{6,4},{7,9},{8,6},{9,11},{10,... | collective-permute-start | bytes 589832 | tf_op jit(solution)/shard_map/ppermute | solution.py:159
  111.5 3.1 %collective-permute-start.13 = (bf16[384,256]{1,0:T(8,128)(2,1)S(1)}, bf16[384,256]{1,0:T(8,128)(2,1)S(1)}, u32[]{:S(2)}, u32[]{:S(2)}) collective-permute-start(bf16[384,256]{1,0:T(8,128)(2,1)S(1)} %collective-permute-done.11.refs_3_), channel_id=1, source_target_pairs={{0,2},{1,15},{2,4},{3,1},{4,6},{5,3},{6,8},{7,5},{8,10},{9,7},{10,... | collective-permute-start | bytes 589832 | tf_op jit(solution)/shard_map/ppermute | solution.py:158
  115.2 5.0 %collective-permute-start.14 = (bf16[384,256]{1,0:T(8,128)(2,1)S(1)}, bf16[384,256]{1,0:T(8,128)(2,1)S(1)}, u32[]{:S(2)}, u32[]{:S(2)}) collective-permute-start(bf16[384,256]{1,0:T(8,128)(2,1)S(1)} %collective-permute-done.12.refs_4_), channel_id=1, source_target_pairs={{0,14},{1,3},{2,0},{3,5},{4,2},{5,7},{6,4},{7,9},{8,6},{9,11},{10,... | collective-permute-start | bytes 589832 | tf_op jit(solution)/shard_map/ppermute | solution.py:159
  122.5 2.0 %collective-permute-done.14.refs_6_ = bf16[384,256]{1,0:T(8,128)(2,1)S(1)} collective-permute-done((bf16[384,256]{1,0:T(8,128)(2,1)S(1)}, bf16[384,256]{1,0:T(8,128)(2,1)S(1)}, u32[]{:S(2)}, u32[]{:S(2)}) %collective-permute-start.14) | collective-permute-done | bytes 196640 | tf_op jit(solution)/shard_map/ppermute | solution.py:159
  124.6 5.3 %collective-permute-done.15.refs_7_ = bf16[384,256]{1,0:T(8,128)(2,1)S(1)} collective-permute-done((bf16[384,256]{1,0:T(8,128)(2,1)S(1)}, bf16[384,256]{1,0:T(8,128)(2,1)S(1)}, u32[]{:S(2)}, u32[]{:S(2)}) %collective-permute-start.15) | collective-permute-done | bytes 196640 | tf_op jit(solution)/shard_map/ppermute | solution.py:161
  130.8 30.8 %all_to_all.10 = bf16[96,8,256]{2,1,0:T(8,128)(2,1)S(1)} all-to-all(bf16[96,8,256]{2,1,0:T(8,128)(2,1)S(1)} %bitcast.10), channel_id=1, replica_groups=mesh['z'=12,'x'=4,'y'=8,'c'=2] {'z','x','c'}, dimensions={0} | all-to-all | bytes 786432 | tf_op jit(solution)/shard_map/all_to_all | solution.py:251
  (40 shorter events, 15.5 us)
Async XLA Ops:
  2.1 41.5 %all-to-all-start = ((bf16[96,8,256]{2,1,0:T(8,128)(2,1)}), bf16[96,8,256]{2,1,0:T(8,128)(2,1)S(1)}, u32[]{:S(2)}, u32[]{:S(2)}) async-start(bf16[96,8,256]{2,1,0:T(8,128)(2,1)} %bitcast.20), calls=%async_computation | async-start | bytes 786432 | tf_op jit(solution)/shard_map/all_to_all | solution.py:186
  22.8 2.3 %copy-start.8 = (f32[256,2]{0,1:T(2,128)S(1)}, f32[256,2]{0,1:T(2,128)}, u32[]{:S(2)}) copy-start(f32[256,2]{0,1:T(2,128)} %param.10) | copy-start | bytes 6148
  25.1 34.2 %copy-start.1 = (bf16[1,4096,128]{2,1,0:T(8,128)(2,1)S(1)}, bf16[1,4096,128]{2,1,0:T(8,128)(2,1)}, u32[]{:S(2)}) copy-start(bf16[1,4096,128]{2,1,0:T(8,128)(2,1)} %param.11) | copy-start | bytes 3145732
  25.1 38.5 %copy-start.2 = (bf16[1,4096,128]{2,1,0:T(8,128)(2,1)S(1)}, bf16[1,4096,128]{2,1,0:T(8,128)(2,1)}, u32[]{:S(2)}) copy-start(bf16[1,4096,128]{2,1,0:T(8,128)(2,1)} %param.12) | copy-start | bytes 3145732
  25.1 59.1 %copy-start = (bf16[1,2048,256]{2,1,0:T(8,128)(2,1)S(1)}, bf16[1,2048,256]{2,1,0:T(8,128)(2,1)}, u32[]{:S(2)}) copy-start(bf16[1,2048,256]{2,1,0:T(8,128)(2,1)} %param.13) | copy-start | bytes 3145732
  43.7 10.3 %collective-permute-start = (bf16[392,512]{1,0:T(8,128)(2,1)S(1)}, bf16[392,512]{1,0:T(8,128)(2,1)S(1)}, u32[]{:S(2)}, u32[]{:S(2)}) collective-permute-start(bf16[392,512]{1,0:T(8,128)(2,1)S(1)} %pack.1.refs_0_), channel_id=1, source_target_pairs={{0,2},{1,15},{2,4},{3,1},{4,6},{5,3},{6,8},{7,5},{8,10},{9,7},{10,... | collective-permute-start | bytes 1204232 | tf_op jit(solution)/shard_map/ppermute | solution.py:158
  48.8 16.8 %collective-permute-start.1 = (bf16[392,512]{1,0:T(8,128)(2,1)S(1)}, bf16[392,512]{1,0:T(8,128)(2,1)S(1)}, u32[]{:S(2)}, u32[]{:S(2)}) collective-permute-start(bf16[392,512]{1,0:T(8,128)(2,1)S(1)} %pack.1.refs_0_), channel_id=1, source_target_pairs={{0,14},{1,3},{2,0},{3,5},{4,2},{5,7},{6,4},{7,9},{8,6},{9,11},{10,... | collective-permute-start | bytes 1204232 | tf_op jit(solution)/shard_map/ppermute | solution.py:159
  54.0 15.7 %collective-permute-start.2 = (bf16[392,512]{1,0:T(8,128)(2,1)S(1)}, bf16[392,512]{1,0:T(8,128)(2,1)S(1)}, u32[]{:S(2)}, u32[]{:S(2)}) collective-permute-start(bf16[392,512]{1,0:T(8,128)(2,1)S(1)} %collective-permute-done.refs_1_), channel_id=1, source_target_pairs={{0,2},{1,15},{2,4},{3,1},{4,6},{5,3},{6,8},{7,5},{8,10},{9,7},{10,... | collective-permute-start | bytes 1204232 | tf_op jit(solution)/shard_map/ppermute | solution.py:158
  59.3 27.7 %collective-permute-start.7 = (bf16[4096,128]{1,0:T(8,128)(2,1)S(1)}, bf16[4096,128]{1,0:T(8,128)(2,1)S(1)}, u32[]{:S(2)}, u32[]{:S(2)}) collective-permute-start(bf16[4096,128]{1,0:T(8,128)(2,1)S(1)} %bitcast.13), channel_id=1, source_target_pairs={{0,1},{1,0},{2,3},{3,2},{4,5},{5,4},{6,7},{7,6},{8,9},{9,8},{10,11... | collective-permute-start | bytes 3145736 | tf_op jit(solution)/shard_map/ppermute | solution.py:166
  63.6 23.4 %collective-permute-start.8 = (bf16[4096,128]{1,0:T(8,128)(2,1)S(1)}, bf16[4096,128]{1,0:T(8,128)(2,1)S(1)}, u32[]{:S(2)}, u32[]{:S(2)}) collective-permute-start(bf16[4096,128]{1,0:T(8,128)(2,1)S(1)} %bitcast.15), channel_id=1, source_target_pairs={{0,1},{1,0},{2,3},{3,2},{4,5},{5,4},{6,7},{7,6},{8,9},{9,8},{10,11... | collective-permute-start | bytes 3145736 | tf_op jit(solution)/shard_map/ppermute | solution.py:166
  65.5 10.3 %collective-permute-start.3 = (bf16[392,512]{1,0:T(8,128)(2,1)S(1)}, bf16[392,512]{1,0:T(8,128)(2,1)S(1)}, u32[]{:S(2)}, u32[]{:S(2)}) collective-permute-start(bf16[392,512]{1,0:T(8,128)(2,1)S(1)} %collective-permute-done.1.refs_2_), channel_id=1, source_target_pairs={{0,14},{1,3},{2,0},{3,5},{4,2},{5,7},{6,4},{7,9},{8,6},{9,11},{10,... | collective-permute-start | bytes 1204232 | tf_op jit(solution)/shard_map/ppermute | solution.py:159
  69.6 10.5 %collective-permute-start.4 = (bf16[392,512]{1,0:T(8,128)(2,1)S(1)}, bf16[392,512]{1,0:T(8,128)(2,1)S(1)}, u32[]{:S(2)}, u32[]{:S(2)}) collective-permute-start(bf16[392,512]{1,0:T(8,128)(2,1)S(1)} %collective-permute-done.2.refs_3_), channel_id=1, source_target_pairs={{0,2},{1,15},{2,4},{3,1},{4,6},{5,3},{6,8},{7,5},{8,10},{9,7},{10,... | collective-permute-start | bytes 1204232 | tf_op jit(solution)/shard_map/ppermute | solution.py:158
  75.8 11.1 %collective-permute-start.5 = (bf16[392,512]{1,0:T(8,128)(2,1)S(1)}, bf16[392,512]{1,0:T(8,128)(2,1)S(1)}, u32[]{:S(2)}, u32[]{:S(2)}) collective-permute-start(bf16[392,512]{1,0:T(8,128)(2,1)S(1)} %collective-permute-done.3.refs_4_), channel_id=1, source_target_pairs={{0,14},{1,3},{2,0},{3,5},{4,2},{5,7},{6,4},{7,9},{8,6},{9,11},{10,... | collective-permute-start | bytes 1204232 | tf_op jit(solution)/shard_map/ppermute | solution.py:159
  80.1 12.2 %collective-permute-start.6 = (bf16[392,512]{1,0:T(8,128)(2,1)S(1)}, bf16[392,512]{1,0:T(8,128)(2,1)S(1)}, u32[]{:S(2)}, u32[]{:S(2)}) collective-permute-start(bf16[392,512]{1,0:T(8,128)(2,1)S(1)} %collective-permute-done.4.refs_5_), channel_id=1, source_target_pairs={{0,2},{1,15},{2,4},{3,1},{4,6},{5,3},{6,8},{7,5},{8,10},{9,7},{10,... | collective-permute-start | bytes 1204232 | tf_op jit(solution)/shard_map/ppermute | solution.py:161
  84.1 38.4 %collective-permute-start.16 = (bf16[2048,256]{1,0:T(8,128)(2,1)S(1)}, bf16[2048,256]{1,0:T(8,128)(2,1)S(1)}, u32[]{:S(2)}, u32[]{:S(2)}) collective-permute-start(bf16[2048,256]{1,0:T(8,128)(2,1)S(1)} %bitcast.11), channel_id=1, source_target_pairs={{0,1},{1,0},{2,3},{3,2},{4,5},{5,4},{6,7},{7,6},{8,9},{9,8},{10,11... | collective-permute-start | bytes 3145736 | tf_op jit(solution)/shard_map/ppermute | solution.py:166
  94.3 7.6 %collective-permute-start.9 = (bf16[384,256]{1,0:T(8,128)(2,1)S(1)}, bf16[384,256]{1,0:T(8,128)(2,1)S(1)}, u32[]{:S(2)}, u32[]{:S(2)}) collective-permute-start(bf16[384,256]{1,0:T(8,128)(2,1)S(1)} %shard_map.73.refs_0_), channel_id=1, source_target_pairs={{0,2},{1,15},{2,4},{3,1},{4,6},{5,3},{6,8},{7,5},{8,10},{9,7},{10,... | collective-permute-start | bytes 589832 | tf_op jit(solution)/shard_map/ppermute | solution.py:158
  99.4 7.6 %collective-permute-start.10 = (bf16[384,256]{1,0:T(8,128)(2,1)S(1)}, bf16[384,256]{1,0:T(8,128)(2,1)S(1)}, u32[]{:S(2)}, u32[]{:S(2)}) collective-permute-start(bf16[384,256]{1,0:T(8,128)(2,1)S(1)} %shard_map.73.refs_0_), channel_id=1, source_target_pairs={{0,14},{1,3},{2,0},{3,5},{4,2},{5,7},{6,4},{7,9},{8,6},{9,11},{10,... | collective-permute-start | bytes 589832 | tf_op jit(solution)/shard_map/ppermute | solution.py:159
  102.0 9.5 %collective-permute-start.11 = (bf16[384,256]{1,0:T(8,128)(2,1)S(1)}, bf16[384,256]{1,0:T(8,128)(2,1)S(1)}, u32[]{:S(2)}, u32[]{:S(2)}) collective-permute-start(bf16[384,256]{1,0:T(8,128)(2,1)S(1)} %collective-permute-done.9.refs_1_), channel_id=1, source_target_pairs={{0,2},{1,15},{2,4},{3,1},{4,6},{5,3},{6,8},{7,5},{8,10},{9,7},{10,... | collective-permute-start | bytes 589832 | tf_op jit(solution)/shard_map/ppermute | solution.py:158
  107.0 8.2 %collective-permute-start.12 = (bf16[384,256]{1,0:T(8,128)(2,1)S(1)}, bf16[384,256]{1,0:T(8,128)(2,1)S(1)}, u32[]{:S(2)}, u32[]{:S(2)}) collective-permute-start(bf16[384,256]{1,0:T(8,128)(2,1)S(1)} %collective-permute-done.10.refs_2_), channel_id=1, source_target_pairs={{0,14},{1,3},{2,0},{3,5},{4,2},{5,7},{6,4},{7,9},{8,6},{9,11},{10,... | collective-permute-start | bytes 589832 | tf_op jit(solution)/shard_map/ppermute | solution.py:159
  111.5 9.1 %collective-permute-start.13 = (bf16[384,256]{1,0:T(8,128)(2,1)S(1)}, bf16[384,256]{1,0:T(8,128)(2,1)S(1)}, u32[]{:S(2)}, u32[]{:S(2)}) collective-permute-start(bf16[384,256]{1,0:T(8,128)(2,1)S(1)} %collective-permute-done.11.refs_3_), channel_id=1, source_target_pairs={{0,2},{1,15},{2,4},{3,1},{4,6},{5,3},{6,8},{7,5},{8,10},{9,7},{10,... | collective-permute-start | bytes 589832 | tf_op jit(solution)/shard_map/ppermute | solution.py:158
  115.2 9.4 %collective-permute-start.14 = (bf16[384,256]{1,0:T(8,128)(2,1)S(1)}, bf16[384,256]{1,0:T(8,128)(2,1)S(1)}, u32[]{:S(2)}, u32[]{:S(2)}) collective-permute-start(bf16[384,256]{1,0:T(8,128)(2,1)S(1)} %collective-permute-done.12.refs_4_), channel_id=1, source_target_pairs={{0,14},{1,3},{2,0},{3,5},{4,2},{5,7},{6,4},{7,9},{8,6},{9,11},{10,... | collective-permute-start | bytes 589832 | tf_op jit(solution)/shard_map/ppermute | solution.py:159
  120.6 9.2 %collective-permute-start.15 = (bf16[384,256]{1,0:T(8,128)(2,1)S(1)}, bf16[384,256]{1,0:T(8,128)(2,1)S(1)}, u32[]{:S(2)}, u32[]{:S(2)}) collective-permute-start(bf16[384,256]{1,0:T(8,128)(2,1)S(1)} %collective-permute-done.13.refs_5_), channel_id=1, source_target_pairs={{0,2},{1,15},{2,4},{3,1},{4,6},{5,3},{6,8},{7,5},{8,10},{9,7},{10,... | collective-permute-start | bytes 589832 | tf_op jit(solution)/shard_map/ppermute | solution.py:161
  129.8 31.8 %copy-start.6 = (f32[2,256,128]{2,1,0:T(8,128)S(1)}, f32[2,256,128]{2,1,0:T(8,128)}, u32[]{:S(2)}) copy-start(f32[2,256,128]{2,1,0:T(8,128)} %copy-done.5) | copy-start | bytes 786436
  130.8 30.8 %copy-start.4 = (bf16[2,256,768]{2,1,0:T(8,128)(2,1)S(1)}, bf16[2,256,768]{2,1,0:T(8,128)(2,1)}, u32[]{:S(2)}) copy-start(bf16[2,256,768]{2,1,0:T(8,128)(2,1)} %copy-done.3) | copy-start | bytes 2359300
  (4 other events, 4.5 us)
